TPU v7x, 128 devices: a whole 4x4x4 slice. The times are simulated.
128 devices in a mesh: fs: 16 (over z, y), tp: 8 (over x, core).
Axes of the slice: x: 4, y: 4, z: 4, core: 2. Of those that a mesh axis runs over, the one named last changes fastest.
Arguments:
- tokens: bfloat16 [16, 384, 2048], P('fs', None, 'tp'), may hold values from -16 to 16
- first_gate: bfloat16 [2048, 6144], P('fs', 'tp'), may hold values from -0.125 to 0.125
- first_up: bfloat16 [2048, 6144], P('fs', 'tp'), may hold values from -0.125 to 0.125
- first_down: bfloat16 [6144, 2048], P('tp', 'fs'), may hold values from -0.078125 to 0.078125
- first_gain: bfloat16 [2048], P('tp'), may hold values from 0.099609375 to 1.8984375
- glu_value: bfloat16 [2048, 1024], P('fs', 'tp'), may hold values from -0.125 to 0.125
- glu_gate: bfloat16 [2048, 1024], P('fs', 'tp'), may hold values from -0.125 to 0.125
- conv_taps: bfloat16 [31, 1024], P(None, 'tp'), may hold values from -3 to 3
- conv_gain: bfloat16 [1024], P('tp'), may hold values from 0.099609375 to 1.8984375
- conv_proj: bfloat16 [1024, 2048], P('tp', 'fs'), may hold values from -0.1875 to 0.1875
- second_gain: bfloat16 [2048], P('tp'), may hold values from 0.099609375 to 1.8984375
- last_gate: bfloat16 [2048, 6144], P('fs', 'tp'), may hold values from -0.125 to 0.125
- last_up: bfloat16 [2048, 6144], P('fs', 'tp'), may hold values from -0.125 to 0.125
- last_down: bfloat16 [6144, 2048], P('tp', 'fs'), may hold values from -0.078125 to 0.078125
- third_gain: bfloat16 [2048], P('tp'), may hold values from 0.099609375 to 1.8984375
Outputs:
- layer_out: bfloat16 [16, 384, 2048], P('fs', None, 'tp')
All inputs are finite; a program needn't handle non-finite values.
Results may differ from a plain program's by a relative error of at most 0.015.
Values may be sent and summed in bfloat16 or wider, within the bound.
No kernel may reach another device: no remote copies, remote signals or barrier semaphores. Data moves between devices by JAX's collectives and lax.ppermute only.
A program may use at most 64 MiB of HBM per device.

v0:
```python
import jax
import jax.numpy as jnp
from jax import lax
from jax.experimental import pallas as pl
from jax.experimental.pallas import tpu as pltpu
from jax.sharding import PartitionSpec as P


ALPHA = 2.0**0.25
EPSILON = 1e-05
F32 = jnp.float32
BF16 = jnp.bfloat16


def pull(value, axis, distance):
    if axis == "z":
        pairs = [(i, ((i // 4 - distance) % 4) * 4 + i % 4) for i in range(16)]
    elif axis == "y":
        pairs = [(i, (i // 4) * 4 + (i % 4 - distance) % 4) for i in range(16)]
    elif axis == "x":
        pairs = [(i, ((i // 2 - distance) % 4) * 2 + i % 2) for i in range(8)]
    else:
        pairs = [(i, i ^ 1) for i in range(8)]
    return lax.ppermute(value, "fs" if axis in "zy" else "tp", pairs)


def neighbours(value, axis):
    return pull(value, axis, 1), pull(value, axis, -1)


def opposite(after, before, axis):
    half = after.shape[0] // 2
    return pull(after[:half], axis, 1), pull(before[half:], axis, -1)


def in_ring(value, near, far):
    return jnp.concatenate([value, near[0], *far, near[1]], axis=0)


def matmul(left, right):
    return jnp.dot(left, right, preferred_element_type=F32)


def matmul_t(left, right):
    return lax.dot_general(left, right, (((1,), (1,)), ((), ())), preferred_element_type=F32)


def gated_hidden(rows, weights, width):
    block = 256
    count = width // block

    def kernel(rows_ref, gate_ref, up_ref, out_ref):
        gate = matmul(rows_ref[...], gate_ref[...])
        up = matmul(rows_ref[...], up_ref[...])
        out_ref[...] = (jax.nn.silu(gate) * up).astype(BF16)

    depth = weights.shape[0]
    return pl.pallas_call(
        kernel,
        grid=(count,),
        in_specs=[
            pl.BlockSpec(rows.shape, lambda j: (0, 0)),
            pl.BlockSpec((depth, block), lambda j: (0, j)),
            pl.BlockSpec((depth, block), lambda j: (0, count + j)),
        ],
        out_specs=pl.BlockSpec((rows.shape[0], block), lambda j: (0, j)),
        out_shape=jax.ShapeDtypeStruct((rows.shape[0], width), BF16),
        compiler_params=pltpu.CompilerParams(vmem_limit_bytes=24 * 2**20),
        name="gated_hidden",
    )(rows, weights, weights)


def rolled(value, axis, shift):
    return lax.dynamic_slice_in_dim(
        jnp.concatenate([value, value], axis=axis), shift, value.shape[axis], axis
    )


def norm_rows(values, gain):
    center = jnp.mean(values, axis=-1, keepdims=True)
    off = values - center
    spread = jnp.mean(off * off, axis=-1, keepdims=True)
    return (off * lax.rsqrt(spread + EPSILON) * gain).astype(BF16)


SIDES = (0, 1, 3, 2)


def across(value):
    blocks = [value] + [pull(value, "x", d) for d in (2, 1, 3)]
    near = jnp.concatenate([blocks[0], blocks[2], blocks[3]], axis=0)
    return near, blocks[1], pull(near, "c", 1), pull(blocks[1], "c", 1)


def summed_rows(rows_other, rows_own):
    came = pull(rows_other.astype(BF16), "c", 1)
    pair = rows_own + came.astype(F32)
    count = pair.shape[0] // 4
    pieces = [pair[count * d : count * (d + 1)] for d in range(4)]
    total = pieces[0]
    for d in (2, 1, 3):
        total = total + pull(pieces[(-d) % 4].astype(BF16), "x", d).astype(F32)
    return total


def by_owner(value, x, core):
    split = value.reshape(4, 2, -1, value.shape[-1])
    out = []
    for c in (1 - core, core):
        part = lax.dynamic_index_in_dim(split, c, 1, keepdims=False)
        out.append(rolled(part, 0, x).reshape(-1, value.shape[-1]))
    return out


def in_order(blocks, x, core):
    flat = jnp.stack(
        [
            jnp.stack([jnp.where(core == 0, a, b), jnp.where(core == 0, b, a)])
            for a, b in blocks
        ]
    )
    return rolled(flat, 0, (4 - x) % 4).reshape(-1, flat.shape[-1])


def channel_stats(mixed):
    count = mixed.shape[-1]
    mean = jnp.sum(mixed, axis=-1) / count
    off = mixed - mean[:, None]
    square = jnp.sum(off * off, axis=-1)
    both = jnp.concatenate([mean, square]).reshape(1, 1, -1)
    both = jnp.broadcast_to(both, (8, 1, both.shape[-1]))
    both = lax.all_to_all(both, "tp", split_axis=0, concat_axis=0, tiled=True)
    mean, square = both[:, 0, : mean.size], both[:, 0, mean.size :]
    center = jnp.mean(mean, axis=0)
    off = mean - center
    spread = jnp.mean(square, axis=0) / count + jnp.mean(off * off, axis=0)
    return center[:, None], spread[:, None]


def layer(
    tokens,
    first_gate,
    first_up,
    first_down,
    first_gain,
    glu_value,
    glu_gate,
    conv_taps,
    conv_gain,
    conv_proj,
    second_gain,
    last_gate,
    last_up,
    last_down,
    third_gain,
):
    tp = lax.axis_index("tp")
    fs = lax.axis_index("fs")
    x, core = tp // 2, tp % 2
    z, y = fs // 4, fs % 4
    current = tokens[0]

    early = lax.all_gather(
        jnp.concatenate([first_down.T, glu_value, glu_gate, conv_proj.T], axis=1),
        "fs",
        axis=0,
        tiled=True,
    )

    near_gate, near_up = neighbours(first_gate, "z"), neighbours(first_up, "y")
    far_gate, far_up = opposite(*near_gate, "z"), opposite(*near_up, "y")
    gate_part = in_ring(first_gate, near_gate, far_gate)
    up_part = in_ring(first_up, near_up, far_up)

    arrays = (last_gate, last_up, last_down, current, first_gain, second_gain, third_gain)
    (*last, current, g1, g2, g3), _, _ = lax.optimization_barrier((arrays, gate_part, up_part))
    last = jnp.concatenate([last[0], last[1], last[2].T], axis=1)
    (current, g1, g2, g3), last = lax.optimization_barrier(((current, g1, g2, g3), last))
    late = lax.all_gather(last, "fs", axis=0, tiled=True)

    length = current.shape[0]
    gains = jnp.pad(jnp.stack([g1, g2, g3]), ((0, 5), (0, 0)))
    rows = jnp.concatenate([current, gains], axis=0)
    blocks = [rows] + [pull(rows, "x", d) for d in (1, 2, 3)]
    blocks = [jnp.concatenate([b, pull(b, "c", 1)], axis=1) for b in blocks]
    turned = [rolled(b[:length], 1, ((y + 2 * core) % 4) * 128) for b in blocks]
    turned = rolled(jnp.concatenate(turned, axis=1), 1, ((z - x) % 4) * 512)
    some = [
        jnp.concatenate(
            [lax.dynamic_slice_in_dim(b, 48 * tp, 48, 0), b[length : length + 8]], axis=0
        )
        for b in blocks
    ]
    some = [rolled(b, 1, core * 256) for b in some]
    some = rolled(jnp.concatenate(some, axis=1), 1, ((4 - x) % 4) * 512)
    own_rows, gains = some[:48].astype(F32), some[48:51].astype(F32)

    near_gate, near_up = neighbours(gate_part, "y"), neighbours(up_part, "z")
    near_gate, near_up, turned = lax.optimization_barrier((near_gate, near_up, turned))
    far_gate, far_up = opposite(*near_gate, "y"), opposite(*near_up, "z")
    gate_of = [
        jnp.concatenate([turned[:, 512 * k + 128 * d :][:, :128] for k in range(4)], axis=1)
        for d in range(4)
    ]
    up_of = [turned[:, 512 * d : 512 * (d + 1)] for d in range(4)]

    def split_sum(left, own, near, far):
        total = matmul(left[0], own)
        total = total + matmul(left[1], near[0])
        total = total + matmul(left[3], near[1])
        total = total + matmul(left[2][:, :256], far[0])
        return total + matmul(left[2][:, 256:], far[1])

    gate = split_sum(gate_of, gate_part, near_gate, far_gate)
    up = split_sum(up_of, up_part, near_up, far_up)
    hidden = (jax.nn.silu(gate) * up).astype(BF16)

    def down(rows_other, rows_own, weight):
        return summed_rows(matmul_t(rows_other, weight), matmul_t(rows_own, weight))

    branch = down(*by_owner(hidden, x, core), early[:, :768])
    first = norm_rows(ALPHA * own_rows + 0.5 * branch, gains[0])

    def every_row(rows):
        near, far, near_other, far_other = across(rows)
        return jnp.concatenate([near, far, near_other, far_other], axis=0)

    def by_distance(values):
        count = values.shape[0] // 8
        at = [values[count * k : count * (k + 1)] for k in range(8)]
        own = [at[SIDES.index(d)] for d in range(4)]
        other = [at[4 + SIDES.index(d)] for d in range(4)]
        return own, other

    def gated_linear(rows):
        both = matmul(rows, early[:, 768:1024])
        return both[:, :128] * jax.nn.sigmoid(both[:, 128:])

    gated = in_order(list(zip(*by_distance(gated_linear(every_row(first))))), x, core)
    reach = (conv_taps.shape[0] - 1) // 2
    padded = jnp.pad(gated, ((reach, reach), (0, 0)))
    taps = conv_taps.astype(F32)
    mixed = jnp.zeros_like(gated)
    for k in range(conv_taps.shape[0]):
        mixed = mixed + taps[k] * padded[k : k + length]
    center, spread = channel_stats(mixed)
    normed = (mixed - center) * lax.rsqrt(spread + EPSILON) * conv_gain.astype(F32)
    act = jax.nn.silu(normed).astype(BF16)
    branch = down(*by_owner(act, x, core), early[:, 1024:])
    second = norm_rows(ALPHA * first.astype(F32) + branch, gains[1])

    own, other = by_distance(gated_hidden(every_row(second), late, 768))
    branch = down(
        jnp.concatenate(other, axis=0), jnp.concatenate(own, axis=0), late[:, 1536:]
    )
    out = norm_rows(ALPHA * second.astype(F32) + 0.5 * branch, gains[2])
    out = out.reshape(-1, 8, 256).transpose(1, 0, 2)
    out = lax.all_to_all(out, "tp", split_axis=0, concat_axis=0, tiled=True)
    return out.reshape(1, -1, 256)


def solution(mesh):
    return jax.shard_map(
        layer,
        mesh=mesh,
        in_specs=(
            P("fs", None, "tp"),
            P("fs", "tp"),
            P("fs", "tp"),
            P("tp", "fs"),
            P("tp"),
            P("fs", "tp"),
            P("fs", "tp"),
            P(None, "tp"),
            P("tp"),
            P("tp", "fs"),
            P("tp"),
            P("fs", "tp"),
            P("fs", "tp"),
            P("tp", "fs"),
            P("tp"),
        ),
        out_specs=P("fs", None, "tp"),
        check_vma=False,
    )
```

profile of v0, /device:TPU:1, one launch (start us, length us, event | category | flops | bytes accessed | tf_op | source)
XLA Modules:
  0.0 224.1 jit_solution(16584150162022583427)
XLA Ops:
  8.3 1.7 pad_maximum_fusion.4
  10.1 3.6 %collective-permute-start.4 = (bf16[128,768]{1,0:T(8,128)(2,1)}, bf16[128,768]{1,0:T(8,128)(2,1)S(1)}, u32[]{:S(2)}, u32[]{:S(2)}) collective-permute-start(bf16[128,768]{1,0:T(8,128)(2,1)} %param.17), channel_id=1, source_target_pairs={{0,24},{8,0},{16,8},{24,16},{32,56},{40,32},{48,40},{56,48},{64,88... | collective-permute-start | bytes 589832 | tf_op jit(solution)/shard_map/ppermute | solution.py:24
  13.7 3.8 %collective-permute-start = (bf16[128,768]{1,0:T(8,128)(2,1)}, bf16[128,768]{1,0:T(8,128)(2,1)S(1)}, u32[]{:S(2)}, u32[]{:S(2)}) collective-permute-start(bf16[128,768]{1,0:T(8,128)(2,1)} %param.16), channel_id=1, source_target_pairs={{0,96},{8,104},{16,112},{24,120},{32,0},{40,8},{48,16},{56,24},{64... | collective-permute-start | bytes 589832 | tf_op jit(solution)/shard_map/ppermute | solution.py:24
  19.2 2.7 %collective-permute-start.5 = (bf16[64,768]{1,0:T(8,128)(2,1)S(1)}, bf16[64,768]{1,0:T(8,128)(2,1)S(1)}, u32[]{:S(2)}, u32[]{:S(2)}) collective-permute-start(bf16[64,768]{1,0:T(8,128)(2,1)S(1)} %slice.599), channel_id=1, source_target_pairs={{0,24},{8,0},{16,8},{24,16},{32,56},{40,32},{48,40},{56,48},{64,88... | collective-permute-start | bytes 294920 | tf_op jit(solution)/shard_map/ppermute | solution.py:24
  22.1 2.9 %collective-permute-start.1 = (bf16[64,768]{1,0:T(8,128)(2,1)S(1)}, bf16[64,768]{1,0:T(8,128)(2,1)S(1)}, u32[]{:S(2)}, u32[]{:S(2)}) collective-permute-start(bf16[64,768]{1,0:T(8,128)(2,1)S(1)} %slice.597), channel_id=1, source_target_pairs={{0,96},{8,104},{16,112},{24,120},{32,0},{40,8},{48,16},{56,24},{64... | collective-permute-start | bytes 294920 | tf_op jit(solution)/shard_map/ppermute | solution.py:24
  25.2 1.5 collective-permute-done.7
  27.0 3.2 %collective-permute-done.3 = bf16[64,768]{1,0:T(8,128)(2,1)S(1)} collective-permute-done((bf16[64,768]{1,0:T(8,128)(2,1)S(1)}, bf16[64,768]{1,0:T(8,128)(2,1)S(1)}, u32[]{:S(2)}, u32[]{:S(2)}) %collective-permute-start.3) | collective-permute-done | bytes 98336 | tf_op jit(solution)/shard_map/ppermute | solution.py:24
  32.3 2.9 %collective-permute-start.8 = (bf16[392,256]{1,0:T(8,128)(2,1)S(1)}, bf16[392,256]{1,0:T(8,128)(2,1)S(1)}, u32[]{:S(2)}, u32[]{:S(2)}) collective-permute-start(bf16[392,256]{1,0:T(8,128)(2,1)S(1)} %pad_maximum_fusion.5), channel_id=1, source_target_pairs={{0,1},{1,0},{2,3},{3,2},{4,5},{5,4},{6,7},{7,6},{8,9},{9,8},{10,11... | collective-permute-start | bytes 602120 | tf_op jit(solution)/shard_map/ppermute | solution.py:24
  35.3 2.7 %collective-permute-start.11 = (bf16[392,256]{1,0:T(8,128)(2,1)S(1)}, bf16[392,256]{1,0:T(8,128)(2,1)S(1)}, u32[]{:S(2)}, u32[]{:S(2)}) collective-permute-start(bf16[392,256]{1,0:T(8,128)(2,1)S(1)} %pad_maximum_fusion.5), channel_id=1, source_target_pairs={{0,4},{1,5},{2,6},{3,7},{4,0},{5,1},{6,2},{7,3},{8,12},{9,13},{10,... | collective-permute-start | bytes 602120 | tf_op jit(solution)/shard_map/ppermute | solution.py:24
  41.2 2.0 collective-permute-done.11
  43.2 4.5 %collective-permute-start.15 = (bf16[512,768]{1,0:T(8,128)(2,1)S(1)}, bf16[512,768]{1,0:T(8,128)(2,1)S(1)}, u32[]{:S(2)}, u32[]{:S(2)}) collective-permute-start(bf16[512,768]{1,0:T(8,128)(2,1)S(1)} %constant_dynamic-update-slice_fusion), channel_id=1, source_target_pairs={{0,24},{8,0},{16,8},{24,16},{32,56},{40,32},{48,40},{56,48},{64,88... | collective-permute-start | bytes 2359304 | tf_op jit(solution)/shard_map/ppermute | solution.py:24
  47.7 1.9 collective-permute-start.12
  54.4 9.8 %collective-permute-done.17 = bf16[512,768]{1,0:T(8,128)(2,1)S(1)} collective-permute-done((bf16[512,768]{1,0:T(8,128)(2,1)}, bf16[512,768]{1,0:T(8,128)(2,1)S(1)}, u32[]{:S(2)}, u32[]{:S(2)}) %collective-permute-start.17) | collective-permute-done | bytes 786464 | tf_op jit(solution)/shard_map/ppermute | solution.py:24
  65.4 9.8 %collective-permute-done.15 = bf16[512,768]{1,0:T(8,128)(2,1)S(1)} collective-permute-done((bf16[512,768]{1,0:T(8,128)(2,1)S(1)}, bf16[512,768]{1,0:T(8,128)(2,1)S(1)}, u32[]{:S(2)}, u32[]{:S(2)}) %collective-permute-start.15) | collective-permute-done | bytes 786464 | tf_op jit(solution)/shard_map/ppermute | solution.py:24
  75.2 4.9 %collective-permute-done.16 = bf16[512,768]{1,0:T(8,128)(2,1)S(1)} collective-permute-done((bf16[512,768]{1,0:T(8,128)(2,1)S(1)}, bf16[512,768]{1,0:T(8,128)(2,1)S(1)}, u32[]{:S(2)}, u32[]{:S(2)}) %collective-permute-start.16) | collective-permute-done | bytes 786464 | tf_op jit(solution)/shard_map/ppermute | solution.py:24
  80.1 3.1 %collective-permute-start.21 = (bf16[256,768]{1,0:T(8,128)(2,1)S(1)}, bf16[256,768]{1,0:T(8,128)(2,1)S(1)}, u32[]{:S(2)}, u32[]{:S(2)}) collective-permute-start(bf16[256,768]{1,0:T(8,128)(2,1)S(1)} %slice.495), channel_id=1, source_target_pairs={{0,96},{8,104},{16,112},{24,120},{32,0},{40,8},{48,16},{56,24},{64... | collective-permute-start | bytes 1179656 | tf_op jit(solution)/shard_map/ppermute | solution.py:24
  87.5 7.6 %collective-permute-done.19 = bf16[256,768]{1,0:T(8,128)(2,1)S(1)} collective-permute-done((bf16[256,768]{1,0:T(8,128)(2,1)S(1)}, bf16[256,768]{1,0:T(8,128)(2,1)S(1)}, u32[]{:S(2)}, u32[]{:S(2)}) %collective-permute-start.19) | collective-permute-done | bytes 393248 | tf_op jit(solution)/shard_map/ppermute | solution.py:24
  98.4 2.8 %fusion.8 = bf16[192,2048]{1,0:T(8,128)(2,1)S(1)} fusion(bf16[192,768]{1,0:T(8,128)(2,1)S(1)} %bitcast.163, bf16[2048,1152]{0,1:T(8,128)(2,1)} %all-gather.3.cloned.1.call-done), kind=kOutput, calls=%fused_computation.8 | convolution fusion | flops 604372992 | bytes 4227072 | tf_op jit(solution)/shard_map/dot_general | solution.py:45
  101.3 2.0 collective-permute-start.23
  103.5 1.7 collective-permute-done.23
  106.1 2.8 %collective-permute-start.24 = (bf16[48,2048]{1,0:T(8,128)(2,1)S(1)}, bf16[48,2048]{1,0:T(8,128)(2,1)S(1)}, u32[]{:S(2)}, u32[]{:S(2)}) collective-permute-start(bf16[48,2048]{1,0:T(8,128)(2,1)S(1)} %get-tuple-element.85), channel_id=1, source_target_pairs={{0,4},{1,5},{2,6},{3,7},{4,0},{5,1},{6,2},{7,3},{8,12},{9,13},{10,... | collective-permute-start | bytes 589832 | tf_op jit(solution)/shard_map/ppermute | solution.py:24
  110.4 3.4 %collective-permute-done.24 = bf16[48,2048]{1,0:T(8,128)(2,1)S(1)} collective-permute-done((bf16[48,2048]{1,0:T(8,128)(2,1)S(1)}, bf16[48,2048]{1,0:T(8,128)(2,1)S(1)}, u32[]{:S(2)}, u32[]{:S(2)}) %collective-permute-start.24) | collective-permute-done | bytes 196640 | tf_op jit(solution)/shard_map/ppermute | solution.py:24
  113.8 4.4 %collective-permute-done.25 = bf16[48,2048]{1,0:T(8,128)(2,1)S(1)} collective-permute-done((bf16[48,2048]{1,0:T(8,128)(2,1)S(1)}, bf16[48,2048]{1,0:T(8,128)(2,1)S(1)}, u32[]{:S(2)}, u32[]{:S(2)}) %collective-permute-start.25) | collective-permute-done | bytes 196640 | tf_op jit(solution)/shard_map/ppermute | solution.py:24
  118.9 3.1 %collective-permute-start.27 = (bf16[48,2048]{1,0:T(8,128)(2,1)S(1)}, bf16[48,2048]{1,0:T(8,128)(2,1)S(1)}, u32[]{:S(2)}, u32[]{:S(2)}) collective-permute-start(bf16[48,2048]{1,0:T(8,128)(2,1)S(1)} %get-tuple-element.50), channel_id=1, source_target_pairs={{0,6},{1,7},{2,0},{3,1},{4,2},{5,3},{6,4},{7,5},{8,14},{9,15},{10,... | collective-permute-start | bytes 589832 | tf_op jit(solution)/shard_map/ppermute | solution.py:24
  121.9 1.7 collective-permute-start.29
  123.7 1.9 collective-permute-done.27
  125.6 4.1 %collective-permute-done.28 = bf16[48,2048]{1,0:T(8,128)(2,1)S(1)} collective-permute-done((bf16[48,2048]{1,0:T(8,128)(2,1)S(1)}, bf16[48,2048]{1,0:T(8,128)(2,1)S(1)}, u32[]{:S(2)}, u32[]{:S(2)}) %collective-permute-start.28) | collective-permute-done | bytes 196640 | tf_op jit(solution)/shard_map/ppermute | solution.py:24
  129.8 5.0 %collective-permute-start.30 = (bf16[144,2048]{1,0:T(8,128)(2,1)S(1)}, bf16[144,2048]{1,0:T(8,128)(2,1)S(1)}, u32[]{:S(2)}, u32[]{:S(2)}) collective-permute-start(bf16[144,2048]{1,0:T(8,128)(2,1)S(1)} %pad_maximum_fusion.1), channel_id=1, source_target_pairs={{0,1},{1,0},{2,3},{3,2},{4,5},{5,4},{6,7},{7,6},{8,9},{9,8},{10,11... | collective-permute-start | bytes 1769480 | tf_op jit(solution)/shard_map/ppermute | solution.py:24
  135.0 1.5 collective-permute-done.30
  139.2 3.6 %all-to-all-start = ((f32[8,1,768]{2,1,0:T(1,128)}), f32[8,1,768]{2,1,0:T(1,128)S(1)}, u32[]{:S(2)}, u32[]{:S(2)}) async-start(f32[8,1,768]{2,1,0:T(1,128)} %broadcast_in_dim.2), calls=%async_computation | async-start | bytes 49152 | tf_op jit(solution)/shard_map/all_to_all | solution.py:132
  142.9 4.8 %all-to-all-done = f32[8,1,768]{2,1,0:T(1,128)S(1)} async-done(((f32[8,1,768]{2,1,0:T(1,128)}), f32[8,1,768]{2,1,0:T(1,128)S(1)}, u32[]{:S(2)}, u32[]{:S(2)}) %all-to-all-start) | async-done | bytes 24608 | tf_op jit(solution)/shard_map/all_to_all | solution.py:132
  150.1 1.9 collective-permute-done.32
  152.0 1.4 fusion.178
  154.5 1.8 collective-permute-start.34
  156.3 4.9 %collective-permute-done.33 = bf16[48,2048]{1,0:T(8,128)(2,1)S(1)} collective-permute-done((bf16[48,2048]{1,0:T(8,128)(2,1)S(1)}, bf16[48,2048]{1,0:T(8,128)(2,1)S(1)}, u32[]{:S(2)}, u32[]{:S(2)}) %collective-permute-start.33) | collective-permute-done | bytes 196640 | tf_op jit(solution)/shard_map/ppermute | solution.py:24
  161.2 2.8 %collective-permute-done.34 = bf16[48,2048]{1,0:T(8,128)(2,1)S(1)} collective-permute-done((bf16[48,2048]{1,0:T(8,128)(2,1)S(1)}, bf16[48,2048]{1,0:T(8,128)(2,1)S(1)}, u32[]{:S(2)}, u32[]{:S(2)}) %collective-permute-start.34) | collective-permute-done | bytes 196640 | tf_op jit(solution)/shard_map/ppermute | solution.py:24
  164.0 2.1 collective-permute-done.35
  169.3 3.5 %collective-permute-done.36 = bf16[48,2048]{1,0:T(8,128)(2,1)S(1)} collective-permute-done((bf16[48,2048]{1,0:T(8,128)(2,1)S(1)}, bf16[48,2048]{1,0:T(8,128)(2,1)S(1)}, u32[]{:S(2)}, u32[]{:S(2)}) %collective-permute-start.36) | collective-permute-done | bytes 196640 | tf_op jit(solution)/shard_map/ppermute | solution.py:24
  172.8 3.2 %collective-permute-done.37 = bf16[48,2048]{1,0:T(8,128)(2,1)S(1)} collective-permute-done((bf16[48,2048]{1,0:T(8,128)(2,1)S(1)}, bf16[48,2048]{1,0:T(8,128)(2,1)S(1)}, u32[]{:S(2)}, u32[]{:S(2)}) %collective-permute-start.37) | collective-permute-done | bytes 196640 | tf_op jit(solution)/shard_map/ppermute | solution.py:24
  176.1 4.6 %collective-permute-start.39 = (bf16[144,2048]{1,0:T(8,128)(2,1)S(1)}, bf16[144,2048]{1,0:T(8,128)(2,1)S(1)}, u32[]{:S(2)}, u32[]{:S(2)}) collective-permute-start(bf16[144,2048]{1,0:T(8,128)(2,1)S(1)} %pad_maximum_fusion.2), channel_id=1, source_target_pairs={{0,1},{1,0},{2,3},{3,2},{4,5},{5,4},{6,7},{7,6},{8,9},{9,8},{10,11... | collective-permute-start | bytes 1769480 | tf_op jit(solution)/shard_map/ppermute | solution.py:24
  180.8 1.5 collective-permute-done.39
  182.6 3.7 %copy-done = bf16[2048,2304]{1,0:T(8,128)(2,1)S(1)} copy-done((bf16[2048,2304]{1,0:T(8,128)(2,1)S(1)}, bf16[2048,2304]{1,0:T(8,128)(2,1)}, u32[]{:S(2)}) %copy-start) | copy-done | bytes 9437208
  186.3 3.4 %gated_hidden.1 = bf16[384,768]{1,0:T(8,128)(2,1)S(1)} custom-call(bf16[384,2048]{1,0:T(8,128)(2,1)S(1)} %constant_dynamic-update-slice_fusion.46.rows_ref, bf16[2048,2304]{1,0:T(8,128)(2,1)S(1)} %copy-done, bf16[2048,2304]{1,0:T(8,128)(2,1)S(1)} %copy-done), custom_call_target="tpu_custom_call" | custom-call | tf_op jit(solution)/shard_map/gated_hidden/pallas_call | solution.py:58
  191.4 1.9 collective-permute-done.41
  194.8 1.5 collective-permute-start.44
  196.2 6.1 %collective-permute-done.42 = bf16[48,2048]{1,0:T(8,128)(2,1)S(1)} collective-permute-done((bf16[48,2048]{1,0:T(8,128)(2,1)S(1)}, bf16[48,2048]{1,0:T(8,128)(2,1)S(1)}, u32[]{:S(2)}, u32[]{:S(2)}) %collective-permute-start.42) | collective-permute-done | bytes 196640 | tf_op jit(solution)/shard_map/ppermute | solution.py:24
  203.4 3.8 %collective-permute-done.44 = bf16[48,2048]{1,0:T(8,128)(2,1)S(1)} collective-permute-done((bf16[48,2048]{1,0:T(8,128)(2,1)S(1)}, bf16[48,2048]{1,0:T(8,128)(2,1)S(1)}, u32[]{:S(2)}, u32[]{:S(2)}) %collective-permute-start.44) | collective-permute-done | bytes 196640 | tf_op jit(solution)/shard_map/ppermute | solution.py:24
  207.9 8.7 %all_to_all.10 = bf16[8,48,256]{2,1,0:T(8,128)(2,1)S(1)} all-to-all(bf16[8,48,256]{2,1,0:T(8,128)(2,1)S(1)} %bitcast.156), channel_id=1, replica_groups=mesh['fs'=16,'tp'=8] {'tp'}, dimensions={0} | all-to-all | bytes 393216 | tf_op jit(solution)/shard_map/all_to_all | solution.py:258
  (226 shorter events, 41.2 us)
Async XLA Ops:
  6.5 91.9 %all-gather.3.cloned.1.call-start = ((), (), s32[]{:S(2)}) async-start(), calls=%async_computation.2 | async-start | bytes 5013504 | tf_op jit(solution)/shard_map/all_gather | solution.py:163
  10.1 172.6 %all-gather.5.cloned.1.call-start = ((), (), s32[]{:S(2)}) async-start(), calls=%async_computation.3 | async-start | bytes 10027008 | tf_op jit(solution)/shard_map/all_gather | solution.py:179
  10.1 9.1 %collective-permute-start.4 = (bf16[128,768]{1,0:T(8,128)(2,1)}, bf16[128,768]{1,0:T(8,128)(2,1)S(1)}, u32[]{:S(2)}, u32[]{:S(2)}) collective-permute-start(bf16[128,768]{1,0:T(8,128)(2,1)} %param.17), channel_id=1, source_target_pairs={{0,24},{8,0},{16,8},{24,16},{32,56},{40,32},{48,40},{56,48},{64,88... | collective-permute-start | bytes 589832 | tf_op jit(solution)/shard_map/ppermute | solution.py:24
  13.7 8.2 %collective-permute-start.6 = (bf16[128,768]{1,0:T(8,128)(2,1)}, bf16[128,768]{1,0:T(8,128)(2,1)S(1)}, u32[]{:S(2)}, u32[]{:S(2)}) collective-permute-start(bf16[128,768]{1,0:T(8,128)(2,1)} %param.17), channel_id=1, source_target_pairs={{0,8},{8,16},{16,24},{24,0},{32,40},{40,48},{48,56},{56,32},{64,72... | collective-permute-start | bytes 589832 | tf_op jit(solution)/shard_map/ppermute | solution.py:24
  13.7 8.3 %collective-permute-start = (bf16[128,768]{1,0:T(8,128)(2,1)}, bf16[128,768]{1,0:T(8,128)(2,1)S(1)}, u32[]{:S(2)}, u32[]{:S(2)}) collective-permute-start(bf16[128,768]{1,0:T(8,128)(2,1)} %param.16), channel_id=1, source_target_pairs={{0,96},{8,104},{16,112},{24,120},{32,0},{40,8},{48,16},{56,24},{64... | collective-permute-start | bytes 589832 | tf_op jit(solution)/shard_map/ppermute | solution.py:24
  17.5 7.5 %collective-permute-start.2 = (bf16[128,768]{1,0:T(8,128)(2,1)}, bf16[128,768]{1,0:T(8,128)(2,1)S(1)}, u32[]{:S(2)}, u32[]{:S(2)}) collective-permute-start(bf16[128,768]{1,0:T(8,128)(2,1)} %param.16), channel_id=1, source_target_pairs={{0,32},{8,40},{16,48},{24,56},{32,64},{40,72},{48,80},{56,88},{64,... | collective-permute-start | bytes 589832 | tf_op jit(solution)/shard_map/ppermute | solution.py:24
  19.2 6.0 %collective-permute-start.5 = (bf16[64,768]{1,0:T(8,128)(2,1)S(1)}, bf16[64,768]{1,0:T(8,128)(2,1)S(1)}, u32[]{:S(2)}, u32[]{:S(2)}) collective-permute-start(bf16[64,768]{1,0:T(8,128)(2,1)S(1)} %slice.599), channel_id=1, source_target_pairs={{0,24},{8,0},{16,8},{24,16},{32,56},{40,32},{48,40},{56,48},{64,88... | collective-permute-start | bytes 294920 | tf_op jit(solution)/shard_map/ppermute | solution.py:24
  22.0 4.7 %collective-permute-start.7 = (bf16[64,768]{1,0:T(8,128)(2,1)S(1)}, bf16[64,768]{1,0:T(8,128)(2,1)S(1)}, u32[]{:S(2)}, u32[]{:S(2)}) collective-permute-start(bf16[64,768]{1,0:T(8,128)(2,1)S(1)} %slice.600), channel_id=1, source_target_pairs={{0,8},{8,16},{16,24},{24,0},{32,40},{40,48},{48,56},{56,32},{64,72... | collective-permute-start | bytes 294920 | tf_op jit(solution)/shard_map/ppermute | solution.py:24
  22.1 4.9 %collective-permute-start.1 = (bf16[64,768]{1,0:T(8,128)(2,1)S(1)}, bf16[64,768]{1,0:T(8,128)(2,1)S(1)}, u32[]{:S(2)}, u32[]{:S(2)}) collective-permute-start(bf16[64,768]{1,0:T(8,128)(2,1)S(1)} %slice.597), channel_id=1, source_target_pairs={{0,96},{8,104},{16,112},{24,120},{32,0},{40,8},{48,16},{56,24},{64... | collective-permute-start | bytes 294920 | tf_op jit(solution)/shard_map/ppermute | solution.py:24
  25.0 5.2 %collective-permute-start.3 = (bf16[64,768]{1,0:T(8,128)(2,1)S(1)}, bf16[64,768]{1,0:T(8,128)(2,1)S(1)}, u32[]{:S(2)}, u32[]{:S(2)}) collective-permute-start(bf16[64,768]{1,0:T(8,128)(2,1)S(1)} %slice.598), channel_id=1, source_target_pairs={{0,32},{8,40},{16,48},{24,56},{32,64},{40,72},{48,80},{56,88},{64,... | collective-permute-start | bytes 294920 | tf_op jit(solution)/shard_map/ppermute | solution.py:24
  32.3 7.4 %collective-permute-start.8 = (bf16[392,256]{1,0:T(8,128)(2,1)S(1)}, bf16[392,256]{1,0:T(8,128)(2,1)S(1)}, u32[]{:S(2)}, u32[]{:S(2)}) collective-permute-start(bf16[392,256]{1,0:T(8,128)(2,1)S(1)} %pad_maximum_fusion.5), channel_id=1, source_target_pairs={{0,1},{1,0},{2,3},{3,2},{4,5},{5,4},{6,7},{7,6},{8,9},{9,8},{10,11... | collective-permute-start | bytes 602120 | tf_op jit(solution)/shard_map/ppermute | solution.py:24
  35.3 8.0 %collective-permute-start.11 = (bf16[392,256]{1,0:T(8,128)(2,1)S(1)}, bf16[392,256]{1,0:T(8,128)(2,1)S(1)}, u32[]{:S(2)}, u32[]{:S(2)}) collective-permute-start(bf16[392,256]{1,0:T(8,128)(2,1)S(1)} %pad_maximum_fusion.5), channel_id=1, source_target_pairs={{0,4},{1,5},{2,6},{3,7},{4,0},{5,1},{6,2},{7,3},{8,12},{9,13},{10,... | collective-permute-start | bytes 602120 | tf_op jit(solution)/shard_map/ppermute | solution.py:24
  38.0 11.8 %collective-permute-start.9 = (bf16[392,256]{1,0:T(8,128)(2,1)S(1)}, bf16[392,256]{1,0:T(8,128)(2,1)S(1)}, u32[]{:S(2)}, u32[]{:S(2)}) collective-permute-start(bf16[392,256]{1,0:T(8,128)(2,1)S(1)} %pad_maximum_fusion.5), channel_id=1, source_target_pairs={{0,6},{1,7},{2,0},{3,1},{4,2},{5,3},{6,4},{7,5},{8,14},{9,15},{10,... | collective-permute-start | bytes 602120 | tf_op jit(solution)/shard_map/ppermute | solution.py:24
  38.9 8.8 %collective-permute-start.13 = (bf16[392,256]{1,0:T(8,128)(2,1)S(1)}, bf16[392,256]{1,0:T(8,128)(2,1)S(1)}, u32[]{:S(2)}, u32[]{:S(2)}) collective-permute-start(bf16[392,256]{1,0:T(8,128)(2,1)S(1)} %pad_maximum_fusion.5), channel_id=1, source_target_pairs={{0,2},{1,3},{2,4},{3,5},{4,6},{5,7},{6,0},{7,1},{8,10},{9,11},{10,... | collective-permute-start | bytes 602120 | tf_op jit(solution)/shard_map/ppermute | solution.py:24
  39.6 24.7 %collective-permute-start.17 = (bf16[512,768]{1,0:T(8,128)(2,1)}, bf16[512,768]{1,0:T(8,128)(2,1)S(1)}, u32[]{:S(2)}, u32[]{:S(2)}) collective-permute-start(bf16[512,768]{1,0:T(8,128)(2,1)} %copy-done.7), channel_id=1, source_target_pairs={{0,96},{8,104},{16,112},{24,120},{32,0},{40,8},{48,16},{56,24},{64... | collective-permute-start | bytes 2359304 | tf_op jit(solution)/shard_map/ppermute | solution.py:24
  39.7 25.7 %collective-permute-start.18 = (bf16[512,768]{1,0:T(8,128)(2,1)}, bf16[512,768]{1,0:T(8,128)(2,1)S(1)}, u32[]{:S(2)}, u32[]{:S(2)}) collective-permute-start(bf16[512,768]{1,0:T(8,128)(2,1)} %copy-done.7), channel_id=1, source_target_pairs={{0,32},{8,40},{16,48},{24,56},{32,64},{40,72},{48,80},{56,88},{64,... | collective-permute-start | bytes 2359304 | tf_op jit(solution)/shard_map/ppermute | solution.py:24
  43.2 31.9 %collective-permute-start.15 = (bf16[512,768]{1,0:T(8,128)(2,1)S(1)}, bf16[512,768]{1,0:T(8,128)(2,1)S(1)}, u32[]{:S(2)}, u32[]{:S(2)}) collective-permute-start(bf16[512,768]{1,0:T(8,128)(2,1)S(1)} %constant_dynamic-update-slice_fusion), channel_id=1, source_target_pairs={{0,24},{8,0},{16,8},{24,16},{32,56},{40,32},{48,40},{56,48},{64,88... | collective-permute-start | bytes 2359304 | tf_op jit(solution)/shard_map/ppermute | solution.py:24
  47.7 2.9 %collective-permute-start.12 = (bf16[392,256]{1,0:T(8,128)(2,1)S(1)}, bf16[392,256]{1,0:T(8,128)(2,1)S(1)}, u32[]{:S(2)}, u32[]{:S(2)}) collective-permute-start(bf16[392,256]{1,0:T(8,128)(2,1)S(1)} %collective-permute-done.11), channel_id=1, source_target_pairs={{0,1},{1,0},{2,3},{3,2},{4,5},{5,4},{6,7},{7,6},{8,9},{9,8},{10,11... | collective-permute-start | bytes 602120 | tf_op jit(solution)/shard_map/ppermute | solution.py:24
  49.8 1.5 collective-permute-start.14
  50.7 29.4 %collective-permute-start.16 = (bf16[512,768]{1,0:T(8,128)(2,1)S(1)}, bf16[512,768]{1,0:T(8,128)(2,1)S(1)}, u32[]{:S(2)}, u32[]{:S(2)}) collective-permute-start(bf16[512,768]{1,0:T(8,128)(2,1)S(1)} %constant_dynamic-update-slice_fusion), channel_id=1, source_target_pairs={{0,8},{8,16},{16,24},{24,0},{32,40},{40,48},{48,56},{56,32},{64,72... | collective-permute-start | bytes 2359304 | tf_op jit(solution)/shard_map/ppermute | solution.py:24
  51.3 1.4 collective-permute-start.10
  80.1 15.7 %collective-permute-start.21 = (bf16[256,768]{1,0:T(8,128)(2,1)S(1)}, bf16[256,768]{1,0:T(8,128)(2,1)S(1)}, u32[]{:S(2)}, u32[]{:S(2)}) collective-permute-start(bf16[256,768]{1,0:T(8,128)(2,1)S(1)} %slice.495), channel_id=1, source_target_pairs={{0,96},{8,104},{16,112},{24,120},{32,0},{40,8},{48,16},{56,24},{64... | collective-permute-start | bytes 1179656 | tf_op jit(solution)/shard_map/ppermute | solution.py:24
  83.3 12.8 %collective-permute-start.22 = (bf16[256,768]{1,0:T(8,128)(2,1)S(1)}, bf16[256,768]{1,0:T(8,128)(2,1)S(1)}, u32[]{:S(2)}, u32[]{:S(2)}) collective-permute-start(bf16[256,768]{1,0:T(8,128)(2,1)S(1)} %slice.497), channel_id=1, source_target_pairs={{0,32},{8,40},{16,48},{24,56},{32,64},{40,72},{48,80},{56,88},{64,... | collective-permute-start | bytes 1179656 | tf_op jit(solution)/shard_map/ppermute | solution.py:24
  83.4 11.7 %collective-permute-start.19 = (bf16[256,768]{1,0:T(8,128)(2,1)S(1)}, bf16[256,768]{1,0:T(8,128)(2,1)S(1)}, u32[]{:S(2)}, u32[]{:S(2)}) collective-permute-start(bf16[256,768]{1,0:T(8,128)(2,1)S(1)} %slice.487), channel_id=1, source_target_pairs={{0,24},{8,0},{16,8},{24,16},{32,56},{40,32},{48,40},{56,48},{64,88... | collective-permute-start | bytes 1179656 | tf_op jit(solution)/shard_map/ppermute | solution.py:24
  84.3 11.1 %collective-permute-start.20 = (bf16[256,768]{1,0:T(8,128)(2,1)S(1)}, bf16[256,768]{1,0:T(8,128)(2,1)S(1)}, u32[]{:S(2)}, u32[]{:S(2)}) collective-permute-start(bf16[256,768]{1,0:T(8,128)(2,1)S(1)} %slice.490), channel_id=1, source_target_pairs={{0,8},{8,16},{16,24},{24,0},{32,40},{40,48},{48,56},{56,32},{64,72... | collective-permute-start | bytes 1179656 | tf_op jit(solution)/shard_map/ppermute | solution.py:24
  101.3 3.9 %collective-permute-start.23 = (bf16[192,2048]{1,0:T(8,128)(2,1)S(1)}, bf16[192,2048]{1,0:T(8,128)(2,1)S(1)}, u32[]{:S(2)}, u32[]{:S(2)}) collective-permute-start(bf16[192,2048]{1,0:T(8,128)(2,1)S(1)} %fusion.8), channel_id=1, source_target_pairs={{0,1},{1,0},{2,3},{3,2},{4,5},{5,4},{6,7},{7,6},{8,9},{9,8},{10,11... | collective-permute-start | bytes 2359304 | tf_op jit(solution)/shard_map/ppermute | solution.py:24
  106.1 7.7 %collective-permute-start.24 = (bf16[48,2048]{1,0:T(8,128)(2,1)S(1)}, bf16[48,2048]{1,0:T(8,128)(2,1)S(1)}, u32[]{:S(2)}, u32[]{:S(2)}) collective-permute-start(bf16[48,2048]{1,0:T(8,128)(2,1)S(1)} %get-tuple-element.85), channel_id=1, source_target_pairs={{0,4},{1,5},{2,6},{3,7},{4,0},{5,1},{6,2},{7,3},{8,12},{9,13},{10,... | collective-permute-start | bytes 589832 | tf_op jit(solution)/shard_map/ppermute | solution.py:24
  108.9 9.3 %collective-permute-start.25 = (bf16[48,2048]{1,0:T(8,128)(2,1)S(1)}, bf16[48,2048]{1,0:T(8,128)(2,1)S(1)}, u32[]{:S(2)}, u32[]{:S(2)}) collective-permute-start(bf16[48,2048]{1,0:T(8,128)(2,1)S(1)} %get-tuple-element.87), channel_id=1, source_target_pairs={{0,6},{1,7},{2,0},{3,1},{4,2},{5,3},{6,4},{7,5},{8,14},{9,15},{10,... | collective-permute-start | bytes 589832 | tf_op jit(solution)/shard_map/ppermute | solution.py:24
  109.8 8.5 %collective-permute-start.26 = (bf16[48,2048]{1,0:T(8,128)(2,1)S(1)}, bf16[48,2048]{1,0:T(8,128)(2,1)S(1)}, u32[]{:S(2)}, u32[]{:S(2)}) collective-permute-start(bf16[48,2048]{1,0:T(8,128)(2,1)S(1)} %get-tuple-element.86), channel_id=1, source_target_pairs={{0,2},{1,3},{2,4},{3,5},{4,6},{5,7},{6,0},{7,1},{8,10},{9,11},{10,... | collective-permute-start | bytes 589832 | tf_op jit(solution)/shard_map/ppermute | solution.py:24
  118.9 6.8 %collective-permute-start.27 = (bf16[48,2048]{1,0:T(8,128)(2,1)S(1)}, bf16[48,2048]{1,0:T(8,128)(2,1)S(1)}, u32[]{:S(2)}, u32[]{:S(2)}) collective-permute-start(bf16[48,2048]{1,0:T(8,128)(2,1)S(1)} %get-tuple-element.50), channel_id=1, source_target_pairs={{0,6},{1,7},{2,0},{3,1},{4,2},{5,3},{6,4},{7,5},{8,14},{9,15},{10,... | collective-permute-start | bytes 589832 | tf_op jit(solution)/shard_map/ppermute | solution.py:24
  121.9 7.8 %collective-permute-start.28 = (bf16[48,2048]{1,0:T(8,128)(2,1)S(1)}, bf16[48,2048]{1,0:T(8,128)(2,1)S(1)}, u32[]{:S(2)}, u32[]{:S(2)}) collective-permute-start(bf16[48,2048]{1,0:T(8,128)(2,1)S(1)} %get-tuple-element.50), channel_id=1, source_target_pairs={{0,2},{1,3},{2,4},{3,5},{4,6},{5,7},{6,0},{7,1},{8,10},{9,11},{10,... | collective-permute-start | bytes 589832 | tf_op jit(solution)/shard_map/ppermute | solution.py:24
  121.9 12.9 %collective-permute-start.29 = (bf16[48,2048]{1,0:T(8,128)(2,1)S(1)}, bf16[48,2048]{1,0:T(8,128)(2,1)S(1)}, u32[]{:S(2)}, u32[]{:S(2)}) collective-permute-start(bf16[48,2048]{1,0:T(8,128)(2,1)S(1)} %get-tuple-element.50), channel_id=1, source_target_pairs={{0,4},{1,5},{2,6},{3,7},{4,0},{5,1},{6,2},{7,3},{8,12},{9,13},{10,... | collective-permute-start | bytes 589832 | tf_op jit(solution)/shard_map/ppermute | solution.py:24
  129.8 6.7 %collective-permute-start.30 = (bf16[144,2048]{1,0:T(8,128)(2,1)S(1)}, bf16[144,2048]{1,0:T(8,128)(2,1)S(1)}, u32[]{:S(2)}, u32[]{:S(2)}) collective-permute-start(bf16[144,2048]{1,0:T(8,128)(2,1)S(1)} %pad_maximum_fusion.1), channel_id=1, source_target_pairs={{0,1},{1,0},{2,3},{3,2},{4,5},{5,4},{6,7},{7,6},{8,9},{9,8},{10,11... | collective-permute-start | bytes 1769480 | tf_op jit(solution)/shard_map/ppermute | solution.py:24
  134.8 1.9 collective-permute-start.31
  139.2 8.4 %all-to-all-start = ((f32[8,1,768]{2,1,0:T(1,128)}), f32[8,1,768]{2,1,0:T(1,128)S(1)}, u32[]{:S(2)}, u32[]{:S(2)}) async-start(f32[8,1,768]{2,1,0:T(1,128)} %broadcast_in_dim.2), calls=%async_computation | async-start | bytes 49152 | tf_op jit(solution)/shard_map/all_to_all | solution.py:132
  149.4 2.7 %collective-permute-start.32 = (bf16[192,2048]{1,0:T(8,128)(2,1)S(1)}, bf16[192,2048]{1,0:T(8,128)(2,1)S(1)}, u32[]{:S(2)}, u32[]{:S(2)}) collective-permute-start(bf16[192,2048]{1,0:T(8,128)(2,1)S(1)} %convolution_convert_fusion), channel_id=1, source_target_pairs={{0,1},{1,0},{2,3},{3,2},{4,5},{5,4},{6,7},{7,6},{8,9},{9,8},{10,11... | collective-permute-start | bytes 2359304 | tf_op jit(solution)/shard_map/ppermute | solution.py:24
  153.5 7.7 %collective-permute-start.33 = (bf16[48,2048]{1,0:T(8,128)(2,1)S(1)}, bf16[48,2048]{1,0:T(8,128)(2,1)S(1)}, u32[]{:S(2)}, u32[]{:S(2)}) collective-permute-start(bf16[48,2048]{1,0:T(8,128)(2,1)S(1)} %get-tuple-element.82), channel_id=1, source_target_pairs={{0,4},{1,5},{2,6},{3,7},{4,0},{5,1},{6,2},{7,3},{8,12},{9,13},{10,... | collective-permute-start | bytes 589832 | tf_op jit(solution)/shard_map/ppermute | solution.py:24
  154.5 9.5 %collective-permute-start.34 = (bf16[48,2048]{1,0:T(8,128)(2,1)S(1)}, bf16[48,2048]{1,0:T(8,128)(2,1)S(1)}, u32[]{:S(2)}, u32[]{:S(2)}) collective-permute-start(bf16[48,2048]{1,0:T(8,128)(2,1)S(1)} %get-tuple-element.84), channel_id=1, source_target_pairs={{0,6},{1,7},{2,0},{3,1},{4,2},{5,3},{6,4},{7,5},{8,14},{9,15},{10,... | collective-permute-start | bytes 589832 | tf_op jit(solution)/shard_map/ppermute | solution.py:24
  156.3 9.8 %collective-permute-start.35 = (bf16[48,2048]{1,0:T(8,128)(2,1)S(1)}, bf16[48,2048]{1,0:T(8,128)(2,1)S(1)}, u32[]{:S(2)}, u32[]{:S(2)}) collective-permute-start(bf16[48,2048]{1,0:T(8,128)(2,1)S(1)} %get-tuple-element.83), channel_id=1, source_target_pairs={{0,2},{1,3},{2,4},{3,5},{4,6},{5,7},{6,0},{7,1},{8,10},{9,11},{10,... | collective-permute-start | bytes 589832 | tf_op jit(solution)/shard_map/ppermute | solution.py:24
  166.7 6.0 %collective-permute-start.36 = (bf16[48,2048]{1,0:T(8,128)(2,1)S(1)}, bf16[48,2048]{1,0:T(8,128)(2,1)S(1)}, u32[]{:S(2)}, u32[]{:S(2)}) collective-permute-start(bf16[48,2048]{1,0:T(8,128)(2,1)S(1)} %get-tuple-element.44), channel_id=1, source_target_pairs={{0,6},{1,7},{2,0},{3,1},{4,2},{5,3},{6,4},{7,5},{8,14},{9,15},{10,... | collective-permute-start | bytes 589832 | tf_op jit(solution)/shard_map/ppermute | solution.py:24
  167.8 8.2 %collective-permute-start.37 = (bf16[48,2048]{1,0:T(8,128)(2,1)S(1)}, bf16[48,2048]{1,0:T(8,128)(2,1)S(1)}, u32[]{:S(2)}, u32[]{:S(2)}) collective-permute-start(bf16[48,2048]{1,0:T(8,128)(2,1)S(1)} %get-tuple-element.44), channel_id=1, source_target_pairs={{0,2},{1,3},{2,4},{3,5},{4,6},{5,7},{6,0},{7,1},{8,10},{9,11},{10,... | collective-permute-start | bytes 589832 | tf_op jit(solution)/shard_map/ppermute | solution.py:24
  168.3 12.4 %collective-permute-start.38 = (bf16[48,2048]{1,0:T(8,128)(2,1)S(1)}, bf16[48,2048]{1,0:T(8,128)(2,1)S(1)}, u32[]{:S(2)}, u32[]{:S(2)}) collective-permute-start(bf16[48,2048]{1,0:T(8,128)(2,1)S(1)} %get-tuple-element.44), channel_id=1, source_target_pairs={{0,4},{1,5},{2,6},{3,7},{4,0},{5,1},{6,2},{7,3},{8,12},{9,13},{10,... | collective-permute-start | bytes 589832 | tf_op jit(solution)/shard_map/ppermute | solution.py:24
  176.1 6.2 %collective-permute-start.39 = (bf16[144,2048]{1,0:T(8,128)(2,1)S(1)}, bf16[144,2048]{1,0:T(8,128)(2,1)S(1)}, u32[]{:S(2)}, u32[]{:S(2)}) collective-permute-start(bf16[144,2048]{1,0:T(8,128)(2,1)S(1)} %pad_maximum_fusion.2), channel_id=1, source_target_pairs={{0,1},{1,0},{2,3},{3,2},{4,5},{5,4},{6,7},{7,6},{8,9},{9,8},{10,11... | collective-permute-start | bytes 1769480 | tf_op jit(solution)/shard_map/ppermute | solution.py:24
  180.7 1.9 collective-permute-start.40
  191.0 2.4 %collective-permute-start.41 = (bf16[192,2048]{1,0:T(8,128)(2,1)S(1)}, bf16[192,2048]{1,0:T(8,128)(2,1)S(1)}, u32[]{:S(2)}, u32[]{:S(2)}) collective-permute-start(bf16[192,2048]{1,0:T(8,128)(2,1)S(1)} %fusion.11), channel_id=1, source_target_pairs={{0,1},{1,0},{2,3},{3,2},{4,5},{5,4},{6,7},{7,6},{8,9},{9,8},{10,11... | collective-permute-start | bytes 2359304 | tf_op jit(solution)/shard_map/ppermute | solution.py:24
  194.6 7.7 %collective-permute-start.42 = (bf16[48,2048]{1,0:T(8,128)(2,1)S(1)}, bf16[48,2048]{1,0:T(8,128)(2,1)S(1)}, u32[]{:S(2)}, u32[]{:S(2)}) collective-permute-start(bf16[48,2048]{1,0:T(8,128)(2,1)S(1)} %get-tuple-element.79), channel_id=1, source_target_pairs={{0,4},{1,5},{2,6},{3,7},{4,0},{5,1},{6,2},{7,3},{8,12},{9,13},{10,... | collective-permute-start | bytes 589832 | tf_op jit(solution)/shard_map/ppermute | solution.py:24
  194.7 8.7 %collective-permute-start.43 = (bf16[48,2048]{1,0:T(8,128)(2,1)S(1)}, bf16[48,2048]{1,0:T(8,128)(2,1)S(1)}, u32[]{:S(2)}, u32[]{:S(2)}) collective-permute-start(bf16[48,2048]{1,0:T(8,128)(2,1)S(1)} %get-tuple-element.81), channel_id=1, source_target_pairs={{0,6},{1,7},{2,0},{3,1},{4,2},{5,3},{6,4},{7,5},{8,14},{9,15},{10,... | collective-permute-start | bytes 589832 | tf_op jit(solution)/shard_map/ppermute | solution.py:24
  194.8 12.4 %collective-permute-start.44 = (bf16[48,2048]{1,0:T(8,128)(2,1)S(1)}, bf16[48,2048]{1,0:T(8,128)(2,1)S(1)}, u32[]{:S(2)}, u32[]{:S(2)}) collective-permute-start(bf16[48,2048]{1,0:T(8,128)(2,1)S(1)} %get-tuple-element.80), channel_id=1, source_target_pairs={{0,2},{1,3},{2,4},{3,5},{4,6},{5,7},{6,0},{7,1},{8,10},{9,11},{10,... | collective-permute-start | bytes 589832 | tf_op jit(solution)/shard_map/ppermute | solution.py:24
  (13 other events, 89.7 us)
Sparse Core Ops, SparseCore 0:
  10.2 77.4 all-gather.2
  89.8 77.9 all-gather.4
where the time goes:
time: 225 us; the launch traced here: 224 us
  waiting for transfers between devices  98 us (44%)
  starting transfers between devices  66.2 us (29%)
  between operations  14.5 us (6%)
  matrix products  13.7 us (6%)
  local copies, waits for them, and re-layouts  11 us (5%)
  blocking collectives  8.74 us (4%)
  other arithmetic  8.59 us (4%)
  Pallas kernels  3.45 us (2%)
    ppermute x45, waiting for transfers between devices, pull(): return lax.ppermute(value, 'fs' if axis in 'zy' else 'tp', pairs)  93.1 us
    ppermute x45, starting transfers between devices, pull(): return lax.ppermute(value, 'fs' if axis in 'zy' else 'tp', pairs)  62.6 us
    unnamed x51, local copies, waits for them, and re-layouts  8.89 us
    dot_general x6, matrix products, matmul_t(): lax.dot_general(left, right, (((1,), (1,)), ((), ())), preferred_element_...  8.8 us
    all_to_all x1, blocking collectives, layer(): out = lax.all_to_all(out, 'tp', split_axis=0, concat_axis=0, tiled=True)  8.74 us
    dot_general x11, matrix products, matmul(): return jnp.dot(left, right, preferred_element_type=F32)  4.91 us
    all_to_all x1, waiting for transfers between devices, channel_stats(): both = lax.all_to_all(both, 'tp', split_axis=0, concat_axis=0, tiled=True)  4.75 us
  transfers between devices with their start and end apart: 48, of which 32 were waited for; matrix products, arithmetic and copies ran while one was open for 9% of the time, Pallas kernels for 0%

commit v1 on v0

--- a/solution.py
+++ b/solution.py
@@ -89,10 +89,12 @@
 def across(value):
     blocks = [value] + [pull(value, "x", d) for d in (2, 1, 3)]
     near = jnp.concatenate([blocks[0], blocks[2], blocks[3]], axis=0)
-    return near, blocks[1], pull(near, "c", 1), pull(blocks[1], "c", 1)
+    near_other = pull(near, "c", 1)
+    return near, blocks[1], near_other, pull(blocks[1], "c", 1)
 
 
 def summed_rows(rows_other, rows_own):
+    rows_own = lax.optimization_barrier(rows_own)
     came = pull(rows_other.astype(BF16), "c", 1)
     pair = rows_own + came.astype(F32)
     count = pair.shape[0] // 4
@@ -249,7 +251,8 @@
     branch = down(*by_owner(act, x, core), early[:, 1024:])
     second = norm_rows(ALPHA * first.astype(F32) + branch, gains[1])
 
-    own, other = by_distance(gated_hidden(every_row(second), late, 768))
+    rows = every_row(second)
+    own, other = by_distance(gated_hidden(rows, late, 768))
     branch = down(
         jnp.concatenate(other, axis=0), jnp.concatenate(own, axis=0), late[:, 1536:]
     )

time: 225 us -> 223 us (level)
  waiting for transfers between devices: 98 us -> 94.8 us
    ppermute x45, waiting for transfers between devices: 93.1 us -> 90 us  [pull(): return lax.ppermute(value, 'fs' if axis in 'zy' else 'tp', pairs)]
  transfers between devices with their start and end apart: 48 -> 48, of which waited for: 32 -> 32; matrix products, arithmetic and copies ran while one was open for 9% -> 10% of each run, Pallas kernels for 0% -> 0%
where the time goes in v1:
time: 223 us; the launch traced here: 222 us
  waiting for transfers between devices  94.8 us (43%)
  starting transfers between devices  66.8 us (30%)
  between operations  14.5 us (7%)
  matrix products  13.7 us (6%)
  local copies, waits for them, and re-layouts  10.9 us (5%)
  other arithmetic  9.42 us (4%)
  blocking collectives  8.74 us (4%)
  Pallas kernels  3.45 us (2%)
    ppermute x45, waiting for transfers between devices, pull(): return lax.ppermute(value, 'fs' if axis in 'zy' else 'tp', pairs)  90 us
    ppermute x45, starting transfers between devices, pull(): return lax.ppermute(value, 'fs' if axis in 'zy' else 'tp', pairs)  63.1 us
    unnamed x51, local copies, waits for them, and re-layouts  8.89 us
    dot_general x6, matrix products, matmul_t(): lax.dot_general(left, right, (((1,), (1,)), ((), ())), preferred_element_...  8.76 us
    all_to_all x1, blocking collectives, layer(): out = lax.all_to_all(out, 'tp', split_axis=0, concat_axis=0, tiled=True)  8.74 us
    dot_general x11, matrix products, matmul(): return jnp.dot(left, right, preferred_element_type=F32)  4.96 us
    all_to_all x1, waiting for transfers between devices, channel_stats(): both = lax.all_to_all(both, 'tp', split_axis=0, concat_axis=0, tiled=True)  4.75 us
  transfers between devices with their start and end apart: 48, of which 32 were waited for; matrix products, arithmetic and copies ran while one was open for 10% of the time, Pallas kernels for 0%

profile of v1, /device:TPU:1, one launch (start us, length us, event | category | flops | bytes accessed | tf_op | source)
XLA Modules:
  0.0 222.4 jit_solution(12126519263752985397)
XLA Ops:
  8.3 1.7 pad_maximum_fusion.4
  10.1 3.6 %collective-permute-start.4 = (bf16[128,768]{1,0:T(8,128)(2,1)}, bf16[128,768]{1,0:T(8,128)(2,1)S(1)}, u32[]{:S(2)}, u32[]{:S(2)}) collective-permute-start(bf16[128,768]{1,0:T(8,128)(2,1)} %param.17), channel_id=1, source_target_pairs={{0,24},{8,0},{16,8},{24,16},{32,56},{40,32},{48,40},{56,48},{64,88... | collective-permute-start | bytes 589832 | tf_op jit(solution)/shard_map/ppermute | solution.py:24
  13.7 3.8 %collective-permute-start = (bf16[128,768]{1,0:T(8,128)(2,1)}, bf16[128,768]{1,0:T(8,128)(2,1)S(1)}, u32[]{:S(2)}, u32[]{:S(2)}) collective-permute-start(bf16[128,768]{1,0:T(8,128)(2,1)} %param.16), channel_id=1, source_target_pairs={{0,96},{8,104},{16,112},{24,120},{32,0},{40,8},{48,16},{56,24},{64... | collective-permute-start | bytes 589832 | tf_op jit(solution)/shard_map/ppermute | solution.py:24
  19.2 2.7 %collective-permute-start.5 = (bf16[64,768]{1,0:T(8,128)(2,1)S(1)}, bf16[64,768]{1,0:T(8,128)(2,1)S(1)}, u32[]{:S(2)}, u32[]{:S(2)}) collective-permute-start(bf16[64,768]{1,0:T(8,128)(2,1)S(1)} %slice.599), channel_id=1, source_target_pairs={{0,24},{8,0},{16,8},{24,16},{32,56},{40,32},{48,40},{56,48},{64,88... | collective-permute-start | bytes 294920 | tf_op jit(solution)/shard_map/ppermute | solution.py:24
  22.1 2.9 %collective-permute-start.1 = (bf16[64,768]{1,0:T(8,128)(2,1)S(1)}, bf16[64,768]{1,0:T(8,128)(2,1)S(1)}, u32[]{:S(2)}, u32[]{:S(2)}) collective-permute-start(bf16[64,768]{1,0:T(8,128)(2,1)S(1)} %slice.597), channel_id=1, source_target_pairs={{0,96},{8,104},{16,112},{24,120},{32,0},{40,8},{48,16},{56,24},{64... | collective-permute-start | bytes 294920 | tf_op jit(solution)/shard_map/ppermute | solution.py:24
  25.2 1.5 collective-permute-done.7
  27.0 3.2 %collective-permute-done.3 = bf16[64,768]{1,0:T(8,128)(2,1)S(1)} collective-permute-done((bf16[64,768]{1,0:T(8,128)(2,1)S(1)}, bf16[64,768]{1,0:T(8,128)(2,1)S(1)}, u32[]{:S(2)}, u32[]{:S(2)}) %collective-permute-start.3) | collective-permute-done | bytes 98336 | tf_op jit(solution)/shard_map/ppermute | solution.py:24
  32.3 2.9 %collective-permute-start.8 = (bf16[392,256]{1,0:T(8,128)(2,1)S(1)}, bf16[392,256]{1,0:T(8,128)(2,1)S(1)}, u32[]{:S(2)}, u32[]{:S(2)}) collective-permute-start(bf16[392,256]{1,0:T(8,128)(2,1)S(1)} %pad_maximum_fusion.5), channel_id=1, source_target_pairs={{0,1},{1,0},{2,3},{3,2},{4,5},{5,4},{6,7},{7,6},{8,9},{9,8},{10,11... | collective-permute-start | bytes 602120 | tf_op jit(solution)/shard_map/ppermute | solution.py:24
  35.3 2.7 %collective-permute-start.11 = (bf16[392,256]{1,0:T(8,128)(2,1)S(1)}, bf16[392,256]{1,0:T(8,128)(2,1)S(1)}, u32[]{:S(2)}, u32[]{:S(2)}) collective-permute-start(bf16[392,256]{1,0:T(8,128)(2,1)S(1)} %pad_maximum_fusion.5), channel_id=1, source_target_pairs={{0,4},{1,5},{2,6},{3,7},{4,0},{5,1},{6,2},{7,3},{8,12},{9,13},{10,... | collective-permute-start | bytes 602120 | tf_op jit(solution)/shard_map/ppermute | solution.py:24
  39.7 1.4 collective-permute-start.18
  41.2 2.0 collective-permute-done.11
  43.2 4.5 %collective-permute-start.15 = (bf16[512,768]{1,0:T(8,128)(2,1)S(1)}, bf16[512,768]{1,0:T(8,128)(2,1)S(1)}, u32[]{:S(2)}, u32[]{:S(2)}) collective-permute-start(bf16[512,768]{1,0:T(8,128)(2,1)S(1)} %constant_dynamic-update-slice_fusion), channel_id=1, source_target_pairs={{0,24},{8,0},{16,8},{24,16},{32,56},{40,32},{48,40},{56,48},{64,88... | collective-permute-start | bytes 2359304 | tf_op jit(solution)/shard_map/ppermute | solution.py:24
  47.7 1.9 collective-permute-start.12
  51.5 1.2 collective-permute-done.10
  54.5 9.8 %collective-permute-done.17 = bf16[512,768]{1,0:T(8,128)(2,1)S(1)} collective-permute-done((bf16[512,768]{1,0:T(8,128)(2,1)}, bf16[512,768]{1,0:T(8,128)(2,1)S(1)}, u32[]{:S(2)}, u32[]{:S(2)}) %collective-permute-start.17) | collective-permute-done | bytes 786464 | tf_op jit(solution)/shard_map/ppermute | solution.py:24
  65.4 9.7 %collective-permute-done.15 = bf16[512,768]{1,0:T(8,128)(2,1)S(1)} collective-permute-done((bf16[512,768]{1,0:T(8,128)(2,1)S(1)}, bf16[512,768]{1,0:T(8,128)(2,1)S(1)}, u32[]{:S(2)}, u32[]{:S(2)}) %collective-permute-start.15) | collective-permute-done | bytes 786464 | tf_op jit(solution)/shard_map/ppermute | solution.py:24
  75.2 4.9 %collective-permute-done.16 = bf16[512,768]{1,0:T(8,128)(2,1)S(1)} collective-permute-done((bf16[512,768]{1,0:T(8,128)(2,1)S(1)}, bf16[512,768]{1,0:T(8,128)(2,1)S(1)}, u32[]{:S(2)}, u32[]{:S(2)}) %collective-permute-start.16) | collective-permute-done | bytes 786464 | tf_op jit(solution)/shard_map/ppermute | solution.py:24
  80.6 3.1 %collective-permute-start.21 = (bf16[256,768]{1,0:T(8,128)(2,1)S(1)}, bf16[256,768]{1,0:T(8,128)(2,1)S(1)}, u32[]{:S(2)}, u32[]{:S(2)}) collective-permute-start(bf16[256,768]{1,0:T(8,128)(2,1)S(1)} %slice.495), channel_id=1, source_target_pairs={{0,96},{8,104},{16,112},{24,120},{32,0},{40,8},{48,16},{56,24},{64... | collective-permute-start | bytes 1179656 | tf_op jit(solution)/shard_map/ppermute | solution.py:24
  87.5 7.6 %collective-permute-done.19 = bf16[256,768]{1,0:T(8,128)(2,1)S(1)} collective-permute-done((bf16[256,768]{1,0:T(8,128)(2,1)S(1)}, bf16[256,768]{1,0:T(8,128)(2,1)S(1)}, u32[]{:S(2)}, u32[]{:S(2)}) %collective-permute-start.19) | collective-permute-done | bytes 393248 | tf_op jit(solution)/shard_map/ppermute | solution.py:24
  98.5 2.8 %fusion.8 = bf16[192,2048]{1,0:T(8,128)(2,1)S(1)} fusion(bf16[192,768]{1,0:T(8,128)(2,1)S(1)} %bitcast.163, bf16[2048,1152]{0,1:T(8,128)(2,1)} %all-gather.3.cloned.1.call-done), kind=kOutput, calls=%fused_computation.8 | convolution fusion | flops 604372992 | bytes 4227072 | tf_op jit(solution)/shard_map/dot_general | solution.py:45
  101.3 2.7 %collective-permute-start.23 = (bf16[192,2048]{1,0:T(8,128)(2,1)S(1)}, bf16[192,2048]{1,0:T(8,128)(2,1)S(1)}, u32[]{:S(2)}, u32[]{:S(2)}) collective-permute-start(bf16[192,2048]{1,0:T(8,128)(2,1)S(1)} %fusion.8), channel_id=1, source_target_pairs={{0,1},{1,0},{2,3},{3,2},{4,5},{5,4},{6,7},{7,6},{8,9},{9,8},{10,11... | collective-permute-start | bytes 2359304 | tf_op jit(solution)/shard_map/ppermute | solution.py:24
  106.3 2.8 %collective-permute-start.24 = (bf16[48,2048]{1,0:T(8,128)(2,1)S(1)}, bf16[48,2048]{1,0:T(8,128)(2,1)S(1)}, u32[]{:S(2)}, u32[]{:S(2)}) collective-permute-start(bf16[48,2048]{1,0:T(8,128)(2,1)S(1)} %get-tuple-element.89), channel_id=1, source_target_pairs={{0,4},{1,5},{2,6},{3,7},{4,0},{5,1},{6,2},{7,3},{8,12},{9,13},{10,... | collective-permute-start | bytes 589832 | tf_op jit(solution)/shard_map/ppermute | solution.py:24
  110.6 3.4 %collective-permute-done.24 = bf16[48,2048]{1,0:T(8,128)(2,1)S(1)} collective-permute-done((bf16[48,2048]{1,0:T(8,128)(2,1)S(1)}, bf16[48,2048]{1,0:T(8,128)(2,1)S(1)}, u32[]{:S(2)}, u32[]{:S(2)}) %collective-permute-start.24) | collective-permute-done | bytes 196640 | tf_op jit(solution)/shard_map/ppermute | solution.py:24
  114.0 4.4 %collective-permute-done.25 = bf16[48,2048]{1,0:T(8,128)(2,1)S(1)} collective-permute-done((bf16[48,2048]{1,0:T(8,128)(2,1)S(1)}, bf16[48,2048]{1,0:T(8,128)(2,1)S(1)}, u32[]{:S(2)}, u32[]{:S(2)}) %collective-permute-start.25) | collective-permute-done | bytes 196640 | tf_op jit(solution)/shard_map/ppermute | solution.py:24
  119.0 3.1 %collective-permute-start.27 = (bf16[48,2048]{1,0:T(8,128)(2,1)S(1)}, bf16[48,2048]{1,0:T(8,128)(2,1)S(1)}, u32[]{:S(2)}, u32[]{:S(2)}) collective-permute-start(bf16[48,2048]{1,0:T(8,128)(2,1)S(1)} %get-tuple-element.54), channel_id=1, source_target_pairs={{0,6},{1,7},{2,0},{3,1},{4,2},{5,3},{6,4},{7,5},{8,14},{9,15},{10,... | collective-permute-start | bytes 589832 | tf_op jit(solution)/shard_map/ppermute | solution.py:24
  122.1 1.7 collective-permute-start.29
  123.8 2.0 collective-permute-done.27
  125.8 4.3 %collective-permute-done.28 = bf16[48,2048]{1,0:T(8,128)(2,1)S(1)} collective-permute-done((bf16[48,2048]{1,0:T(8,128)(2,1)S(1)}, bf16[48,2048]{1,0:T(8,128)(2,1)S(1)}, u32[]{:S(2)}, u32[]{:S(2)}) %collective-permute-start.28) | collective-permute-done | bytes 196640 | tf_op jit(solution)/shard_map/ppermute | solution.py:24
  130.1 4.9 %collective-permute-start.30 = (bf16[144,2048]{1,0:T(8,128)(2,1)S(1)}, bf16[144,2048]{1,0:T(8,128)(2,1)S(1)}, u32[]{:S(2)}, u32[]{:S(2)}) collective-permute-start(bf16[144,2048]{1,0:T(8,128)(2,1)S(1)} %pad_maximum_fusion.1), channel_id=1, source_target_pairs={{0,1},{1,0},{2,3},{3,2},{4,5},{5,4},{6,7},{7,6},{8,9},{9,8},{10,11... | collective-permute-start | bytes 1769480 | tf_op jit(solution)/shard_map/ppermute | solution.py:24
  135.2 1.5 collective-permute-done.30
  139.5 3.6 %all-to-all-start = ((f32[8,1,768]{2,1,0:T(1,128)}), f32[8,1,768]{2,1,0:T(1,128)S(1)}, u32[]{:S(2)}, u32[]{:S(2)}) async-start(f32[8,1,768]{2,1,0:T(1,128)} %broadcast_in_dim.2), calls=%async_computation | async-start | bytes 49152 | tf_op jit(solution)/shard_map/all_to_all | solution.py:134
  143.1 4.8 %all-to-all-done = f32[8,1,768]{2,1,0:T(1,128)S(1)} async-done(((f32[8,1,768]{2,1,0:T(1,128)}), f32[8,1,768]{2,1,0:T(1,128)S(1)}, u32[]{:S(2)}, u32[]{:S(2)}) %all-to-all-start) | async-done | bytes 24608 | tf_op jit(solution)/shard_map/all_to_all | solution.py:134
  148.2 1.4 convolution_convert_fusion
  150.4 1.4 fusion.23
  153.6 1.9 collective-permute-start.34
  155.4 4.8 %collective-permute-done.33 = bf16[48,2048]{1,0:T(8,128)(2,1)S(1)} collective-permute-done((bf16[48,2048]{1,0:T(8,128)(2,1)S(1)}, bf16[48,2048]{1,0:T(8,128)(2,1)S(1)}, u32[]{:S(2)}, u32[]{:S(2)}) %collective-permute-start.33) | collective-permute-done | bytes 196640 | tf_op jit(solution)/shard_map/ppermute | solution.py:24
  160.3 2.9 %collective-permute-done.34 = bf16[48,2048]{1,0:T(8,128)(2,1)S(1)} collective-permute-done((bf16[48,2048]{1,0:T(8,128)(2,1)S(1)}, bf16[48,2048]{1,0:T(8,128)(2,1)S(1)}, u32[]{:S(2)}, u32[]{:S(2)}) %collective-permute-start.34) | collective-permute-done | bytes 196640 | tf_op jit(solution)/shard_map/ppermute | solution.py:24
  163.1 2.1 collective-permute-done.35
  168.4 3.5 %collective-permute-done.36 = bf16[48,2048]{1,0:T(8,128)(2,1)S(1)} collective-permute-done((bf16[48,2048]{1,0:T(8,128)(2,1)S(1)}, bf16[48,2048]{1,0:T(8,128)(2,1)S(1)}, u32[]{:S(2)}, u32[]{:S(2)}) %collective-permute-start.36) | collective-permute-done | bytes 196640 | tf_op jit(solution)/shard_map/ppermute | solution.py:24
  171.9 3.3 %collective-permute-done.37 = bf16[48,2048]{1,0:T(8,128)(2,1)S(1)} collective-permute-done((bf16[48,2048]{1,0:T(8,128)(2,1)S(1)}, bf16[48,2048]{1,0:T(8,128)(2,1)S(1)}, u32[]{:S(2)}, u32[]{:S(2)}) %collective-permute-start.37) | collective-permute-done | bytes 196640 | tf_op jit(solution)/shard_map/ppermute | solution.py:24
  175.2 4.6 %collective-permute-start.39 = (bf16[144,2048]{1,0:T(8,128)(2,1)S(1)}, bf16[144,2048]{1,0:T(8,128)(2,1)S(1)}, u32[]{:S(2)}, u32[]{:S(2)}) collective-permute-start(bf16[144,2048]{1,0:T(8,128)(2,1)S(1)} %pad_maximum_fusion.2), channel_id=1, source_target_pairs={{0,1},{1,0},{2,3},{3,2},{4,5},{5,4},{6,7},{7,6},{8,9},{9,8},{10,11... | collective-permute-start | bytes 1769480 | tf_op jit(solution)/shard_map/ppermute | solution.py:24
  179.9 1.5 collective-permute-done.39
  181.8 3.7 %copy-done = bf16[2048,2304]{1,0:T(8,128)(2,1)S(1)} copy-done((bf16[2048,2304]{1,0:T(8,128)(2,1)S(1)}, bf16[2048,2304]{1,0:T(8,128)(2,1)}, u32[]{:S(2)}) %copy-start) | copy-done | bytes 9437208
  185.4 3.4 %gated_hidden.1 = bf16[384,768]{1,0:T(8,128)(2,1)S(1)} custom-call(bf16[384,2048]{1,0:T(8,128)(2,1)S(1)} %constant_dynamic-update-slice_fusion.46.rows_ref, bf16[2048,2304]{1,0:T(8,128)(2,1)S(1)} %copy-done, bf16[2048,2304]{1,0:T(8,128)(2,1)S(1)} %copy-done), custom_call_target="tpu_custom_call" | custom-call | tf_op jit(solution)/shard_map/gated_hidden/pallas_call | solution.py:58
  193.0 1.5 collective-permute-start.44
  194.5 6.1 %collective-permute-done.42 = bf16[48,2048]{1,0:T(8,128)(2,1)S(1)} collective-permute-done((bf16[48,2048]{1,0:T(8,128)(2,1)S(1)}, bf16[48,2048]{1,0:T(8,128)(2,1)S(1)}, u32[]{:S(2)}, u32[]{:S(2)}) %collective-permute-start.42) | collective-permute-done | bytes 196640 | tf_op jit(solution)/shard_map/ppermute | solution.py:24
  201.7 3.8 %collective-permute-done.44 = bf16[48,2048]{1,0:T(8,128)(2,1)S(1)} collective-permute-done((bf16[48,2048]{1,0:T(8,128)(2,1)S(1)}, bf16[48,2048]{1,0:T(8,128)(2,1)S(1)}, u32[]{:S(2)}, u32[]{:S(2)}) %collective-permute-start.44) | collective-permute-done | bytes 196640 | tf_op jit(solution)/shard_map/ppermute | solution.py:24
  206.1 8.7 %all_to_all.10 = bf16[8,48,256]{2,1,0:T(8,128)(2,1)S(1)} all-to-all(bf16[8,48,256]{2,1,0:T(8,128)(2,1)S(1)} %bitcast.155), channel_id=1, replica_groups=mesh['fs'=16,'tp'=8] {'tp'}, dimensions={0} | all-to-all | bytes 393216 | tf_op jit(solution)/shard_map/all_to_all | solution.py:261
  (228 shorter events, 40.2 us)
Async XLA Ops:
  6.5 91.9 %all-gather.3.cloned.1.call-start = ((), (), s32[]{:S(2)}) async-start(), calls=%async_computation.2 | async-start | bytes 5013504 | tf_op jit(solution)/shard_map/all_gather | solution.py:165
  10.1 171.7 %all-gather.5.cloned.1.call-start = ((), (), s32[]{:S(2)}) async-start(), calls=%async_computation.3 | async-start | bytes 10027008 | tf_op jit(solution)/shard_map/all_gather | solution.py:181
  10.1 9.1 %collective-permute-start.4 = (bf16[128,768]{1,0:T(8,128)(2,1)}, bf16[128,768]{1,0:T(8,128)(2,1)S(1)}, u32[]{:S(2)}, u32[]{:S(2)}) collective-permute-start(bf16[128,768]{1,0:T(8,128)(2,1)} %param.17), channel_id=1, source_target_pairs={{0,24},{8,0},{16,8},{24,16},{32,56},{40,32},{48,40},{56,48},{64,88... | collective-permute-start | bytes 589832 | tf_op jit(solution)/shard_map/ppermute | solution.py:24
  13.7 8.2 %collective-permute-start.6 = (bf16[128,768]{1,0:T(8,128)(2,1)}, bf16[128,768]{1,0:T(8,128)(2,1)S(1)}, u32[]{:S(2)}, u32[]{:S(2)}) collective-permute-start(bf16[128,768]{1,0:T(8,128)(2,1)} %param.17), channel_id=1, source_target_pairs={{0,8},{8,16},{16,24},{24,0},{32,40},{40,48},{48,56},{56,32},{64,72... | collective-permute-start | bytes 589832 | tf_op jit(solution)/shard_map/ppermute | solution.py:24
  13.7 8.3 %collective-permute-start = (bf16[128,768]{1,0:T(8,128)(2,1)}, bf16[128,768]{1,0:T(8,128)(2,1)S(1)}, u32[]{:S(2)}, u32[]{:S(2)}) collective-permute-start(bf16[128,768]{1,0:T(8,128)(2,1)} %param.16), channel_id=1, source_target_pairs={{0,96},{8,104},{16,112},{24,120},{32,0},{40,8},{48,16},{56,24},{64... | collective-permute-start | bytes 589832 | tf_op jit(solution)/shard_map/ppermute | solution.py:24
  17.5 7.5 %collective-permute-start.2 = (bf16[128,768]{1,0:T(8,128)(2,1)}, bf16[128,768]{1,0:T(8,128)(2,1)S(1)}, u32[]{:S(2)}, u32[]{:S(2)}) collective-permute-start(bf16[128,768]{1,0:T(8,128)(2,1)} %param.16), channel_id=1, source_target_pairs={{0,32},{8,40},{16,48},{24,56},{32,64},{40,72},{48,80},{56,88},{64,... | collective-permute-start | bytes 589832 | tf_op jit(solution)/shard_map/ppermute | solution.py:24
  19.2 6.0 %collective-permute-start.5 = (bf16[64,768]{1,0:T(8,128)(2,1)S(1)}, bf16[64,768]{1,0:T(8,128)(2,1)S(1)}, u32[]{:S(2)}, u32[]{:S(2)}) collective-permute-start(bf16[64,768]{1,0:T(8,128)(2,1)S(1)} %slice.599), channel_id=1, source_target_pairs={{0,24},{8,0},{16,8},{24,16},{32,56},{40,32},{48,40},{56,48},{64,88... | collective-permute-start | bytes 294920 | tf_op jit(solution)/shard_map/ppermute | solution.py:24
  22.0 4.7 %collective-permute-start.7 = (bf16[64,768]{1,0:T(8,128)(2,1)S(1)}, bf16[64,768]{1,0:T(8,128)(2,1)S(1)}, u32[]{:S(2)}, u32[]{:S(2)}) collective-permute-start(bf16[64,768]{1,0:T(8,128)(2,1)S(1)} %slice.600), channel_id=1, source_target_pairs={{0,8},{8,16},{16,24},{24,0},{32,40},{40,48},{48,56},{56,32},{64,72... | collective-permute-start | bytes 294920 | tf_op jit(solution)/shard_map/ppermute | solution.py:24
  22.1 4.9 %collective-permute-start.1 = (bf16[64,768]{1,0:T(8,128)(2,1)S(1)}, bf16[64,768]{1,0:T(8,128)(2,1)S(1)}, u32[]{:S(2)}, u32[]{:S(2)}) collective-permute-start(bf16[64,768]{1,0:T(8,128)(2,1)S(1)} %slice.597), channel_id=1, source_target_pairs={{0,96},{8,104},{16,112},{24,120},{32,0},{40,8},{48,16},{56,24},{64... | collective-permute-start | bytes 294920 | tf_op jit(solution)/shard_map/ppermute | solution.py:24
  25.0 5.2 %collective-permute-start.3 = (bf16[64,768]{1,0:T(8,128)(2,1)S(1)}, bf16[64,768]{1,0:T(8,128)(2,1)S(1)}, u32[]{:S(2)}, u32[]{:S(2)}) collective-permute-start(bf16[64,768]{1,0:T(8,128)(2,1)S(1)} %slice.598), channel_id=1, source_target_pairs={{0,32},{8,40},{16,48},{24,56},{32,64},{40,72},{48,80},{56,88},{64,... | collective-permute-start | bytes 294920 | tf_op jit(solution)/shard_map/ppermute | solution.py:24
  32.3 7.4 %collective-permute-start.8 = (bf16[392,256]{1,0:T(8,128)(2,1)S(1)}, bf16[392,256]{1,0:T(8,128)(2,1)S(1)}, u32[]{:S(2)}, u32[]{:S(2)}) collective-permute-start(bf16[392,256]{1,0:T(8,128)(2,1)S(1)} %pad_maximum_fusion.5), channel_id=1, source_target_pairs={{0,1},{1,0},{2,3},{3,2},{4,5},{5,4},{6,7},{7,6},{8,9},{9,8},{10,11... | collective-permute-start | bytes 602120 | tf_op jit(solution)/shard_map/ppermute | solution.py:24
  35.3 8.0 %collective-permute-start.11 = (bf16[392,256]{1,0:T(8,128)(2,1)S(1)}, bf16[392,256]{1,0:T(8,128)(2,1)S(1)}, u32[]{:S(2)}, u32[]{:S(2)}) collective-permute-start(bf16[392,256]{1,0:T(8,128)(2,1)S(1)} %pad_maximum_fusion.5), channel_id=1, source_target_pairs={{0,4},{1,5},{2,6},{3,7},{4,0},{5,1},{6,2},{7,3},{8,12},{9,13},{10,... | collective-permute-start | bytes 602120 | tf_op jit(solution)/shard_map/ppermute | solution.py:24
  38.0 11.8 %collective-permute-start.9 = (bf16[392,256]{1,0:T(8,128)(2,1)S(1)}, bf16[392,256]{1,0:T(8,128)(2,1)S(1)}, u32[]{:S(2)}, u32[]{:S(2)}) collective-permute-start(bf16[392,256]{1,0:T(8,128)(2,1)S(1)} %pad_maximum_fusion.5), channel_id=1, source_target_pairs={{0,6},{1,7},{2,0},{3,1},{4,2},{5,3},{6,4},{7,5},{8,14},{9,15},{10,... | collective-permute-start | bytes 602120 | tf_op jit(solution)/shard_map/ppermute | solution.py:24
  39.0 8.8 %collective-permute-start.13 = (bf16[392,256]{1,0:T(8,128)(2,1)S(1)}, bf16[392,256]{1,0:T(8,128)(2,1)S(1)}, u32[]{:S(2)}, u32[]{:S(2)}) collective-permute-start(bf16[392,256]{1,0:T(8,128)(2,1)S(1)} %pad_maximum_fusion.5), channel_id=1, source_target_pairs={{0,2},{1,3},{2,4},{3,5},{4,6},{5,7},{6,0},{7,1},{8,10},{9,11},{10,... | collective-permute-start | bytes 602120 | tf_op jit(solution)/shard_map/ppermute | solution.py:24
  39.6 24.7 %collective-permute-start.17 = (bf16[512,768]{1,0:T(8,128)(2,1)}, bf16[512,768]{1,0:T(8,128)(2,1)S(1)}, u32[]{:S(2)}, u32[]{:S(2)}) collective-permute-start(bf16[512,768]{1,0:T(8,128)(2,1)} %copy-done.7), channel_id=1, source_target_pairs={{0,96},{8,104},{16,112},{24,120},{32,0},{40,8},{48,16},{56,24},{64... | collective-permute-start | bytes 2359304 | tf_op jit(solution)/shard_map/ppermute | solution.py:24
  39.7 25.7 %collective-permute-start.18 = (bf16[512,768]{1,0:T(8,128)(2,1)}, bf16[512,768]{1,0:T(8,128)(2,1)S(1)}, u32[]{:S(2)}, u32[]{:S(2)}) collective-permute-start(bf16[512,768]{1,0:T(8,128)(2,1)} %copy-done.7), channel_id=1, source_target_pairs={{0,32},{8,40},{16,48},{24,56},{32,64},{40,72},{48,80},{56,88},{64,... | collective-permute-start | bytes 2359304 | tf_op jit(solution)/shard_map/ppermute | solution.py:24
  43.2 31.9 %collective-permute-start.15 = (bf16[512,768]{1,0:T(8,128)(2,1)S(1)}, bf16[512,768]{1,0:T(8,128)(2,1)S(1)}, u32[]{:S(2)}, u32[]{:S(2)}) collective-permute-start(bf16[512,768]{1,0:T(8,128)(2,1)S(1)} %constant_dynamic-update-slice_fusion), channel_id=1, source_target_pairs={{0,24},{8,0},{16,8},{24,16},{32,56},{40,32},{48,40},{56,48},{64,88... | collective-permute-start | bytes 2359304 | tf_op jit(solution)/shard_map/ppermute | solution.py:24
  47.7 2.9 %collective-permute-start.12 = (bf16[392,256]{1,0:T(8,128)(2,1)S(1)}, bf16[392,256]{1,0:T(8,128)(2,1)S(1)}, u32[]{:S(2)}, u32[]{:S(2)}) collective-permute-start(bf16[392,256]{1,0:T(8,128)(2,1)S(1)} %collective-permute-done.11), channel_id=1, source_target_pairs={{0,1},{1,0},{2,3},{3,2},{4,5},{5,4},{6,7},{7,6},{8,9},{9,8},{10,11... | collective-permute-start | bytes 602120 | tf_op jit(solution)/shard_map/ppermute | solution.py:24
  49.8 1.5 collective-permute-start.14
  50.7 29.4 %collective-permute-start.16 = (bf16[512,768]{1,0:T(8,128)(2,1)S(1)}, bf16[512,768]{1,0:T(8,128)(2,1)S(1)}, u32[]{:S(2)}, u32[]{:S(2)}) collective-permute-start(bf16[512,768]{1,0:T(8,128)(2,1)S(1)} %constant_dynamic-update-slice_fusion), channel_id=1, source_target_pairs={{0,8},{8,16},{16,24},{24,0},{32,40},{40,48},{48,56},{56,32},{64,72... | collective-permute-start | bytes 2359304 | tf_op jit(solution)/shard_map/ppermute | solution.py:24
  51.3 1.4 collective-permute-start.10
  80.6 15.1 %collective-permute-start.21 = (bf16[256,768]{1,0:T(8,128)(2,1)S(1)}, bf16[256,768]{1,0:T(8,128)(2,1)S(1)}, u32[]{:S(2)}, u32[]{:S(2)}) collective-permute-start(bf16[256,768]{1,0:T(8,128)(2,1)S(1)} %slice.495), channel_id=1, source_target_pairs={{0,96},{8,104},{16,112},{24,120},{32,0},{40,8},{48,16},{56,24},{64... | collective-permute-start | bytes 1179656 | tf_op jit(solution)/shard_map/ppermute | solution.py:24
  83.7 12.3 %collective-permute-start.22 = (bf16[256,768]{1,0:T(8,128)(2,1)S(1)}, bf16[256,768]{1,0:T(8,128)(2,1)S(1)}, u32[]{:S(2)}, u32[]{:S(2)}) collective-permute-start(bf16[256,768]{1,0:T(8,128)(2,1)S(1)} %slice.497), channel_id=1, source_target_pairs={{0,32},{8,40},{16,48},{24,56},{32,64},{40,72},{48,80},{56,88},{64,... | collective-permute-start | bytes 1179656 | tf_op jit(solution)/shard_map/ppermute | solution.py:24
  83.9 11.2 %collective-permute-start.19 = (bf16[256,768]{1,0:T(8,128)(2,1)S(1)}, bf16[256,768]{1,0:T(8,128)(2,1)S(1)}, u32[]{:S(2)}, u32[]{:S(2)}) collective-permute-start(bf16[256,768]{1,0:T(8,128)(2,1)S(1)} %slice.487), channel_id=1, source_target_pairs={{0,24},{8,0},{16,8},{24,16},{32,56},{40,32},{48,40},{56,48},{64,88... | collective-permute-start | bytes 1179656 | tf_op jit(solution)/shard_map/ppermute | solution.py:24
  84.8 10.6 %collective-permute-start.20 = (bf16[256,768]{1,0:T(8,128)(2,1)S(1)}, bf16[256,768]{1,0:T(8,128)(2,1)S(1)}, u32[]{:S(2)}, u32[]{:S(2)}) collective-permute-start(bf16[256,768]{1,0:T(8,128)(2,1)S(1)} %slice.490), channel_id=1, source_target_pairs={{0,8},{8,16},{16,24},{24,0},{32,40},{40,48},{48,56},{56,32},{64,72... | collective-permute-start | bytes 1179656 | tf_op jit(solution)/shard_map/ppermute | solution.py:24
  101.3 4.6 %collective-permute-start.23 = (bf16[192,2048]{1,0:T(8,128)(2,1)S(1)}, bf16[192,2048]{1,0:T(8,128)(2,1)S(1)}, u32[]{:S(2)}, u32[]{:S(2)}) collective-permute-start(bf16[192,2048]{1,0:T(8,128)(2,1)S(1)} %fusion.8), channel_id=1, source_target_pairs={{0,1},{1,0},{2,3},{3,2},{4,5},{5,4},{6,7},{7,6},{8,9},{9,8},{10,11... | collective-permute-start | bytes 2359304 | tf_op jit(solution)/shard_map/ppermute | solution.py:24
  106.3 7.7 %collective-permute-start.24 = (bf16[48,2048]{1,0:T(8,128)(2,1)S(1)}, bf16[48,2048]{1,0:T(8,128)(2,1)S(1)}, u32[]{:S(2)}, u32[]{:S(2)}) collective-permute-start(bf16[48,2048]{1,0:T(8,128)(2,1)S(1)} %get-tuple-element.89), channel_id=1, source_target_pairs={{0,4},{1,5},{2,6},{3,7},{4,0},{5,1},{6,2},{7,3},{8,12},{9,13},{10,... | collective-permute-start | bytes 589832 | tf_op jit(solution)/shard_map/ppermute | solution.py:24
  109.1 9.2 %collective-permute-start.25 = (bf16[48,2048]{1,0:T(8,128)(2,1)S(1)}, bf16[48,2048]{1,0:T(8,128)(2,1)S(1)}, u32[]{:S(2)}, u32[]{:S(2)}) collective-permute-start(bf16[48,2048]{1,0:T(8,128)(2,1)S(1)} %get-tuple-element.91), channel_id=1, source_target_pairs={{0,6},{1,7},{2,0},{3,1},{4,2},{5,3},{6,4},{7,5},{8,14},{9,15},{10,... | collective-permute-start | bytes 589832 | tf_op jit(solution)/shard_map/ppermute | solution.py:24
  110.0 8.3 %collective-permute-start.26 = (bf16[48,2048]{1,0:T(8,128)(2,1)S(1)}, bf16[48,2048]{1,0:T(8,128)(2,1)S(1)}, u32[]{:S(2)}, u32[]{:S(2)}) collective-permute-start(bf16[48,2048]{1,0:T(8,128)(2,1)S(1)} %get-tuple-element.90), channel_id=1, source_target_pairs={{0,2},{1,3},{2,4},{3,5},{4,6},{5,7},{6,0},{7,1},{8,10},{9,11},{10,... | collective-permute-start | bytes 589832 | tf_op jit(solution)/shard_map/ppermute | solution.py:24
  119.0 6.8 %collective-permute-start.27 = (bf16[48,2048]{1,0:T(8,128)(2,1)S(1)}, bf16[48,2048]{1,0:T(8,128)(2,1)S(1)}, u32[]{:S(2)}, u32[]{:S(2)}) collective-permute-start(bf16[48,2048]{1,0:T(8,128)(2,1)S(1)} %get-tuple-element.54), channel_id=1, source_target_pairs={{0,6},{1,7},{2,0},{3,1},{4,2},{5,3},{6,4},{7,5},{8,14},{9,15},{10,... | collective-permute-start | bytes 589832 | tf_op jit(solution)/shard_map/ppermute | solution.py:24
  122.1 8.0 %collective-permute-start.28 = (bf16[48,2048]{1,0:T(8,128)(2,1)S(1)}, bf16[48,2048]{1,0:T(8,128)(2,1)S(1)}, u32[]{:S(2)}, u32[]{:S(2)}) collective-permute-start(bf16[48,2048]{1,0:T(8,128)(2,1)S(1)} %get-tuple-element.54), channel_id=1, source_target_pairs={{0,2},{1,3},{2,4},{3,5},{4,6},{5,7},{6,0},{7,1},{8,10},{9,11},{10,... | collective-permute-start | bytes 589832 | tf_op jit(solution)/shard_map/ppermute | solution.py:24
  122.1 12.9 %collective-permute-start.29 = (bf16[48,2048]{1,0:T(8,128)(2,1)S(1)}, bf16[48,2048]{1,0:T(8,128)(2,1)S(1)}, u32[]{:S(2)}, u32[]{:S(2)}) collective-permute-start(bf16[48,2048]{1,0:T(8,128)(2,1)S(1)} %get-tuple-element.54), channel_id=1, source_target_pairs={{0,4},{1,5},{2,6},{3,7},{4,0},{5,1},{6,2},{7,3},{8,12},{9,13},{10,... | collective-permute-start | bytes 589832 | tf_op jit(solution)/shard_map/ppermute | solution.py:24
  130.1 6.5 %collective-permute-start.30 = (bf16[144,2048]{1,0:T(8,128)(2,1)S(1)}, bf16[144,2048]{1,0:T(8,128)(2,1)S(1)}, u32[]{:S(2)}, u32[]{:S(2)}) collective-permute-start(bf16[144,2048]{1,0:T(8,128)(2,1)S(1)} %pad_maximum_fusion.1), channel_id=1, source_target_pairs={{0,1},{1,0},{2,3},{3,2},{4,5},{5,4},{6,7},{7,6},{8,9},{9,8},{10,11... | collective-permute-start | bytes 1769480 | tf_op jit(solution)/shard_map/ppermute | solution.py:24
  135.0 1.9 collective-permute-start.31
  139.5 8.4 %all-to-all-start = ((f32[8,1,768]{2,1,0:T(1,128)}), f32[8,1,768]{2,1,0:T(1,128)S(1)}, u32[]{:S(2)}, u32[]{:S(2)}) async-start(f32[8,1,768]{2,1,0:T(1,128)} %broadcast_in_dim.2), calls=%async_computation | async-start | bytes 49152 | tf_op jit(solution)/shard_map/all_to_all | solution.py:134
  149.6 2.6 %collective-permute-start.32 = (bf16[192,2048]{1,0:T(8,128)(2,1)S(1)}, bf16[192,2048]{1,0:T(8,128)(2,1)S(1)}, u32[]{:S(2)}, u32[]{:S(2)}) collective-permute-start(bf16[192,2048]{1,0:T(8,128)(2,1)S(1)} %convolution_convert_fusion), channel_id=1, source_target_pairs={{0,1},{1,0},{2,3},{3,2},{4,5},{5,4},{6,7},{7,6},{8,9},{9,8},{10,11... | collective-permute-start | bytes 2359304 | tf_op jit(solution)/shard_map/ppermute | solution.py:24
  152.6 7.7 %collective-permute-start.33 = (bf16[48,2048]{1,0:T(8,128)(2,1)S(1)}, bf16[48,2048]{1,0:T(8,128)(2,1)S(1)}, u32[]{:S(2)}, u32[]{:S(2)}) collective-permute-start(bf16[48,2048]{1,0:T(8,128)(2,1)S(1)} %get-tuple-element.86), channel_id=1, source_target_pairs={{0,4},{1,5},{2,6},{3,7},{4,0},{5,1},{6,2},{7,3},{8,12},{9,13},{10,... | collective-permute-start | bytes 589832 | tf_op jit(solution)/shard_map/ppermute | solution.py:24
  153.6 9.6 %collective-permute-start.34 = (bf16[48,2048]{1,0:T(8,128)(2,1)S(1)}, bf16[48,2048]{1,0:T(8,128)(2,1)S(1)}, u32[]{:S(2)}, u32[]{:S(2)}) collective-permute-start(bf16[48,2048]{1,0:T(8,128)(2,1)S(1)} %get-tuple-element.88), channel_id=1, source_target_pairs={{0,6},{1,7},{2,0},{3,1},{4,2},{5,3},{6,4},{7,5},{8,14},{9,15},{10,... | collective-permute-start | bytes 589832 | tf_op jit(solution)/shard_map/ppermute | solution.py:24
  155.4 9.8 %collective-permute-start.35 = (bf16[48,2048]{1,0:T(8,128)(2,1)S(1)}, bf16[48,2048]{1,0:T(8,128)(2,1)S(1)}, u32[]{:S(2)}, u32[]{:S(2)}) collective-permute-start(bf16[48,2048]{1,0:T(8,128)(2,1)S(1)} %get-tuple-element.87), channel_id=1, source_target_pairs={{0,2},{1,3},{2,4},{3,5},{4,6},{5,7},{6,0},{7,1},{8,10},{9,11},{10,... | collective-permute-start | bytes 589832 | tf_op jit(solution)/shard_map/ppermute | solution.py:24
  165.8 6.0 %collective-permute-start.36 = (bf16[48,2048]{1,0:T(8,128)(2,1)S(1)}, bf16[48,2048]{1,0:T(8,128)(2,1)S(1)}, u32[]{:S(2)}, u32[]{:S(2)}) collective-permute-start(bf16[48,2048]{1,0:T(8,128)(2,1)S(1)} %get-tuple-element.46), channel_id=1, source_target_pairs={{0,6},{1,7},{2,0},{3,1},{4,2},{5,3},{6,4},{7,5},{8,14},{9,15},{10,... | collective-permute-start | bytes 589832 | tf_op jit(solution)/shard_map/ppermute | solution.py:24
  166.9 8.3 %collective-permute-start.37 = (bf16[48,2048]{1,0:T(8,128)(2,1)S(1)}, bf16[48,2048]{1,0:T(8,128)(2,1)S(1)}, u32[]{:S(2)}, u32[]{:S(2)}) collective-permute-start(bf16[48,2048]{1,0:T(8,128)(2,1)S(1)} %get-tuple-element.46), channel_id=1, source_target_pairs={{0,2},{1,3},{2,4},{3,5},{4,6},{5,7},{6,0},{7,1},{8,10},{9,11},{10,... | collective-permute-start | bytes 589832 | tf_op jit(solution)/shard_map/ppermute | solution.py:24
  167.4 12.4 %collective-permute-start.38 = (bf16[48,2048]{1,0:T(8,128)(2,1)S(1)}, bf16[48,2048]{1,0:T(8,128)(2,1)S(1)}, u32[]{:S(2)}, u32[]{:S(2)}) collective-permute-start(bf16[48,2048]{1,0:T(8,128)(2,1)S(1)} %get-tuple-element.46), channel_id=1, source_target_pairs={{0,4},{1,5},{2,6},{3,7},{4,0},{5,1},{6,2},{7,3},{8,12},{9,13},{10,... | collective-permute-start | bytes 589832 | tf_op jit(solution)/shard_map/ppermute | solution.py:24
  175.2 6.2 %collective-permute-start.39 = (bf16[144,2048]{1,0:T(8,128)(2,1)S(1)}, bf16[144,2048]{1,0:T(8,128)(2,1)S(1)}, u32[]{:S(2)}, u32[]{:S(2)}) collective-permute-start(bf16[144,2048]{1,0:T(8,128)(2,1)S(1)} %pad_maximum_fusion.2), channel_id=1, source_target_pairs={{0,1},{1,0},{2,3},{3,2},{4,5},{5,4},{6,7},{7,6},{8,9},{9,8},{10,11... | collective-permute-start | bytes 1769480 | tf_op jit(solution)/shard_map/ppermute | solution.py:24
  179.8 1.9 collective-permute-start.40
  190.1 2.4 %collective-permute-start.41 = (bf16[192,2048]{1,0:T(8,128)(2,1)S(1)}, bf16[192,2048]{1,0:T(8,128)(2,1)S(1)}, u32[]{:S(2)}, u32[]{:S(2)}) collective-permute-start(bf16[192,2048]{1,0:T(8,128)(2,1)S(1)} %fusion.11), channel_id=1, source_target_pairs={{0,1},{1,0},{2,3},{3,2},{4,5},{5,4},{6,7},{7,6},{8,9},{9,8},{10,11... | collective-permute-start | bytes 2359304 | tf_op jit(solution)/shard_map/ppermute | solution.py:24
  192.8 7.7 %collective-permute-start.42 = (bf16[48,2048]{1,0:T(8,128)(2,1)S(1)}, bf16[48,2048]{1,0:T(8,128)(2,1)S(1)}, u32[]{:S(2)}, u32[]{:S(2)}) collective-permute-start(bf16[48,2048]{1,0:T(8,128)(2,1)S(1)} %get-tuple-element.83), channel_id=1, source_target_pairs={{0,4},{1,5},{2,6},{3,7},{4,0},{5,1},{6,2},{7,3},{8,12},{9,13},{10,... | collective-permute-start | bytes 589832 | tf_op jit(solution)/shard_map/ppermute | solution.py:24
  192.9 8.7 %collective-permute-start.43 = (bf16[48,2048]{1,0:T(8,128)(2,1)S(1)}, bf16[48,2048]{1,0:T(8,128)(2,1)S(1)}, u32[]{:S(2)}, u32[]{:S(2)}) collective-permute-start(bf16[48,2048]{1,0:T(8,128)(2,1)S(1)} %get-tuple-element.85), channel_id=1, source_target_pairs={{0,6},{1,7},{2,0},{3,1},{4,2},{5,3},{6,4},{7,5},{8,14},{9,15},{10,... | collective-permute-start | bytes 589832 | tf_op jit(solution)/shard_map/ppermute | solution.py:24
  193.0 12.4 %collective-permute-start.44 = (bf16[48,2048]{1,0:T(8,128)(2,1)S(1)}, bf16[48,2048]{1,0:T(8,128)(2,1)S(1)}, u32[]{:S(2)}, u32[]{:S(2)}) collective-permute-start(bf16[48,2048]{1,0:T(8,128)(2,1)S(1)} %get-tuple-element.84), channel_id=1, source_target_pairs={{0,2},{1,3},{2,4},{3,5},{4,6},{5,7},{6,0},{7,1},{8,10},{9,11},{10,... | collective-permute-start | bytes 589832 | tf_op jit(solution)/shard_map/ppermute | solution.py:24
  (13 other events, 88.5 us)
Sparse Core Ops, SparseCore 0:
  10.2 77.4 all-gather.2
  89.8 77.3 all-gather.4

commit v2 on v1

--- a/solution.py
+++ b/solution.py
@@ -43,6 +43,23 @@
 
 def matmul_t(left, right):
     return lax.dot_general(left, right, (((1,), (1,)), ((), ())), preferred_element_type=F32)
+
+
+def packed(down, proj, value, gate):
+    sizes = [down.shape[0], proj.shape[0], value.shape[1], gate.shape[1]]
+    ends = [sum(sizes[: k + 1]) for k in range(4)]
+
+    def kernel(down_ref, proj_ref, value_ref, gate_ref, out_ref):
+        out_ref[: ends[0]] = down_ref[...]
+        out_ref[ends[0] : ends[1]] = proj_ref[...]
+        out_ref[ends[1] : ends[2]] = value_ref[...].T
+        out_ref[ends[2] :] = gate_ref[...].T
+
+    return pl.pallas_call(
+        kernel,
+        out_shape=jax.ShapeDtypeStruct((ends[3], down.shape[1]), BF16),
+        name="packed",
+    )(down, proj, value, gate)
 
 
 def gated_hidden(rows, weights, width):
@@ -163,10 +180,7 @@
     current = tokens[0]
 
     early = lax.all_gather(
-        jnp.concatenate([first_down.T, glu_value, glu_gate, conv_proj.T], axis=1),
-        "fs",
-        axis=0,
-        tiled=True,
+        packed(first_down, conv_proj, glu_value, glu_gate), "fs", axis=1, tiled=True
     )
 
     near_gate, near_up = neighbours(first_gate, "z"), neighbours(first_up, "y")
@@ -198,7 +212,6 @@
     own_rows, gains = some[:48].astype(F32), some[48:51].astype(F32)
 
     near_gate, near_up = neighbours(gate_part, "y"), neighbours(up_part, "z")
-    near_gate, near_up, turned = lax.optimization_barrier((near_gate, near_up, turned))
     far_gate, far_up = opposite(*near_gate, "y"), opposite(*near_up, "z")
     gate_of = [
         jnp.concatenate([turned[:, 512 * k + 128 * d :][:, :128] for k in range(4)], axis=1)
@@ -217,10 +230,10 @@
     up = split_sum(up_of, up_part, near_up, far_up)
     hidden = (jax.nn.silu(gate) * up).astype(BF16)
 
-    def down(rows_other, rows_own, weight):
-        return summed_rows(matmul_t(rows_other, weight), matmul_t(rows_own, weight))
-
-    branch = down(*by_owner(hidden, x, core), early[:, :768])
+    def down(rows_other, rows_own, weight, product=matmul):
+        return summed_rows(product(rows_other, weight), product(rows_own, weight))
+
+    branch = down(*by_owner(hidden, x, core), early[:768])
     first = norm_rows(ALPHA * own_rows + 0.5 * branch, gains[0])
 
     def every_row(rows):
@@ -235,7 +248,7 @@
         return own, other
 
     def gated_linear(rows):
-        both = matmul(rows, early[:, 768:1024])
+        both = matmul_t(rows, early[896:])
         return both[:, :128] * jax.nn.sigmoid(both[:, 128:])
 
     gated = in_order(list(zip(*by_distance(gated_linear(every_row(first))))), x, core)
@@ -248,13 +261,13 @@
     center, spread = channel_stats(mixed)
     normed = (mixed - center) * lax.rsqrt(spread + EPSILON) * conv_gain.astype(F32)
     act = jax.nn.silu(normed).astype(BF16)
-    branch = down(*by_owner(act, x, core), early[:, 1024:])
+    branch = down(*by_owner(act, x, core), early[768:896])
     second = norm_rows(ALPHA * first.astype(F32) + branch, gains[1])
 
     rows = every_row(second)
     own, other = by_distance(gated_hidden(rows, late, 768))
     branch = down(
-        jnp.concatenate(other, axis=0), jnp.concatenate(own, axis=0), late[:, 1536:]
+        jnp.concatenate(other, axis=0), jnp.concatenate(own, axis=0), late[:, 1536:], matmul_t
     )
     out = norm_rows(ALPHA * second.astype(F32) + 0.5 * branch, gains[2])
     out = out.reshape(-1, 8, 256).transpose(1, 0, 2)

time: 223 us -> 220 us (0.987)
  starting transfers between devices: 66.8 us -> 61.7 us
  waiting for transfers between devices: 94.8 us -> 98.1 us
    dot_general x11 -> x14, matrix products: 4.96 us -> 10.8 us  [matmul(): return jnp.dot(left, right, preferred_element_type=F32)]
    dot_general x6 -> x3, matrix products: 8.76 us -> 2.99 us  [matmul_t(): lax.dot_general(left, right, (((1,), (1,)), ((), ())), preferred_element_...]
    ppermute x45, starting transfers between devices: 63.1 us -> 58 us  [pull(): return lax.ppermute(value, 'fs' if axis in 'zy' else 'tp', pairs)]
    ppermute x45, waiting for transfers between devices: 90 us -> 93.3 us  [pull(): return lax.ppermute(value, 'fs' if axis in 'zy' else 'tp', pairs)]
    unnamed x51 -> x47, local copies, waits for them, and re-layouts: 8.89 us -> 8.05 us
  transfers between devices with their start and end apart: 48 -> 48, of which waited for: 32 -> 33; matrix products, arithmetic and copies ran while one was open for 10% -> 11% of each run, Pallas kernels for 0% -> 0%
where the time goes in v2:
time: 220 us
  waiting for transfers between devices  98.1 us (45%)
  starting transfers between devices  61.7 us (28%)
  between operations  14.5 us (7%)
  matrix products  13.7 us (6%)
  local copies, waits for them, and re-layouts  10 us (5%)
  blocking collectives  8.74 us (4%)
  other arithmetic  7.69 us (3%)
  Pallas kernels  5.21 us (2%)
    ppermute x45, waiting for transfers between devices, pull(): return lax.ppermute(value, 'fs' if axis in 'zy' else 'tp', pairs)  93.3 us
    ppermute x45, starting transfers between devices, pull(): return lax.ppermute(value, 'fs' if axis in 'zy' else 'tp', pairs)  58 us
    dot_general x14, matrix products, matmul(): return jnp.dot(left, right, preferred_element_type=F32)  10.8 us
    all_to_all x1, blocking collectives, layer(): out = lax.all_to_all(out, 'tp', split_axis=0, concat_axis=0, tiled=True)  8.74 us
    unnamed x47, local copies, waits for them, and re-layouts  8.05 us
    all_to_all x1, waiting for transfers between devices, channel_stats(): both = lax.all_to_all(both, 'tp', split_axis=0, concat_axis=0, tiled=True)  4.75 us
  transfers between devices with their start and end apart: 48, of which 33 were waited for; matrix products, arithmetic and copies ran while one was open for 11% of the time, Pallas kernels for 0%

profile of v2, /device:TPU:1, one launch (start us, length us, event | category | flops | bytes accessed | tf_op | source)
XLA Modules:
  0.0 219.7 jit_solution(1776966198836886279)
XLA Ops:
  6.5 1.8 packed.1
  8.4 3.6 %collective-permute-start.4 = (bf16[128,768]{1,0:T(8,128)(2,1)}, bf16[128,768]{1,0:T(8,128)(2,1)S(1)}, u32[]{:S(2)}, u32[]{:S(2)}) collective-permute-start(bf16[128,768]{1,0:T(8,128)(2,1)} %param.17), channel_id=1, source_target_pairs={{0,24},{8,0},{16,8},{24,16},{32,56},{40,32},{48,40},{56,48},{64,88... | collective-permute-start | bytes 589832 | tf_op jit(solution)/shard_map/ppermute | solution.py:24
  12.0 3.8 %collective-permute-start = (bf16[128,768]{1,0:T(8,128)(2,1)}, bf16[128,768]{1,0:T(8,128)(2,1)S(1)}, u32[]{:S(2)}, u32[]{:S(2)}) collective-permute-start(bf16[128,768]{1,0:T(8,128)(2,1)} %param.16), channel_id=1, source_target_pairs={{0,96},{8,104},{16,112},{24,120},{32,0},{40,8},{48,16},{56,24},{64... | collective-permute-start | bytes 589832 | tf_op jit(solution)/shard_map/ppermute | solution.py:24
  18.4 2.7 %collective-permute-start.5 = (bf16[64,768]{1,0:T(8,128)(2,1)S(1)}, bf16[64,768]{1,0:T(8,128)(2,1)S(1)}, u32[]{:S(2)}, u32[]{:S(2)}) collective-permute-start(bf16[64,768]{1,0:T(8,128)(2,1)S(1)} %slice.599), channel_id=1, source_target_pairs={{0,24},{8,0},{16,8},{24,16},{32,56},{40,32},{48,40},{56,48},{64,88... | collective-permute-start | bytes 294920 | tf_op jit(solution)/shard_map/ppermute | solution.py:24
  21.3 2.7 %collective-permute-start.1 = (bf16[64,768]{1,0:T(8,128)(2,1)S(1)}, bf16[64,768]{1,0:T(8,128)(2,1)S(1)}, u32[]{:S(2)}, u32[]{:S(2)}) collective-permute-start(bf16[64,768]{1,0:T(8,128)(2,1)S(1)} %slice.597), channel_id=1, source_target_pairs={{0,96},{8,104},{16,112},{24,120},{32,0},{40,8},{48,16},{56,24},{64... | collective-permute-start | bytes 294920 | tf_op jit(solution)/shard_map/ppermute | solution.py:24
  24.2 1.7 collective-permute-done.7
  26.3 3.3 %collective-permute-done.3 = bf16[64,768]{1,0:T(8,128)(2,1)S(1)} collective-permute-done((bf16[64,768]{1,0:T(8,128)(2,1)S(1)}, bf16[64,768]{1,0:T(8,128)(2,1)S(1)}, u32[]{:S(2)}, u32[]{:S(2)}) %collective-permute-start.3) | collective-permute-done | bytes 98336 | tf_op jit(solution)/shard_map/ppermute | solution.py:24
  31.7 2.8 %collective-permute-start.8 = (bf16[392,256]{1,0:T(8,128)(2,1)S(1)}, bf16[392,256]{1,0:T(8,128)(2,1)S(1)}, u32[]{:S(2)}, u32[]{:S(2)}) collective-permute-start(bf16[392,256]{1,0:T(8,128)(2,1)S(1)} %pad_maximum_fusion.4), channel_id=1, source_target_pairs={{0,1},{1,0},{2,3},{3,2},{4,5},{5,4},{6,7},{7,6},{8,9},{9,8},{10,11... | collective-permute-start | bytes 602120 | tf_op jit(solution)/shard_map/ppermute | solution.py:24
  34.4 2.5 %collective-permute-start.9 = (bf16[392,256]{1,0:T(8,128)(2,1)S(1)}, bf16[392,256]{1,0:T(8,128)(2,1)S(1)}, u32[]{:S(2)}, u32[]{:S(2)}) collective-permute-start(bf16[392,256]{1,0:T(8,128)(2,1)S(1)} %pad_maximum_fusion.4), channel_id=1, source_target_pairs={{0,6},{1,7},{2,0},{3,1},{4,2},{5,3},{6,4},{7,5},{8,14},{9,15},{10,... | collective-permute-start | bytes 602120 | tf_op jit(solution)/shard_map/ppermute | solution.py:24
  39.8 5.6 %collective-permute-done.9 = bf16[392,256]{1,0:T(8,128)(2,1)S(1)} collective-permute-done((bf16[392,256]{1,0:T(8,128)(2,1)S(1)}, bf16[392,256]{1,0:T(8,128)(2,1)S(1)}, u32[]{:S(2)}, u32[]{:S(2)}) %collective-permute-start.9) | collective-permute-done | bytes 200736 | tf_op jit(solution)/shard_map/ppermute | solution.py:24
  45.4 4.3 %collective-permute-start.15 = (bf16[512,768]{1,0:T(8,128)(2,1)S(1)}, bf16[512,768]{1,0:T(8,128)(2,1)S(1)}, u32[]{:S(2)}, u32[]{:S(2)}) collective-permute-start(bf16[512,768]{1,0:T(8,128)(2,1)S(1)} %constant_dynamic-update-slice_fusion), channel_id=1, source_target_pairs={{0,24},{8,0},{16,8},{24,16},{32,56},{40,32},{48,40},{56,48},{64,88... | collective-permute-start | bytes 2359304 | tf_op jit(solution)/shard_map/ppermute | solution.py:24
  49.6 1.4 collective-permute-start.10
  56.4 6.4 %collective-permute-done.19 = bf16[512,768]{1,0:T(8,128)(2,1)S(1)} collective-permute-done((bf16[512,768]{1,0:T(8,128)(2,1)}, bf16[512,768]{1,0:T(8,128)(2,1)S(1)}, u32[]{:S(2)}, u32[]{:S(2)}) %collective-permute-start.19) | collective-permute-done | bytes 786464 | tf_op jit(solution)/shard_map/ppermute | solution.py:24
  62.9 1.5 collective-permute-start.21
  64.5 11.3 %collective-permute-done.15 = bf16[512,768]{1,0:T(8,128)(2,1)S(1)} collective-permute-done((bf16[512,768]{1,0:T(8,128)(2,1)S(1)}, bf16[512,768]{1,0:T(8,128)(2,1)S(1)}, u32[]{:S(2)}, u32[]{:S(2)}) %collective-permute-start.15) | collective-permute-done | bytes 786464 | tf_op jit(solution)/shard_map/ppermute | solution.py:24
  75.8 2.3 %collective-permute-start.17 = (bf16[256,768]{1,0:T(8,128)(2,1)S(1)}, bf16[256,768]{1,0:T(8,128)(2,1)S(1)}, u32[]{:S(2)}, u32[]{:S(2)}) collective-permute-start(bf16[256,768]{1,0:T(8,128)(2,1)S(1)} %slice.609), channel_id=1, source_target_pairs={{0,24},{8,0},{16,8},{24,16},{32,56},{40,32},{48,40},{56,48},{64,88... | collective-permute-start | bytes 1179656 | tf_op jit(solution)/shard_map/ppermute | solution.py:24
  78.1 1.3 collective-permute-done.16
  82.0 1.6 collective-permute-done.22
  84.0 7.6 %collective-permute-done.17 = bf16[256,768]{1,0:T(8,128)(2,1)S(1)} collective-permute-done((bf16[256,768]{1,0:T(8,128)(2,1)S(1)}, bf16[256,768]{1,0:T(8,128)(2,1)S(1)}, u32[]{:S(2)}, u32[]{:S(2)}) %collective-permute-start.17) | collective-permute-done | bytes 393248 | tf_op jit(solution)/shard_map/ppermute | solution.py:24
  91.9 3.4 %collective-permute-done.18 = bf16[256,768]{1,0:T(8,128)(2,1)S(1)} collective-permute-done((bf16[256,768]{1,0:T(8,128)(2,1)S(1)}, bf16[256,768]{1,0:T(8,128)(2,1)S(1)}, u32[]{:S(2)}, u32[]{:S(2)}) %collective-permute-start.18) | collective-permute-done | bytes 393248 | tf_op jit(solution)/shard_map/ppermute | solution.py:24
  97.8 2.8 %fusion.8 = bf16[192,2048]{1,0:T(8,128)(2,1)S(1)} fusion(bf16[192,768]{1,0:T(8,128)(2,1)S(1)} %bitcast.161, bf16[1152,2048]{1,0:T(8,128)(2,1)} %all-gather.3.cloned.1.call-done), kind=kOutput, calls=%fused_computation.8 | convolution fusion | flops 604372992 | bytes 4227072 | tf_op jit(solution)/shard_map/dot_general | solution.py:41
  103.7 2.5 %collective-permute-start.24 = (bf16[48,2048]{1,0:T(8,128)(2,1)S(1)}, bf16[48,2048]{1,0:T(8,128)(2,1)S(1)}, u32[]{:S(2)}, u32[]{:S(2)}) collective-permute-start(bf16[48,2048]{1,0:T(8,128)(2,1)S(1)} %get-tuple-element.79), channel_id=1, source_target_pairs={{0,4},{1,5},{2,6},{3,7},{4,0},{5,1},{6,2},{7,3},{8,12},{9,13},{10,... | collective-permute-start | bytes 589832 | tf_op jit(solution)/shard_map/ppermute | solution.py:24
  107.7 3.7 %collective-permute-done.24 = bf16[48,2048]{1,0:T(8,128)(2,1)S(1)} collective-permute-done((bf16[48,2048]{1,0:T(8,128)(2,1)S(1)}, bf16[48,2048]{1,0:T(8,128)(2,1)S(1)}, u32[]{:S(2)}, u32[]{:S(2)}) %collective-permute-start.24) | collective-permute-done | bytes 196640 | tf_op jit(solution)/shard_map/ppermute | solution.py:24
  111.4 4.3 %collective-permute-done.25 = bf16[48,2048]{1,0:T(8,128)(2,1)S(1)} collective-permute-done((bf16[48,2048]{1,0:T(8,128)(2,1)S(1)}, bf16[48,2048]{1,0:T(8,128)(2,1)S(1)}, u32[]{:S(2)}, u32[]{:S(2)}) %collective-permute-start.25) | collective-permute-done | bytes 196640 | tf_op jit(solution)/shard_map/ppermute | solution.py:24
  116.6 2.9 %collective-permute-start.27 = (bf16[48,2048]{1,0:T(8,128)(2,1)S(1)}, bf16[48,2048]{1,0:T(8,128)(2,1)S(1)}, u32[]{:S(2)}, u32[]{:S(2)}) collective-permute-start(bf16[48,2048]{1,0:T(8,128)(2,1)S(1)} %get-tuple-element.44), channel_id=1, source_target_pairs={{0,6},{1,7},{2,0},{3,1},{4,2},{5,3},{6,4},{7,5},{8,14},{9,15},{10,... | collective-permute-start | bytes 589832 | tf_op jit(solution)/shard_map/ppermute | solution.py:24
  119.5 1.5 collective-permute-start.29
  121.1 2.2 collective-permute-done.27
  123.2 4.4 %collective-permute-done.28 = bf16[48,2048]{1,0:T(8,128)(2,1)S(1)} collective-permute-done((bf16[48,2048]{1,0:T(8,128)(2,1)S(1)}, bf16[48,2048]{1,0:T(8,128)(2,1)S(1)}, u32[]{:S(2)}, u32[]{:S(2)}) %collective-permute-start.28) | collective-permute-done | bytes 196640 | tf_op jit(solution)/shard_map/ppermute | solution.py:24
  127.7 4.7 %collective-permute-start.30 = (bf16[144,2048]{1,0:T(8,128)(2,1)S(1)}, bf16[144,2048]{1,0:T(8,128)(2,1)S(1)}, u32[]{:S(2)}, u32[]{:S(2)}) collective-permute-start(bf16[144,2048]{1,0:T(8,128)(2,1)S(1)} %pad_maximum_fusion.1), channel_id=1, source_target_pairs={{0,1},{1,0},{2,3},{3,2},{4,5},{5,4},{6,7},{7,6},{8,9},{9,8},{10,11... | collective-permute-start | bytes 1769480 | tf_op jit(solution)/shard_map/ppermute | solution.py:24
  132.6 1.5 collective-permute-done.30
  136.9 3.6 %all-to-all-start = ((f32[8,1,768]{2,1,0:T(1,128)}), f32[8,1,768]{2,1,0:T(1,128)S(1)}, u32[]{:S(2)}, u32[]{:S(2)}) async-start(f32[8,1,768]{2,1,0:T(1,128)} %broadcast_in_dim.2), calls=%async_computation | async-start | bytes 49152 | tf_op jit(solution)/shard_map/all_to_all | solution.py:151
  140.5 4.8 %all-to-all-done = f32[8,1,768]{2,1,0:T(1,128)S(1)} async-done(((f32[8,1,768]{2,1,0:T(1,128)}), f32[8,1,768]{2,1,0:T(1,128)S(1)}, u32[]{:S(2)}, u32[]{:S(2)}) %all-to-all-start) | async-done | bytes 24608 | tf_op jit(solution)/shard_map/all_to_all | solution.py:151
  145.6 1.4 convolution_convert_fusion
  147.8 1.4 fusion.23
  150.9 1.9 collective-permute-start.34
  152.8 4.8 %collective-permute-done.33 = bf16[48,2048]{1,0:T(8,128)(2,1)S(1)} collective-permute-done((bf16[48,2048]{1,0:T(8,128)(2,1)S(1)}, bf16[48,2048]{1,0:T(8,128)(2,1)S(1)}, u32[]{:S(2)}, u32[]{:S(2)}) %collective-permute-start.33) | collective-permute-done | bytes 196640 | tf_op jit(solution)/shard_map/ppermute | solution.py:24
  157.7 2.8 %collective-permute-done.34 = bf16[48,2048]{1,0:T(8,128)(2,1)S(1)} collective-permute-done((bf16[48,2048]{1,0:T(8,128)(2,1)S(1)}, bf16[48,2048]{1,0:T(8,128)(2,1)S(1)}, u32[]{:S(2)}, u32[]{:S(2)}) %collective-permute-start.34) | collective-permute-done | bytes 196640 | tf_op jit(solution)/shard_map/ppermute | solution.py:24
  160.5 2.1 collective-permute-done.35
  165.8 3.7 %collective-permute-done.36 = bf16[48,2048]{1,0:T(8,128)(2,1)S(1)} collective-permute-done((bf16[48,2048]{1,0:T(8,128)(2,1)S(1)}, bf16[48,2048]{1,0:T(8,128)(2,1)S(1)}, u32[]{:S(2)}, u32[]{:S(2)}) %collective-permute-start.36) | collective-permute-done | bytes 196640 | tf_op jit(solution)/shard_map/ppermute | solution.py:24
  169.4 3.1 %collective-permute-done.37 = bf16[48,2048]{1,0:T(8,128)(2,1)S(1)} collective-permute-done((bf16[48,2048]{1,0:T(8,128)(2,1)S(1)}, bf16[48,2048]{1,0:T(8,128)(2,1)S(1)}, u32[]{:S(2)}, u32[]{:S(2)}) %collective-permute-start.37) | collective-permute-done | bytes 196640 | tf_op jit(solution)/shard_map/ppermute | solution.py:24
  172.6 4.5 %collective-permute-start.39 = (bf16[144,2048]{1,0:T(8,128)(2,1)S(1)}, bf16[144,2048]{1,0:T(8,128)(2,1)S(1)}, u32[]{:S(2)}, u32[]{:S(2)}) collective-permute-start(bf16[144,2048]{1,0:T(8,128)(2,1)S(1)} %pad_maximum_fusion.2), channel_id=1, source_target_pairs={{0,1},{1,0},{2,3},{3,2},{4,5},{5,4},{6,7},{7,6},{8,9},{9,8},{10,11... | collective-permute-start | bytes 1769480 | tf_op jit(solution)/shard_map/ppermute | solution.py:24
  177.3 1.5 collective-permute-done.39
  179.1 3.7 %copy-done = bf16[2048,2304]{1,0:T(8,128)(2,1)S(1)} copy-done((bf16[2048,2304]{1,0:T(8,128)(2,1)S(1)}, bf16[2048,2304]{1,0:T(8,128)(2,1)}, u32[]{:S(2)}) %copy-start) | copy-done | bytes 9437208
  182.8 3.4 %gated_hidden.1 = bf16[384,768]{1,0:T(8,128)(2,1)S(1)} custom-call(bf16[384,2048]{1,0:T(8,128)(2,1)S(1)} %constant_dynamic-update-slice_fusion.46.rows_ref, bf16[2048,2304]{1,0:T(8,128)(2,1)S(1)} %copy-done, bf16[2048,2304]{1,0:T(8,128)(2,1)S(1)} %copy-done), custom_call_target="tpu_custom_call" | custom-call | tf_op jit(solution)/shard_map/gated_hidden/pallas_call | solution.py:75
  190.4 1.5 collective-permute-start.44
  191.8 6.1 %collective-permute-done.42 = bf16[48,2048]{1,0:T(8,128)(2,1)S(1)} collective-permute-done((bf16[48,2048]{1,0:T(8,128)(2,1)S(1)}, bf16[48,2048]{1,0:T(8,128)(2,1)S(1)}, u32[]{:S(2)}, u32[]{:S(2)}) %collective-permute-start.42) | collective-permute-done | bytes 196640 | tf_op jit(solution)/shard_map/ppermute | solution.py:24
  199.0 3.8 %collective-permute-done.44 = bf16[48,2048]{1,0:T(8,128)(2,1)S(1)} collective-permute-done((bf16[48,2048]{1,0:T(8,128)(2,1)S(1)}, bf16[48,2048]{1,0:T(8,128)(2,1)S(1)}, u32[]{:S(2)}, u32[]{:S(2)}) %collective-permute-start.44) | collective-permute-done | bytes 196640 | tf_op jit(solution)/shard_map/ppermute | solution.py:24
  203.5 8.7 %all_to_all.10 = bf16[8,48,256]{2,1,0:T(8,128)(2,1)S(1)} all-to-all(bf16[8,48,256]{2,1,0:T(8,128)(2,1)S(1)} %bitcast.153), channel_id=1, replica_groups=mesh['fs'=16,'tp'=8] {'tp'}, dimensions={0} | all-to-all | bytes 393216 | tf_op jit(solution)/shard_map/all_to_all | solution.py:274
  (223 shorter events, 40.3 us)
Async XLA Ops:
  6.5 91.2 %all-gather.3.cloned.1.call-start = ((), (), s32[]{:S(2)}) async-start(), calls=%async_computation.2 | async-start | bytes 5013504 | tf_op jit(solution)/shard_map/all_gather | solution.py:182
  8.3 170.8 %all-gather.5.cloned.1.call-start = ((), (), s32[]{:S(2)}) async-start(), calls=%async_computation.3 | async-start | bytes 10027008 | tf_op jit(solution)/shard_map/all_gather | solution.py:195
  8.4 10.0 %collective-permute-start.4 = (bf16[128,768]{1,0:T(8,128)(2,1)}, bf16[128,768]{1,0:T(8,128)(2,1)S(1)}, u32[]{:S(2)}, u32[]{:S(2)}) collective-permute-start(bf16[128,768]{1,0:T(8,128)(2,1)} %param.17), channel_id=1, source_target_pairs={{0,24},{8,0},{16,8},{24,16},{32,56},{40,32},{48,40},{56,48},{64,88... | collective-permute-start | bytes 589832 | tf_op jit(solution)/shard_map/ppermute | solution.py:24
  12.0 9.1 %collective-permute-start.6 = (bf16[128,768]{1,0:T(8,128)(2,1)}, bf16[128,768]{1,0:T(8,128)(2,1)S(1)}, u32[]{:S(2)}, u32[]{:S(2)}) collective-permute-start(bf16[128,768]{1,0:T(8,128)(2,1)} %param.17), channel_id=1, source_target_pairs={{0,8},{8,16},{16,24},{24,0},{32,40},{40,48},{48,56},{56,32},{64,72... | collective-permute-start | bytes 589832 | tf_op jit(solution)/shard_map/ppermute | solution.py:24
  12.0 9.3 %collective-permute-start = (bf16[128,768]{1,0:T(8,128)(2,1)}, bf16[128,768]{1,0:T(8,128)(2,1)S(1)}, u32[]{:S(2)}, u32[]{:S(2)}) collective-permute-start(bf16[128,768]{1,0:T(8,128)(2,1)} %param.16), channel_id=1, source_target_pairs={{0,96},{8,104},{16,112},{24,120},{32,0},{40,8},{48,16},{56,24},{64... | collective-permute-start | bytes 589832 | tf_op jit(solution)/shard_map/ppermute | solution.py:24
  15.8 8.3 %collective-permute-start.2 = (bf16[128,768]{1,0:T(8,128)(2,1)}, bf16[128,768]{1,0:T(8,128)(2,1)S(1)}, u32[]{:S(2)}, u32[]{:S(2)}) collective-permute-start(bf16[128,768]{1,0:T(8,128)(2,1)} %param.16), channel_id=1, source_target_pairs={{0,32},{8,40},{16,48},{24,56},{32,64},{40,72},{48,80},{56,88},{64,... | collective-permute-start | bytes 589832 | tf_op jit(solution)/shard_map/ppermute | solution.py:24
  18.4 5.8 %collective-permute-start.5 = (bf16[64,768]{1,0:T(8,128)(2,1)S(1)}, bf16[64,768]{1,0:T(8,128)(2,1)S(1)}, u32[]{:S(2)}, u32[]{:S(2)}) collective-permute-start(bf16[64,768]{1,0:T(8,128)(2,1)S(1)} %slice.599), channel_id=1, source_target_pairs={{0,24},{8,0},{16,8},{24,16},{32,56},{40,32},{48,40},{56,48},{64,88... | collective-permute-start | bytes 294920 | tf_op jit(solution)/shard_map/ppermute | solution.py:24
  21.2 4.7 %collective-permute-start.7 = (bf16[64,768]{1,0:T(8,128)(2,1)S(1)}, bf16[64,768]{1,0:T(8,128)(2,1)S(1)}, u32[]{:S(2)}, u32[]{:S(2)}) collective-permute-start(bf16[64,768]{1,0:T(8,128)(2,1)S(1)} %slice.600), channel_id=1, source_target_pairs={{0,8},{8,16},{16,24},{24,0},{32,40},{40,48},{48,56},{56,32},{64,72... | collective-permute-start | bytes 294920 | tf_op jit(solution)/shard_map/ppermute | solution.py:24
  21.3 5.0 %collective-permute-start.1 = (bf16[64,768]{1,0:T(8,128)(2,1)S(1)}, bf16[64,768]{1,0:T(8,128)(2,1)S(1)}, u32[]{:S(2)}, u32[]{:S(2)}) collective-permute-start(bf16[64,768]{1,0:T(8,128)(2,1)S(1)} %slice.597), channel_id=1, source_target_pairs={{0,96},{8,104},{16,112},{24,120},{32,0},{40,8},{48,16},{56,24},{64... | collective-permute-start | bytes 294920 | tf_op jit(solution)/shard_map/ppermute | solution.py:24
  24.0 5.5 %collective-permute-start.3 = (bf16[64,768]{1,0:T(8,128)(2,1)S(1)}, bf16[64,768]{1,0:T(8,128)(2,1)S(1)}, u32[]{:S(2)}, u32[]{:S(2)}) collective-permute-start(bf16[64,768]{1,0:T(8,128)(2,1)S(1)} %slice.598), channel_id=1, source_target_pairs={{0,32},{8,40},{16,48},{24,56},{32,64},{40,72},{48,80},{56,88},{64,... | collective-permute-start | bytes 294920 | tf_op jit(solution)/shard_map/ppermute | solution.py:24
  31.7 6.7 %collective-permute-start.8 = (bf16[392,256]{1,0:T(8,128)(2,1)S(1)}, bf16[392,256]{1,0:T(8,128)(2,1)S(1)}, u32[]{:S(2)}, u32[]{:S(2)}) collective-permute-start(bf16[392,256]{1,0:T(8,128)(2,1)S(1)} %pad_maximum_fusion.4), channel_id=1, source_target_pairs={{0,1},{1,0},{2,3},{3,2},{4,5},{5,4},{6,7},{7,6},{8,9},{9,8},{10,11... | collective-permute-start | bytes 602120 | tf_op jit(solution)/shard_map/ppermute | solution.py:24
  34.4 10.9 %collective-permute-start.9 = (bf16[392,256]{1,0:T(8,128)(2,1)S(1)}, bf16[392,256]{1,0:T(8,128)(2,1)S(1)}, u32[]{:S(2)}, u32[]{:S(2)}) collective-permute-start(bf16[392,256]{1,0:T(8,128)(2,1)S(1)} %pad_maximum_fusion.4), channel_id=1, source_target_pairs={{0,6},{1,7},{2,0},{3,1},{4,2},{5,3},{6,4},{7,5},{8,14},{9,15},{10,... | collective-permute-start | bytes 602120 | tf_op jit(solution)/shard_map/ppermute | solution.py:24
  36.9 12.7 %collective-permute-start.11 = (bf16[392,256]{1,0:T(8,128)(2,1)S(1)}, bf16[392,256]{1,0:T(8,128)(2,1)S(1)}, u32[]{:S(2)}, u32[]{:S(2)}) collective-permute-start(bf16[392,256]{1,0:T(8,128)(2,1)S(1)} %pad_maximum_fusion.4), channel_id=1, source_target_pairs={{0,4},{1,5},{2,6},{3,7},{4,0},{5,1},{6,2},{7,3},{8,12},{9,13},{10,... | collective-permute-start | bytes 602120 | tf_op jit(solution)/shard_map/ppermute | solution.py:24
  37.6 13.7 %collective-permute-start.13 = (bf16[392,256]{1,0:T(8,128)(2,1)S(1)}, bf16[392,256]{1,0:T(8,128)(2,1)S(1)}, u32[]{:S(2)}, u32[]{:S(2)}) collective-permute-start(bf16[392,256]{1,0:T(8,128)(2,1)S(1)} %pad_maximum_fusion.4), channel_id=1, source_target_pairs={{0,2},{1,3},{2,4},{3,5},{4,6},{5,7},{6,0},{7,1},{8,10},{9,11},{10,... | collective-permute-start | bytes 602120 | tf_op jit(solution)/shard_map/ppermute | solution.py:24
  38.1 24.7 %collective-permute-start.19 = (bf16[512,768]{1,0:T(8,128)(2,1)}, bf16[512,768]{1,0:T(8,128)(2,1)S(1)}, u32[]{:S(2)}, u32[]{:S(2)}) collective-permute-start(bf16[512,768]{1,0:T(8,128)(2,1)} %copy-done.6), channel_id=1, source_target_pairs={{0,96},{8,104},{16,112},{24,120},{32,0},{40,8},{48,16},{56,24},{64... | collective-permute-start | bytes 2359304 | tf_op jit(solution)/shard_map/ppermute | solution.py:24
  38.4 26.0 %collective-permute-start.20 = (bf16[512,768]{1,0:T(8,128)(2,1)}, bf16[512,768]{1,0:T(8,128)(2,1)S(1)}, u32[]{:S(2)}, u32[]{:S(2)}) collective-permute-start(bf16[512,768]{1,0:T(8,128)(2,1)} %copy-done.6), channel_id=1, source_target_pairs={{0,32},{8,40},{16,48},{24,56},{32,64},{40,72},{48,80},{56,88},{64,... | collective-permute-start | bytes 2359304 | tf_op jit(solution)/shard_map/ppermute | solution.py:24
  45.4 30.5 %collective-permute-start.15 = (bf16[512,768]{1,0:T(8,128)(2,1)S(1)}, bf16[512,768]{1,0:T(8,128)(2,1)S(1)}, u32[]{:S(2)}, u32[]{:S(2)}) collective-permute-start(bf16[512,768]{1,0:T(8,128)(2,1)S(1)} %constant_dynamic-update-slice_fusion), channel_id=1, source_target_pairs={{0,24},{8,0},{16,8},{24,16},{32,56},{40,32},{48,40},{56,48},{64,88... | collective-permute-start | bytes 2359304 | tf_op jit(solution)/shard_map/ppermute | solution.py:24
  49.6 3.2 %collective-permute-start.10 = (bf16[392,256]{1,0:T(8,128)(2,1)S(1)}, bf16[392,256]{1,0:T(8,128)(2,1)S(1)}, u32[]{:S(2)}, u32[]{:S(2)}) collective-permute-start(bf16[392,256]{1,0:T(8,128)(2,1)S(1)} %collective-permute-done.9), channel_id=1, source_target_pairs={{0,1},{1,0},{2,3},{3,2},{4,5},{5,4},{6,7},{7,6},{8,9},{9,8},{10,11... | collective-permute-start | bytes 602120 | tf_op jit(solution)/shard_map/ppermute | solution.py:24
  51.3 1.5 collective-permute-start.12
  52.8 26.7 %collective-permute-start.16 = (bf16[512,768]{1,0:T(8,128)(2,1)S(1)}, bf16[512,768]{1,0:T(8,128)(2,1)S(1)}, u32[]{:S(2)}, u32[]{:S(2)}) collective-permute-start(bf16[512,768]{1,0:T(8,128)(2,1)S(1)} %constant_dynamic-update-slice_fusion), channel_id=1, source_target_pairs={{0,8},{8,16},{16,24},{24,0},{32,40},{40,48},{48,56},{56,32},{64,72... | collective-permute-start | bytes 2359304 | tf_op jit(solution)/shard_map/ppermute | solution.py:24
  52.9 1.5 collective-permute-start.14
  62.9 18.8 %collective-permute-start.21 = (bf16[256,768]{1,0:T(8,128)(2,1)S(1)}, bf16[256,768]{1,0:T(8,128)(2,1)S(1)}, u32[]{:S(2)}, u32[]{:S(2)}) collective-permute-start(bf16[256,768]{1,0:T(8,128)(2,1)S(1)} %slice.611), channel_id=1, source_target_pairs={{0,96},{8,104},{16,112},{24,120},{32,0},{40,8},{48,16},{56,24},{64... | collective-permute-start | bytes 1179656 | tf_op jit(solution)/shard_map/ppermute | solution.py:24
  64.4 19.2 %collective-permute-start.22 = (bf16[256,768]{1,0:T(8,128)(2,1)S(1)}, bf16[256,768]{1,0:T(8,128)(2,1)S(1)}, u32[]{:S(2)}, u32[]{:S(2)}) collective-permute-start(bf16[256,768]{1,0:T(8,128)(2,1)S(1)} %slice.612), channel_id=1, source_target_pairs={{0,32},{8,40},{16,48},{24,56},{32,64},{40,72},{48,80},{56,88},{64,... | collective-permute-start | bytes 1179656 | tf_op jit(solution)/shard_map/ppermute | solution.py:24
  75.8 15.7 %collective-permute-start.17 = (bf16[256,768]{1,0:T(8,128)(2,1)S(1)}, bf16[256,768]{1,0:T(8,128)(2,1)S(1)}, u32[]{:S(2)}, u32[]{:S(2)}) collective-permute-start(bf16[256,768]{1,0:T(8,128)(2,1)S(1)} %slice.609), channel_id=1, source_target_pairs={{0,24},{8,0},{16,8},{24,16},{32,56},{40,32},{48,40},{56,48},{64,88... | collective-permute-start | bytes 1179656 | tf_op jit(solution)/shard_map/ppermute | solution.py:24
  79.5 15.8 %collective-permute-start.18 = (bf16[256,768]{1,0:T(8,128)(2,1)S(1)}, bf16[256,768]{1,0:T(8,128)(2,1)S(1)}, u32[]{:S(2)}, u32[]{:S(2)}) collective-permute-start(bf16[256,768]{1,0:T(8,128)(2,1)S(1)} %slice.610), channel_id=1, source_target_pairs={{0,8},{8,16},{16,24},{24,0},{32,40},{40,48},{48,56},{56,32},{64,72... | collective-permute-start | bytes 1179656 | tf_op jit(solution)/shard_map/ppermute | solution.py:24
  100.6 2.8 %collective-permute-start.23 = (bf16[192,2048]{1,0:T(8,128)(2,1)S(1)}, bf16[192,2048]{1,0:T(8,128)(2,1)S(1)}, u32[]{:S(2)}, u32[]{:S(2)}) collective-permute-start(bf16[192,2048]{1,0:T(8,128)(2,1)S(1)} %fusion.8), channel_id=1, source_target_pairs={{0,1},{1,0},{2,3},{3,2},{4,5},{5,4},{6,7},{7,6},{8,9},{9,8},{10,11... | collective-permute-start | bytes 2359304 | tf_op jit(solution)/shard_map/ppermute | solution.py:24
  103.7 7.7 %collective-permute-start.24 = (bf16[48,2048]{1,0:T(8,128)(2,1)S(1)}, bf16[48,2048]{1,0:T(8,128)(2,1)S(1)}, u32[]{:S(2)}, u32[]{:S(2)}) collective-permute-start(bf16[48,2048]{1,0:T(8,128)(2,1)S(1)} %get-tuple-element.79), channel_id=1, source_target_pairs={{0,4},{1,5},{2,6},{3,7},{4,0},{5,1},{6,2},{7,3},{8,12},{9,13},{10,... | collective-permute-start | bytes 589832 | tf_op jit(solution)/shard_map/ppermute | solution.py:24
  106.2 9.5 %collective-permute-start.25 = (bf16[48,2048]{1,0:T(8,128)(2,1)S(1)}, bf16[48,2048]{1,0:T(8,128)(2,1)S(1)}, u32[]{:S(2)}, u32[]{:S(2)}) collective-permute-start(bf16[48,2048]{1,0:T(8,128)(2,1)S(1)} %get-tuple-element.81), channel_id=1, source_target_pairs={{0,6},{1,7},{2,0},{3,1},{4,2},{5,3},{6,4},{7,5},{8,14},{9,15},{10,... | collective-permute-start | bytes 589832 | tf_op jit(solution)/shard_map/ppermute | solution.py:24
  107.3 8.7 %collective-permute-start.26 = (bf16[48,2048]{1,0:T(8,128)(2,1)S(1)}, bf16[48,2048]{1,0:T(8,128)(2,1)S(1)}, u32[]{:S(2)}, u32[]{:S(2)}) collective-permute-start(bf16[48,2048]{1,0:T(8,128)(2,1)S(1)} %get-tuple-element.80), channel_id=1, source_target_pairs={{0,2},{1,3},{2,4},{3,5},{4,6},{5,7},{6,0},{7,1},{8,10},{9,11},{10,... | collective-permute-start | bytes 589832 | tf_op jit(solution)/shard_map/ppermute | solution.py:24
  116.6 6.6 %collective-permute-start.27 = (bf16[48,2048]{1,0:T(8,128)(2,1)S(1)}, bf16[48,2048]{1,0:T(8,128)(2,1)S(1)}, u32[]{:S(2)}, u32[]{:S(2)}) collective-permute-start(bf16[48,2048]{1,0:T(8,128)(2,1)S(1)} %get-tuple-element.44), channel_id=1, source_target_pairs={{0,6},{1,7},{2,0},{3,1},{4,2},{5,3},{6,4},{7,5},{8,14},{9,15},{10,... | collective-permute-start | bytes 589832 | tf_op jit(solution)/shard_map/ppermute | solution.py:24
  119.5 8.1 %collective-permute-start.28 = (bf16[48,2048]{1,0:T(8,128)(2,1)S(1)}, bf16[48,2048]{1,0:T(8,128)(2,1)S(1)}, u32[]{:S(2)}, u32[]{:S(2)}) collective-permute-start(bf16[48,2048]{1,0:T(8,128)(2,1)S(1)} %get-tuple-element.44), channel_id=1, source_target_pairs={{0,2},{1,3},{2,4},{3,5},{4,6},{5,7},{6,0},{7,1},{8,10},{9,11},{10,... | collective-permute-start | bytes 589832 | tf_op jit(solution)/shard_map/ppermute | solution.py:24
  119.5 12.9 %collective-permute-start.29 = (bf16[48,2048]{1,0:T(8,128)(2,1)S(1)}, bf16[48,2048]{1,0:T(8,128)(2,1)S(1)}, u32[]{:S(2)}, u32[]{:S(2)}) collective-permute-start(bf16[48,2048]{1,0:T(8,128)(2,1)S(1)} %get-tuple-element.44), channel_id=1, source_target_pairs={{0,4},{1,5},{2,6},{3,7},{4,0},{5,1},{6,2},{7,3},{8,12},{9,13},{10,... | collective-permute-start | bytes 589832 | tf_op jit(solution)/shard_map/ppermute | solution.py:24
  127.7 6.3 %collective-permute-start.30 = (bf16[144,2048]{1,0:T(8,128)(2,1)S(1)}, bf16[144,2048]{1,0:T(8,128)(2,1)S(1)}, u32[]{:S(2)}, u32[]{:S(2)}) collective-permute-start(bf16[144,2048]{1,0:T(8,128)(2,1)S(1)} %pad_maximum_fusion.1), channel_id=1, source_target_pairs={{0,1},{1,0},{2,3},{3,2},{4,5},{5,4},{6,7},{7,6},{8,9},{9,8},{10,11... | collective-permute-start | bytes 1769480 | tf_op jit(solution)/shard_map/ppermute | solution.py:24
  132.4 1.9 collective-permute-start.31
  136.9 8.4 %all-to-all-start = ((f32[8,1,768]{2,1,0:T(1,128)}), f32[8,1,768]{2,1,0:T(1,128)S(1)}, u32[]{:S(2)}, u32[]{:S(2)}) async-start(f32[8,1,768]{2,1,0:T(1,128)} %broadcast_in_dim.2), calls=%async_computation | async-start | bytes 49152 | tf_op jit(solution)/shard_map/all_to_all | solution.py:151
  147.0 2.7 %collective-permute-start.32 = (bf16[192,2048]{1,0:T(8,128)(2,1)S(1)}, bf16[192,2048]{1,0:T(8,128)(2,1)S(1)}, u32[]{:S(2)}, u32[]{:S(2)}) collective-permute-start(bf16[192,2048]{1,0:T(8,128)(2,1)S(1)} %convolution_convert_fusion), channel_id=1, source_target_pairs={{0,1},{1,0},{2,3},{3,2},{4,5},{5,4},{6,7},{7,6},{8,9},{9,8},{10,11... | collective-permute-start | bytes 2359304 | tf_op jit(solution)/shard_map/ppermute | solution.py:24
  150.0 7.7 %collective-permute-start.33 = (bf16[48,2048]{1,0:T(8,128)(2,1)S(1)}, bf16[48,2048]{1,0:T(8,128)(2,1)S(1)}, u32[]{:S(2)}, u32[]{:S(2)}) collective-permute-start(bf16[48,2048]{1,0:T(8,128)(2,1)S(1)} %get-tuple-element.76), channel_id=1, source_target_pairs={{0,4},{1,5},{2,6},{3,7},{4,0},{5,1},{6,2},{7,3},{8,12},{9,13},{10,... | collective-permute-start | bytes 589832 | tf_op jit(solution)/shard_map/ppermute | solution.py:24
  150.9 9.5 %collective-permute-start.34 = (bf16[48,2048]{1,0:T(8,128)(2,1)S(1)}, bf16[48,2048]{1,0:T(8,128)(2,1)S(1)}, u32[]{:S(2)}, u32[]{:S(2)}) collective-permute-start(bf16[48,2048]{1,0:T(8,128)(2,1)S(1)} %get-tuple-element.78), channel_id=1, source_target_pairs={{0,6},{1,7},{2,0},{3,1},{4,2},{5,3},{6,4},{7,5},{8,14},{9,15},{10,... | collective-permute-start | bytes 589832 | tf_op jit(solution)/shard_map/ppermute | solution.py:24
  152.8 9.8 %collective-permute-start.35 = (bf16[48,2048]{1,0:T(8,128)(2,1)S(1)}, bf16[48,2048]{1,0:T(8,128)(2,1)S(1)}, u32[]{:S(2)}, u32[]{:S(2)}) collective-permute-start(bf16[48,2048]{1,0:T(8,128)(2,1)S(1)} %get-tuple-element.77), channel_id=1, source_target_pairs={{0,2},{1,3},{2,4},{3,5},{4,6},{5,7},{6,0},{7,1},{8,10},{9,11},{10,... | collective-permute-start | bytes 589832 | tf_op jit(solution)/shard_map/ppermute | solution.py:24
  163.3 6.2 %collective-permute-start.36 = (bf16[48,2048]{1,0:T(8,128)(2,1)S(1)}, bf16[48,2048]{1,0:T(8,128)(2,1)S(1)}, u32[]{:S(2)}, u32[]{:S(2)}) collective-permute-start(bf16[48,2048]{1,0:T(8,128)(2,1)S(1)} %get-tuple-element.36), channel_id=1, source_target_pairs={{0,6},{1,7},{2,0},{3,1},{4,2},{5,3},{6,4},{7,5},{8,14},{9,15},{10,... | collective-permute-start | bytes 589832 | tf_op jit(solution)/shard_map/ppermute | solution.py:24
  164.3 8.3 %collective-permute-start.37 = (bf16[48,2048]{1,0:T(8,128)(2,1)S(1)}, bf16[48,2048]{1,0:T(8,128)(2,1)S(1)}, u32[]{:S(2)}, u32[]{:S(2)}) collective-permute-start(bf16[48,2048]{1,0:T(8,128)(2,1)S(1)} %get-tuple-element.36), channel_id=1, source_target_pairs={{0,2},{1,3},{2,4},{3,5},{4,6},{5,7},{6,0},{7,1},{8,10},{9,11},{10,... | collective-permute-start | bytes 589832 | tf_op jit(solution)/shard_map/ppermute | solution.py:24
  164.8 12.4 %collective-permute-start.38 = (bf16[48,2048]{1,0:T(8,128)(2,1)S(1)}, bf16[48,2048]{1,0:T(8,128)(2,1)S(1)}, u32[]{:S(2)}, u32[]{:S(2)}) collective-permute-start(bf16[48,2048]{1,0:T(8,128)(2,1)S(1)} %get-tuple-element.36), channel_id=1, source_target_pairs={{0,4},{1,5},{2,6},{3,7},{4,0},{5,1},{6,2},{7,3},{8,12},{9,13},{10,... | collective-permute-start | bytes 589832 | tf_op jit(solution)/shard_map/ppermute | solution.py:24
  172.6 6.2 %collective-permute-start.39 = (bf16[144,2048]{1,0:T(8,128)(2,1)S(1)}, bf16[144,2048]{1,0:T(8,128)(2,1)S(1)}, u32[]{:S(2)}, u32[]{:S(2)}) collective-permute-start(bf16[144,2048]{1,0:T(8,128)(2,1)S(1)} %pad_maximum_fusion.2), channel_id=1, source_target_pairs={{0,1},{1,0},{2,3},{3,2},{4,5},{5,4},{6,7},{7,6},{8,9},{9,8},{10,11... | collective-permute-start | bytes 1769480 | tf_op jit(solution)/shard_map/ppermute | solution.py:24
  177.2 1.9 collective-permute-start.40
  187.5 2.4 %collective-permute-start.41 = (bf16[192,2048]{1,0:T(8,128)(2,1)S(1)}, bf16[192,2048]{1,0:T(8,128)(2,1)S(1)}, u32[]{:S(2)}, u32[]{:S(2)}) collective-permute-start(bf16[192,2048]{1,0:T(8,128)(2,1)S(1)} %fusion.11), channel_id=1, source_target_pairs={{0,1},{1,0},{2,3},{3,2},{4,5},{5,4},{6,7},{7,6},{8,9},{9,8},{10,11... | collective-permute-start | bytes 2359304 | tf_op jit(solution)/shard_map/ppermute | solution.py:24
  190.2 7.7 %collective-permute-start.42 = (bf16[48,2048]{1,0:T(8,128)(2,1)S(1)}, bf16[48,2048]{1,0:T(8,128)(2,1)S(1)}, u32[]{:S(2)}, u32[]{:S(2)}) collective-permute-start(bf16[48,2048]{1,0:T(8,128)(2,1)S(1)} %get-tuple-element.73), channel_id=1, source_target_pairs={{0,4},{1,5},{2,6},{3,7},{4,0},{5,1},{6,2},{7,3},{8,12},{9,13},{10,... | collective-permute-start | bytes 589832 | tf_op jit(solution)/shard_map/ppermute | solution.py:24
  190.3 8.7 %collective-permute-start.43 = (bf16[48,2048]{1,0:T(8,128)(2,1)S(1)}, bf16[48,2048]{1,0:T(8,128)(2,1)S(1)}, u32[]{:S(2)}, u32[]{:S(2)}) collective-permute-start(bf16[48,2048]{1,0:T(8,128)(2,1)S(1)} %get-tuple-element.75), channel_id=1, source_target_pairs={{0,6},{1,7},{2,0},{3,1},{4,2},{5,3},{6,4},{7,5},{8,14},{9,15},{10,... | collective-permute-start | bytes 589832 | tf_op jit(solution)/shard_map/ppermute | solution.py:24
  190.4 12.4 %collective-permute-start.44 = (bf16[48,2048]{1,0:T(8,128)(2,1)S(1)}, bf16[48,2048]{1,0:T(8,128)(2,1)S(1)}, u32[]{:S(2)}, u32[]{:S(2)}) collective-permute-start(bf16[48,2048]{1,0:T(8,128)(2,1)S(1)} %get-tuple-element.74), channel_id=1, source_target_pairs={{0,2},{1,3},{2,4},{3,5},{4,6},{5,7},{6,0},{7,1},{8,10},{9,11},{10,... | collective-permute-start | bytes 589832 | tf_op jit(solution)/shard_map/ppermute | solution.py:24
  (12 other events, 75.8 us)
Sparse Core Ops, SparseCore 0:
  9.4 82.0 all-gather.2
  93.6 76.5 all-gather.4

commit v3 on v2

--- a/solution.py
+++ b/solution.py
@@ -72,6 +72,7 @@
         out_ref[...] = (jax.nn.silu(gate) * up).astype(BF16)
 
     depth = weights.shape[0]
+    source = pltpu.with_memory_space_constraint(weights, pltpu.HBM)
     return pl.pallas_call(
         kernel,
         grid=(count,),
@@ -84,7 +85,7 @@
         out_shape=jax.ShapeDtypeStruct((rows.shape[0], width), BF16),
         compiler_params=pltpu.CompilerParams(vmem_limit_bytes=24 * 2**20),
         name="gated_hidden",
-    )(rows, weights, weights)
+    )(rows, source, source)
 
 
 def rolled(value, axis, shift):
@@ -107,7 +108,8 @@
     blocks = [value] + [pull(value, "x", d) for d in (2, 1, 3)]
     near = jnp.concatenate([blocks[0], blocks[2], blocks[3]], axis=0)
     near_other = pull(near, "c", 1)
-    return near, blocks[1], near_other, pull(blocks[1], "c", 1)
+    far_other = pull(blocks[1], "c", 1)
+    return near, blocks[1], near_other, far_other
 
 
 def summed_rows(rows_other, rows_own):

time: 220 us -> 219 us (level)
  local copies, waits for them, and re-layouts: 10 us -> 6.36 us
  Pallas kernels: 5.21 us -> 7.41 us
    unnamed x47, local copies, waits for them, and re-layouts: 8.05 us -> 4.38 us
    pallas_call x1, Pallas kernels: 3.45 us -> 5.65 us  [gated_hidden(): pl.pallas_call(kernel, grid=(count,), in_specs=[pl.BlockSpec(rows.shape,...]
where the time goes in v3:
time: 219 us; the launch traced here: 218 us
  waiting for transfers between devices  98.1 us (45%)
  starting transfers between devices  61.7 us (28%)
  between operations  14.5 us (7%)
  matrix products  13.8 us (6%)
  blocking collectives  8.74 us (4%)
  other arithmetic  7.69 us (4%)
  Pallas kernels  7.41 us (3%)
  local copies, waits for them, and re-layouts  6.36 us (3%)
    ppermute x45, waiting for transfers between devices, pull(): return lax.ppermute(value, 'fs' if axis in 'zy' else 'tp', pairs)  93.3 us
    ppermute x45, starting transfers between devices, pull(): return lax.ppermute(value, 'fs' if axis in 'zy' else 'tp', pairs)  58 us
    dot_general x14, matrix products, matmul(): return jnp.dot(left, right, preferred_element_type=F32)  10.8 us
    all_to_all x1, blocking collectives, layer(): out = lax.all_to_all(out, 'tp', split_axis=0, concat_axis=0, tiled=True)  8.74 us
    pallas_call x1, Pallas kernels, gated_hidden(): pl.pallas_call(kernel, grid=(count,), in_specs=[pl.BlockSpec(rows.shape,...  5.65 us
    all_to_all x1, waiting for transfers between devices, channel_stats(): both = lax.all_to_all(both, 'tp', split_axis=0, concat_axis=0, tiled=True)  4.75 us
    unnamed x47, local copies, waits for them, and re-layouts  4.38 us
  transfers between devices with their start and end apart: 48, of which 33 were waited for; matrix products, arithmetic and copies ran while one was open for 11% of the time, Pallas kernels for 0%

profile of v3, /device:TPU:1, one launch (start us, length us, event | category | flops | bytes accessed | tf_op | source)
XLA Modules:
  0.0 218.3 jit_solution(10443946095142550572)
XLA Ops:
  6.5 1.8 packed.1
  8.4 3.6 %collective-permute-start.4 = (bf16[128,768]{1,0:T(8,128)(2,1)}, bf16[128,768]{1,0:T(8,128)(2,1)S(1)}, u32[]{:S(2)}, u32[]{:S(2)}) collective-permute-start(bf16[128,768]{1,0:T(8,128)(2,1)} %param.17), channel_id=1, source_target_pairs={{0,24},{8,0},{16,8},{24,16},{32,56},{40,32},{48,40},{56,48},{64,88... | collective-permute-start | bytes 589832 | tf_op jit(solution)/shard_map/ppermute | solution.py:24
  12.0 3.8 %collective-permute-start = (bf16[128,768]{1,0:T(8,128)(2,1)}, bf16[128,768]{1,0:T(8,128)(2,1)S(1)}, u32[]{:S(2)}, u32[]{:S(2)}) collective-permute-start(bf16[128,768]{1,0:T(8,128)(2,1)} %param.16), channel_id=1, source_target_pairs={{0,96},{8,104},{16,112},{24,120},{32,0},{40,8},{48,16},{56,24},{64... | collective-permute-start | bytes 589832 | tf_op jit(solution)/shard_map/ppermute | solution.py:24
  18.4 2.7 %collective-permute-start.5 = (bf16[64,768]{1,0:T(8,128)(2,1)S(1)}, bf16[64,768]{1,0:T(8,128)(2,1)S(1)}, u32[]{:S(2)}, u32[]{:S(2)}) collective-permute-start(bf16[64,768]{1,0:T(8,128)(2,1)S(1)} %slice.599), channel_id=1, source_target_pairs={{0,24},{8,0},{16,8},{24,16},{32,56},{40,32},{48,40},{56,48},{64,88... | collective-permute-start | bytes 294920 | tf_op jit(solution)/shard_map/ppermute | solution.py:24
  21.3 2.7 %collective-permute-start.1 = (bf16[64,768]{1,0:T(8,128)(2,1)S(1)}, bf16[64,768]{1,0:T(8,128)(2,1)S(1)}, u32[]{:S(2)}, u32[]{:S(2)}) collective-permute-start(bf16[64,768]{1,0:T(8,128)(2,1)S(1)} %slice.597), channel_id=1, source_target_pairs={{0,96},{8,104},{16,112},{24,120},{32,0},{40,8},{48,16},{56,24},{64... | collective-permute-start | bytes 294920 | tf_op jit(solution)/shard_map/ppermute | solution.py:24
  24.2 1.7 collective-permute-done.7
  26.3 3.3 %collective-permute-done.3 = bf16[64,768]{1,0:T(8,128)(2,1)S(1)} collective-permute-done((bf16[64,768]{1,0:T(8,128)(2,1)S(1)}, bf16[64,768]{1,0:T(8,128)(2,1)S(1)}, u32[]{:S(2)}, u32[]{:S(2)}) %collective-permute-start.3) | collective-permute-done | bytes 98336 | tf_op jit(solution)/shard_map/ppermute | solution.py:24
  31.7 2.8 %collective-permute-start.8 = (bf16[392,256]{1,0:T(8,128)(2,1)S(1)}, bf16[392,256]{1,0:T(8,128)(2,1)S(1)}, u32[]{:S(2)}, u32[]{:S(2)}) collective-permute-start(bf16[392,256]{1,0:T(8,128)(2,1)S(1)} %pad_maximum_fusion.4), channel_id=1, source_target_pairs={{0,1},{1,0},{2,3},{3,2},{4,5},{5,4},{6,7},{7,6},{8,9},{9,8},{10,11... | collective-permute-start | bytes 602120 | tf_op jit(solution)/shard_map/ppermute | solution.py:24
  34.4 2.5 %collective-permute-start.9 = (bf16[392,256]{1,0:T(8,128)(2,1)S(1)}, bf16[392,256]{1,0:T(8,128)(2,1)S(1)}, u32[]{:S(2)}, u32[]{:S(2)}) collective-permute-start(bf16[392,256]{1,0:T(8,128)(2,1)S(1)} %pad_maximum_fusion.4), channel_id=1, source_target_pairs={{0,6},{1,7},{2,0},{3,1},{4,2},{5,3},{6,4},{7,5},{8,14},{9,15},{10,... | collective-permute-start | bytes 602120 | tf_op jit(solution)/shard_map/ppermute | solution.py:24
  39.8 5.6 %collective-permute-done.9 = bf16[392,256]{1,0:T(8,128)(2,1)S(1)} collective-permute-done((bf16[392,256]{1,0:T(8,128)(2,1)S(1)}, bf16[392,256]{1,0:T(8,128)(2,1)S(1)}, u32[]{:S(2)}, u32[]{:S(2)}) %collective-permute-start.9) | collective-permute-done | bytes 200736 | tf_op jit(solution)/shard_map/ppermute | solution.py:24
  45.4 4.3 %collective-permute-start.15 = (bf16[512,768]{1,0:T(8,128)(2,1)S(1)}, bf16[512,768]{1,0:T(8,128)(2,1)S(1)}, u32[]{:S(2)}, u32[]{:S(2)}) collective-permute-start(bf16[512,768]{1,0:T(8,128)(2,1)S(1)} %constant_dynamic-update-slice_fusion), channel_id=1, source_target_pairs={{0,24},{8,0},{16,8},{24,16},{32,56},{40,32},{48,40},{56,48},{64,88... | collective-permute-start | bytes 2359304 | tf_op jit(solution)/shard_map/ppermute | solution.py:24
  49.6 1.4 collective-permute-start.10
  51.5 1.3 collective-permute-done.12
  56.4 6.4 %collective-permute-done.19 = bf16[512,768]{1,0:T(8,128)(2,1)S(1)} collective-permute-done((bf16[512,768]{1,0:T(8,128)(2,1)}, bf16[512,768]{1,0:T(8,128)(2,1)S(1)}, u32[]{:S(2)}, u32[]{:S(2)}) %collective-permute-start.19) | collective-permute-done | bytes 786464 | tf_op jit(solution)/shard_map/ppermute | solution.py:24
  62.9 1.5 collective-permute-start.21
  64.5 11.3 %collective-permute-done.15 = bf16[512,768]{1,0:T(8,128)(2,1)S(1)} collective-permute-done((bf16[512,768]{1,0:T(8,128)(2,1)S(1)}, bf16[512,768]{1,0:T(8,128)(2,1)S(1)}, u32[]{:S(2)}, u32[]{:S(2)}) %collective-permute-start.15) | collective-permute-done | bytes 786464 | tf_op jit(solution)/shard_map/ppermute | solution.py:24
  75.8 2.3 %collective-permute-start.17 = (bf16[256,768]{1,0:T(8,128)(2,1)S(1)}, bf16[256,768]{1,0:T(8,128)(2,1)S(1)}, u32[]{:S(2)}, u32[]{:S(2)}) collective-permute-start(bf16[256,768]{1,0:T(8,128)(2,1)S(1)} %slice.609), channel_id=1, source_target_pairs={{0,24},{8,0},{16,8},{24,16},{32,56},{40,32},{48,40},{56,48},{64,88... | collective-permute-start | bytes 1179656 | tf_op jit(solution)/shard_map/ppermute | solution.py:24
  78.1 1.3 collective-permute-done.16
  82.0 1.6 collective-permute-done.22
  84.0 7.6 %collective-permute-done.17 = bf16[256,768]{1,0:T(8,128)(2,1)S(1)} collective-permute-done((bf16[256,768]{1,0:T(8,128)(2,1)S(1)}, bf16[256,768]{1,0:T(8,128)(2,1)S(1)}, u32[]{:S(2)}, u32[]{:S(2)}) %collective-permute-start.17) | collective-permute-done | bytes 393248 | tf_op jit(solution)/shard_map/ppermute | solution.py:24
  91.9 3.4 %collective-permute-done.18 = bf16[256,768]{1,0:T(8,128)(2,1)S(1)} collective-permute-done((bf16[256,768]{1,0:T(8,128)(2,1)S(1)}, bf16[256,768]{1,0:T(8,128)(2,1)S(1)}, u32[]{:S(2)}, u32[]{:S(2)}) %collective-permute-start.18) | collective-permute-done | bytes 393248 | tf_op jit(solution)/shard_map/ppermute | solution.py:24
  97.8 2.8 %fusion.8 = bf16[192,2048]{1,0:T(8,128)(2,1)S(1)} fusion(bf16[192,768]{1,0:T(8,128)(2,1)S(1)} %bitcast.161, bf16[1152,2048]{1,0:T(8,128)(2,1)} %all-gather.3.cloned.1.call-done), kind=kOutput, calls=%fused_computation.8 | convolution fusion | flops 604372992 | bytes 4227072 | tf_op jit(solution)/shard_map/dot_general | solution.py:41
  103.7 2.5 %collective-permute-start.24 = (bf16[48,2048]{1,0:T(8,128)(2,1)S(1)}, bf16[48,2048]{1,0:T(8,128)(2,1)S(1)}, u32[]{:S(2)}, u32[]{:S(2)}) collective-permute-start(bf16[48,2048]{1,0:T(8,128)(2,1)S(1)} %get-tuple-element.79), channel_id=1, source_target_pairs={{0,4},{1,5},{2,6},{3,7},{4,0},{5,1},{6,2},{7,3},{8,12},{9,13},{10,... | collective-permute-start | bytes 589832 | tf_op jit(solution)/shard_map/ppermute | solution.py:24
  107.7 3.7 %collective-permute-done.24 = bf16[48,2048]{1,0:T(8,128)(2,1)S(1)} collective-permute-done((bf16[48,2048]{1,0:T(8,128)(2,1)S(1)}, bf16[48,2048]{1,0:T(8,128)(2,1)S(1)}, u32[]{:S(2)}, u32[]{:S(2)}) %collective-permute-start.24) | collective-permute-done | bytes 196640 | tf_op jit(solution)/shard_map/ppermute | solution.py:24
  111.4 4.3 %collective-permute-done.25 = bf16[48,2048]{1,0:T(8,128)(2,1)S(1)} collective-permute-done((bf16[48,2048]{1,0:T(8,128)(2,1)S(1)}, bf16[48,2048]{1,0:T(8,128)(2,1)S(1)}, u32[]{:S(2)}, u32[]{:S(2)}) %collective-permute-start.25) | collective-permute-done | bytes 196640 | tf_op jit(solution)/shard_map/ppermute | solution.py:24
  116.6 2.9 %collective-permute-start.27 = (bf16[48,2048]{1,0:T(8,128)(2,1)S(1)}, bf16[48,2048]{1,0:T(8,128)(2,1)S(1)}, u32[]{:S(2)}, u32[]{:S(2)}) collective-permute-start(bf16[48,2048]{1,0:T(8,128)(2,1)S(1)} %get-tuple-element.44), channel_id=1, source_target_pairs={{0,6},{1,7},{2,0},{3,1},{4,2},{5,3},{6,4},{7,5},{8,14},{9,15},{10,... | collective-permute-start | bytes 589832 | tf_op jit(solution)/shard_map/ppermute | solution.py:24
  119.5 1.5 collective-permute-start.29
  121.1 2.2 collective-permute-done.27
  123.2 4.4 %collective-permute-done.28 = bf16[48,2048]{1,0:T(8,128)(2,1)S(1)} collective-permute-done((bf16[48,2048]{1,0:T(8,128)(2,1)S(1)}, bf16[48,2048]{1,0:T(8,128)(2,1)S(1)}, u32[]{:S(2)}, u32[]{:S(2)}) %collective-permute-start.28) | collective-permute-done | bytes 196640 | tf_op jit(solution)/shard_map/ppermute | solution.py:24
  127.7 4.7 %collective-permute-start.30 = (bf16[144,2048]{1,0:T(8,128)(2,1)S(1)}, bf16[144,2048]{1,0:T(8,128)(2,1)S(1)}, u32[]{:S(2)}, u32[]{:S(2)}) collective-permute-start(bf16[144,2048]{1,0:T(8,128)(2,1)S(1)} %pad_maximum_fusion.1), channel_id=1, source_target_pairs={{0,1},{1,0},{2,3},{3,2},{4,5},{5,4},{6,7},{7,6},{8,9},{9,8},{10,11... | collective-permute-start | bytes 1769480 | tf_op jit(solution)/shard_map/ppermute | solution.py:24
  132.6 1.5 collective-permute-done.30
  136.9 3.6 %all-to-all-start = ((f32[8,1,768]{2,1,0:T(1,128)}), f32[8,1,768]{2,1,0:T(1,128)S(1)}, u32[]{:S(2)}, u32[]{:S(2)}) async-start(f32[8,1,768]{2,1,0:T(1,128)} %broadcast_in_dim.2), calls=%async_computation | async-start | bytes 49152 | tf_op jit(solution)/shard_map/all_to_all | solution.py:153
  140.5 4.8 %all-to-all-done = f32[8,1,768]{2,1,0:T(1,128)S(1)} async-done(((f32[8,1,768]{2,1,0:T(1,128)}), f32[8,1,768]{2,1,0:T(1,128)S(1)}, u32[]{:S(2)}, u32[]{:S(2)}) %all-to-all-start) | async-done | bytes 24608 | tf_op jit(solution)/shard_map/all_to_all | solution.py:153
  145.6 1.4 convolution_convert_fusion
  147.8 1.4 fusion.23
  150.9 1.9 collective-permute-start.34
  152.8 4.8 %collective-permute-done.33 = bf16[48,2048]{1,0:T(8,128)(2,1)S(1)} collective-permute-done((bf16[48,2048]{1,0:T(8,128)(2,1)S(1)}, bf16[48,2048]{1,0:T(8,128)(2,1)S(1)}, u32[]{:S(2)}, u32[]{:S(2)}) %collective-permute-start.33) | collective-permute-done | bytes 196640 | tf_op jit(solution)/shard_map/ppermute | solution.py:24
  157.7 2.8 %collective-permute-done.34 = bf16[48,2048]{1,0:T(8,128)(2,1)S(1)} collective-permute-done((bf16[48,2048]{1,0:T(8,128)(2,1)S(1)}, bf16[48,2048]{1,0:T(8,128)(2,1)S(1)}, u32[]{:S(2)}, u32[]{:S(2)}) %collective-permute-start.34) | collective-permute-done | bytes 196640 | tf_op jit(solution)/shard_map/ppermute | solution.py:24
  160.5 2.1 collective-permute-done.35
  165.8 3.7 %collective-permute-done.36 = bf16[48,2048]{1,0:T(8,128)(2,1)S(1)} collective-permute-done((bf16[48,2048]{1,0:T(8,128)(2,1)S(1)}, bf16[48,2048]{1,0:T(8,128)(2,1)S(1)}, u32[]{:S(2)}, u32[]{:S(2)}) %collective-permute-start.36) | collective-permute-done | bytes 196640 | tf_op jit(solution)/shard_map/ppermute | solution.py:24
  169.4 3.1 %collective-permute-done.37 = bf16[48,2048]{1,0:T(8,128)(2,1)S(1)} collective-permute-done((bf16[48,2048]{1,0:T(8,128)(2,1)S(1)}, bf16[48,2048]{1,0:T(8,128)(2,1)S(1)}, u32[]{:S(2)}, u32[]{:S(2)}) %collective-permute-start.37) | collective-permute-done | bytes 196640 | tf_op jit(solution)/shard_map/ppermute | solution.py:24
  172.6 4.5 %collective-permute-start.39 = (bf16[144,2048]{1,0:T(8,128)(2,1)S(1)}, bf16[144,2048]{1,0:T(8,128)(2,1)S(1)}, u32[]{:S(2)}, u32[]{:S(2)}) collective-permute-start(bf16[144,2048]{1,0:T(8,128)(2,1)S(1)} %pad_maximum_fusion.2), channel_id=1, source_target_pairs={{0,1},{1,0},{2,3},{3,2},{4,5},{5,4},{6,7},{7,6},{8,9},{9,8},{10,11... | collective-permute-start | bytes 1769480 | tf_op jit(solution)/shard_map/ppermute | solution.py:24
  177.3 1.5 collective-permute-done.39
  179.1 5.7 %gated_hidden.1 = bf16[384,768]{1,0:T(8,128)(2,1)S(1)} custom-call(bf16[384,2048]{1,0:T(8,128)(2,1)S(1)} %constant_dynamic-update-slice_fusion.46.rows_ref, bf16[2048,2304]{1,0:T(8,128)(2,1)} %all-gather.5.cloned.1.call-done.gate_ref.up_ref, bf16[2048,2304]{1,0:T(8,128)(2,1)} %all-gather.5.cloned.1.call-done.gate_ref.up_ref), custom_call_target="tpu_custom_call" | custom-call | tf_op jit(solution)/shard_map/gated_hidden/pallas_call | solution.py:76
  188.9 1.5 collective-permute-start.44
  190.4 6.1 %collective-permute-done.42 = bf16[48,2048]{1,0:T(8,128)(2,1)S(1)} collective-permute-done((bf16[48,2048]{1,0:T(8,128)(2,1)S(1)}, bf16[48,2048]{1,0:T(8,128)(2,1)S(1)}, u32[]{:S(2)}, u32[]{:S(2)}) %collective-permute-start.42) | collective-permute-done | bytes 196640 | tf_op jit(solution)/shard_map/ppermute | solution.py:24
  197.6 3.8 %collective-permute-done.44 = bf16[48,2048]{1,0:T(8,128)(2,1)S(1)} collective-permute-done((bf16[48,2048]{1,0:T(8,128)(2,1)S(1)}, bf16[48,2048]{1,0:T(8,128)(2,1)S(1)}, u32[]{:S(2)}, u32[]{:S(2)}) %collective-permute-start.44) | collective-permute-done | bytes 196640 | tf_op jit(solution)/shard_map/ppermute | solution.py:24
  202.0 8.7 %all_to_all.10 = bf16[8,48,256]{2,1,0:T(8,128)(2,1)S(1)} all-to-all(bf16[8,48,256]{2,1,0:T(8,128)(2,1)S(1)} %bitcast.153), channel_id=1, replica_groups=mesh['fs'=16,'tp'=8] {'tp'}, dimensions={0} | all-to-all | bytes 393216 | tf_op jit(solution)/shard_map/all_to_all | solution.py:276
  (223 shorter events, 39.0 us)
Async XLA Ops:
  6.5 91.2 %all-gather.3.cloned.1.call-start = ((), (), s32[]{:S(2)}) async-start(), calls=%async_computation.2 | async-start | bytes 5013504 | tf_op jit(solution)/shard_map/all_gather | solution.py:184
  8.3 170.8 %all-gather.5.cloned.1.call-start = ((), (), s32[]{:S(2)}) async-start(), calls=%async_computation.3 | async-start | bytes 10027008 | tf_op jit(solution)/shard_map/all_gather | solution.py:197
  8.4 10.0 %collective-permute-start.4 = (bf16[128,768]{1,0:T(8,128)(2,1)}, bf16[128,768]{1,0:T(8,128)(2,1)S(1)}, u32[]{:S(2)}, u32[]{:S(2)}) collective-permute-start(bf16[128,768]{1,0:T(8,128)(2,1)} %param.17), channel_id=1, source_target_pairs={{0,24},{8,0},{16,8},{24,16},{32,56},{40,32},{48,40},{56,48},{64,88... | collective-permute-start | bytes 589832 | tf_op jit(solution)/shard_map/ppermute | solution.py:24
  12.0 9.1 %collective-permute-start.6 = (bf16[128,768]{1,0:T(8,128)(2,1)}, bf16[128,768]{1,0:T(8,128)(2,1)S(1)}, u32[]{:S(2)}, u32[]{:S(2)}) collective-permute-start(bf16[128,768]{1,0:T(8,128)(2,1)} %param.17), channel_id=1, source_target_pairs={{0,8},{8,16},{16,24},{24,0},{32,40},{40,48},{48,56},{56,32},{64,72... | collective-permute-start | bytes 589832 | tf_op jit(solution)/shard_map/ppermute | solution.py:24
  12.0 9.3 %collective-permute-start = (bf16[128,768]{1,0:T(8,128)(2,1)}, bf16[128,768]{1,0:T(8,128)(2,1)S(1)}, u32[]{:S(2)}, u32[]{:S(2)}) collective-permute-start(bf16[128,768]{1,0:T(8,128)(2,1)} %param.16), channel_id=1, source_target_pairs={{0,96},{8,104},{16,112},{24,120},{32,0},{40,8},{48,16},{56,24},{64... | collective-permute-start | bytes 589832 | tf_op jit(solution)/shard_map/ppermute | solution.py:24
  15.8 8.3 %collective-permute-start.2 = (bf16[128,768]{1,0:T(8,128)(2,1)}, bf16[128,768]{1,0:T(8,128)(2,1)S(1)}, u32[]{:S(2)}, u32[]{:S(2)}) collective-permute-start(bf16[128,768]{1,0:T(8,128)(2,1)} %param.16), channel_id=1, source_target_pairs={{0,32},{8,40},{16,48},{24,56},{32,64},{40,72},{48,80},{56,88},{64,... | collective-permute-start | bytes 589832 | tf_op jit(solution)/shard_map/ppermute | solution.py:24
  18.4 5.8 %collective-permute-start.5 = (bf16[64,768]{1,0:T(8,128)(2,1)S(1)}, bf16[64,768]{1,0:T(8,128)(2,1)S(1)}, u32[]{:S(2)}, u32[]{:S(2)}) collective-permute-start(bf16[64,768]{1,0:T(8,128)(2,1)S(1)} %slice.599), channel_id=1, source_target_pairs={{0,24},{8,0},{16,8},{24,16},{32,56},{40,32},{48,40},{56,48},{64,88... | collective-permute-start | bytes 294920 | tf_op jit(solution)/shard_map/ppermute | solution.py:24
  21.2 4.7 %collective-permute-start.7 = (bf16[64,768]{1,0:T(8,128)(2,1)S(1)}, bf16[64,768]{1,0:T(8,128)(2,1)S(1)}, u32[]{:S(2)}, u32[]{:S(2)}) collective-permute-start(bf16[64,768]{1,0:T(8,128)(2,1)S(1)} %slice.600), channel_id=1, source_target_pairs={{0,8},{8,16},{16,24},{24,0},{32,40},{40,48},{48,56},{56,32},{64,72... | collective-permute-start | bytes 294920 | tf_op jit(solution)/shard_map/ppermute | solution.py:24
  21.3 5.0 %collective-permute-start.1 = (bf16[64,768]{1,0:T(8,128)(2,1)S(1)}, bf16[64,768]{1,0:T(8,128)(2,1)S(1)}, u32[]{:S(2)}, u32[]{:S(2)}) collective-permute-start(bf16[64,768]{1,0:T(8,128)(2,1)S(1)} %slice.597), channel_id=1, source_target_pairs={{0,96},{8,104},{16,112},{24,120},{32,0},{40,8},{48,16},{56,24},{64... | collective-permute-start | bytes 294920 | tf_op jit(solution)/shard_map/ppermute | solution.py:24
  24.0 5.5 %collective-permute-start.3 = (bf16[64,768]{1,0:T(8,128)(2,1)S(1)}, bf16[64,768]{1,0:T(8,128)(2,1)S(1)}, u32[]{:S(2)}, u32[]{:S(2)}) collective-permute-start(bf16[64,768]{1,0:T(8,128)(2,1)S(1)} %slice.598), channel_id=1, source_target_pairs={{0,32},{8,40},{16,48},{24,56},{32,64},{40,72},{48,80},{56,88},{64,... | collective-permute-start | bytes 294920 | tf_op jit(solution)/shard_map/ppermute | solution.py:24
  31.7 6.7 %collective-permute-start.8 = (bf16[392,256]{1,0:T(8,128)(2,1)S(1)}, bf16[392,256]{1,0:T(8,128)(2,1)S(1)}, u32[]{:S(2)}, u32[]{:S(2)}) collective-permute-start(bf16[392,256]{1,0:T(8,128)(2,1)S(1)} %pad_maximum_fusion.4), channel_id=1, source_target_pairs={{0,1},{1,0},{2,3},{3,2},{4,5},{5,4},{6,7},{7,6},{8,9},{9,8},{10,11... | collective-permute-start | bytes 602120 | tf_op jit(solution)/shard_map/ppermute | solution.py:24
  34.4 10.9 %collective-permute-start.9 = (bf16[392,256]{1,0:T(8,128)(2,1)S(1)}, bf16[392,256]{1,0:T(8,128)(2,1)S(1)}, u32[]{:S(2)}, u32[]{:S(2)}) collective-permute-start(bf16[392,256]{1,0:T(8,128)(2,1)S(1)} %pad_maximum_fusion.4), channel_id=1, source_target_pairs={{0,6},{1,7},{2,0},{3,1},{4,2},{5,3},{6,4},{7,5},{8,14},{9,15},{10,... | collective-permute-start | bytes 602120 | tf_op jit(solution)/shard_map/ppermute | solution.py:24
  36.9 12.7 %collective-permute-start.11 = (bf16[392,256]{1,0:T(8,128)(2,1)S(1)}, bf16[392,256]{1,0:T(8,128)(2,1)S(1)}, u32[]{:S(2)}, u32[]{:S(2)}) collective-permute-start(bf16[392,256]{1,0:T(8,128)(2,1)S(1)} %pad_maximum_fusion.4), channel_id=1, source_target_pairs={{0,4},{1,5},{2,6},{3,7},{4,0},{5,1},{6,2},{7,3},{8,12},{9,13},{10,... | collective-permute-start | bytes 602120 | tf_op jit(solution)/shard_map/ppermute | solution.py:24
  37.6 13.7 %collective-permute-start.13 = (bf16[392,256]{1,0:T(8,128)(2,1)S(1)}, bf16[392,256]{1,0:T(8,128)(2,1)S(1)}, u32[]{:S(2)}, u32[]{:S(2)}) collective-permute-start(bf16[392,256]{1,0:T(8,128)(2,1)S(1)} %pad_maximum_fusion.4), channel_id=1, source_target_pairs={{0,2},{1,3},{2,4},{3,5},{4,6},{5,7},{6,0},{7,1},{8,10},{9,11},{10,... | collective-permute-start | bytes 602120 | tf_op jit(solution)/shard_map/ppermute | solution.py:24
  38.1 24.7 %collective-permute-start.19 = (bf16[512,768]{1,0:T(8,128)(2,1)}, bf16[512,768]{1,0:T(8,128)(2,1)S(1)}, u32[]{:S(2)}, u32[]{:S(2)}) collective-permute-start(bf16[512,768]{1,0:T(8,128)(2,1)} %copy-done.6), channel_id=1, source_target_pairs={{0,96},{8,104},{16,112},{24,120},{32,0},{40,8},{48,16},{56,24},{64... | collective-permute-start | bytes 2359304 | tf_op jit(solution)/shard_map/ppermute | solution.py:24
  38.4 26.0 %collective-permute-start.20 = (bf16[512,768]{1,0:T(8,128)(2,1)}, bf16[512,768]{1,0:T(8,128)(2,1)S(1)}, u32[]{:S(2)}, u32[]{:S(2)}) collective-permute-start(bf16[512,768]{1,0:T(8,128)(2,1)} %copy-done.6), channel_id=1, source_target_pairs={{0,32},{8,40},{16,48},{24,56},{32,64},{40,72},{48,80},{56,88},{64,... | collective-permute-start | bytes 2359304 | tf_op jit(solution)/shard_map/ppermute | solution.py:24
  45.4 30.5 %collective-permute-start.15 = (bf16[512,768]{1,0:T(8,128)(2,1)S(1)}, bf16[512,768]{1,0:T(8,128)(2,1)S(1)}, u32[]{:S(2)}, u32[]{:S(2)}) collective-permute-start(bf16[512,768]{1,0:T(8,128)(2,1)S(1)} %constant_dynamic-update-slice_fusion), channel_id=1, source_target_pairs={{0,24},{8,0},{16,8},{24,16},{32,56},{40,32},{48,40},{56,48},{64,88... | collective-permute-start | bytes 2359304 | tf_op jit(solution)/shard_map/ppermute | solution.py:24
  49.6 3.2 %collective-permute-start.10 = (bf16[392,256]{1,0:T(8,128)(2,1)S(1)}, bf16[392,256]{1,0:T(8,128)(2,1)S(1)}, u32[]{:S(2)}, u32[]{:S(2)}) collective-permute-start(bf16[392,256]{1,0:T(8,128)(2,1)S(1)} %collective-permute-done.9), channel_id=1, source_target_pairs={{0,1},{1,0},{2,3},{3,2},{4,5},{5,4},{6,7},{7,6},{8,9},{9,8},{10,11... | collective-permute-start | bytes 602120 | tf_op jit(solution)/shard_map/ppermute | solution.py:24
  51.3 1.5 collective-permute-start.12
  52.8 26.7 %collective-permute-start.16 = (bf16[512,768]{1,0:T(8,128)(2,1)S(1)}, bf16[512,768]{1,0:T(8,128)(2,1)S(1)}, u32[]{:S(2)}, u32[]{:S(2)}) collective-permute-start(bf16[512,768]{1,0:T(8,128)(2,1)S(1)} %constant_dynamic-update-slice_fusion), channel_id=1, source_target_pairs={{0,8},{8,16},{16,24},{24,0},{32,40},{40,48},{48,56},{56,32},{64,72... | collective-permute-start | bytes 2359304 | tf_op jit(solution)/shard_map/ppermute | solution.py:24
  52.9 1.5 collective-permute-start.14
  62.9 18.8 %collective-permute-start.21 = (bf16[256,768]{1,0:T(8,128)(2,1)S(1)}, bf16[256,768]{1,0:T(8,128)(2,1)S(1)}, u32[]{:S(2)}, u32[]{:S(2)}) collective-permute-start(bf16[256,768]{1,0:T(8,128)(2,1)S(1)} %slice.611), channel_id=1, source_target_pairs={{0,96},{8,104},{16,112},{24,120},{32,0},{40,8},{48,16},{56,24},{64... | collective-permute-start | bytes 1179656 | tf_op jit(solution)/shard_map/ppermute | solution.py:24
  64.4 19.2 %collective-permute-start.22 = (bf16[256,768]{1,0:T(8,128)(2,1)S(1)}, bf16[256,768]{1,0:T(8,128)(2,1)S(1)}, u32[]{:S(2)}, u32[]{:S(2)}) collective-permute-start(bf16[256,768]{1,0:T(8,128)(2,1)S(1)} %slice.612), channel_id=1, source_target_pairs={{0,32},{8,40},{16,48},{24,56},{32,64},{40,72},{48,80},{56,88},{64,... | collective-permute-start | bytes 1179656 | tf_op jit(solution)/shard_map/ppermute | solution.py:24
  75.8 15.7 %collective-permute-start.17 = (bf16[256,768]{1,0:T(8,128)(2,1)S(1)}, bf16[256,768]{1,0:T(8,128)(2,1)S(1)}, u32[]{:S(2)}, u32[]{:S(2)}) collective-permute-start(bf16[256,768]{1,0:T(8,128)(2,1)S(1)} %slice.609), channel_id=1, source_target_pairs={{0,24},{8,0},{16,8},{24,16},{32,56},{40,32},{48,40},{56,48},{64,88... | collective-permute-start | bytes 1179656 | tf_op jit(solution)/shard_map/ppermute | solution.py:24
  79.5 15.8 %collective-permute-start.18 = (bf16[256,768]{1,0:T(8,128)(2,1)S(1)}, bf16[256,768]{1,0:T(8,128)(2,1)S(1)}, u32[]{:S(2)}, u32[]{:S(2)}) collective-permute-start(bf16[256,768]{1,0:T(8,128)(2,1)S(1)} %slice.610), channel_id=1, source_target_pairs={{0,8},{8,16},{16,24},{24,0},{32,40},{40,48},{48,56},{56,32},{64,72... | collective-permute-start | bytes 1179656 | tf_op jit(solution)/shard_map/ppermute | solution.py:24
  100.6 2.8 %collective-permute-start.23 = (bf16[192,2048]{1,0:T(8,128)(2,1)S(1)}, bf16[192,2048]{1,0:T(8,128)(2,1)S(1)}, u32[]{:S(2)}, u32[]{:S(2)}) collective-permute-start(bf16[192,2048]{1,0:T(8,128)(2,1)S(1)} %fusion.8), channel_id=1, source_target_pairs={{0,1},{1,0},{2,3},{3,2},{4,5},{5,4},{6,7},{7,6},{8,9},{9,8},{10,11... | collective-permute-start | bytes 2359304 | tf_op jit(solution)/shard_map/ppermute | solution.py:24
  103.7 7.7 %collective-permute-start.24 = (bf16[48,2048]{1,0:T(8,128)(2,1)S(1)}, bf16[48,2048]{1,0:T(8,128)(2,1)S(1)}, u32[]{:S(2)}, u32[]{:S(2)}) collective-permute-start(bf16[48,2048]{1,0:T(8,128)(2,1)S(1)} %get-tuple-element.79), channel_id=1, source_target_pairs={{0,4},{1,5},{2,6},{3,7},{4,0},{5,1},{6,2},{7,3},{8,12},{9,13},{10,... | collective-permute-start | bytes 589832 | tf_op jit(solution)/shard_map/ppermute | solution.py:24
  106.2 9.5 %collective-permute-start.25 = (bf16[48,2048]{1,0:T(8,128)(2,1)S(1)}, bf16[48,2048]{1,0:T(8,128)(2,1)S(1)}, u32[]{:S(2)}, u32[]{:S(2)}) collective-permute-start(bf16[48,2048]{1,0:T(8,128)(2,1)S(1)} %get-tuple-element.81), channel_id=1, source_target_pairs={{0,6},{1,7},{2,0},{3,1},{4,2},{5,3},{6,4},{7,5},{8,14},{9,15},{10,... | collective-permute-start | bytes 589832 | tf_op jit(solution)/shard_map/ppermute | solution.py:24
  107.3 8.7 %collective-permute-start.26 = (bf16[48,2048]{1,0:T(8,128)(2,1)S(1)}, bf16[48,2048]{1,0:T(8,128)(2,1)S(1)}, u32[]{:S(2)}, u32[]{:S(2)}) collective-permute-start(bf16[48,2048]{1,0:T(8,128)(2,1)S(1)} %get-tuple-element.80), channel_id=1, source_target_pairs={{0,2},{1,3},{2,4},{3,5},{4,6},{5,7},{6,0},{7,1},{8,10},{9,11},{10,... | collective-permute-start | bytes 589832 | tf_op jit(solution)/shard_map/ppermute | solution.py:24
  116.6 6.6 %collective-permute-start.27 = (bf16[48,2048]{1,0:T(8,128)(2,1)S(1)}, bf16[48,2048]{1,0:T(8,128)(2,1)S(1)}, u32[]{:S(2)}, u32[]{:S(2)}) collective-permute-start(bf16[48,2048]{1,0:T(8,128)(2,1)S(1)} %get-tuple-element.44), channel_id=1, source_target_pairs={{0,6},{1,7},{2,0},{3,1},{4,2},{5,3},{6,4},{7,5},{8,14},{9,15},{10,... | collective-permute-start | bytes 589832 | tf_op jit(solution)/shard_map/ppermute | solution.py:24
  119.5 8.1 %collective-permute-start.28 = (bf16[48,2048]{1,0:T(8,128)(2,1)S(1)}, bf16[48,2048]{1,0:T(8,128)(2,1)S(1)}, u32[]{:S(2)}, u32[]{:S(2)}) collective-permute-start(bf16[48,2048]{1,0:T(8,128)(2,1)S(1)} %get-tuple-element.44), channel_id=1, source_target_pairs={{0,2},{1,3},{2,4},{3,5},{4,6},{5,7},{6,0},{7,1},{8,10},{9,11},{10,... | collective-permute-start | bytes 589832 | tf_op jit(solution)/shard_map/ppermute | solution.py:24
  119.5 12.9 %collective-permute-start.29 = (bf16[48,2048]{1,0:T(8,128)(2,1)S(1)}, bf16[48,2048]{1,0:T(8,128)(2,1)S(1)}, u32[]{:S(2)}, u32[]{:S(2)}) collective-permute-start(bf16[48,2048]{1,0:T(8,128)(2,1)S(1)} %get-tuple-element.44), channel_id=1, source_target_pairs={{0,4},{1,5},{2,6},{3,7},{4,0},{5,1},{6,2},{7,3},{8,12},{9,13},{10,... | collective-permute-start | bytes 589832 | tf_op jit(solution)/shard_map/ppermute | solution.py:24
  127.7 6.3 %collective-permute-start.30 = (bf16[144,2048]{1,0:T(8,128)(2,1)S(1)}, bf16[144,2048]{1,0:T(8,128)(2,1)S(1)}, u32[]{:S(2)}, u32[]{:S(2)}) collective-permute-start(bf16[144,2048]{1,0:T(8,128)(2,1)S(1)} %pad_maximum_fusion.1), channel_id=1, source_target_pairs={{0,1},{1,0},{2,3},{3,2},{4,5},{5,4},{6,7},{7,6},{8,9},{9,8},{10,11... | collective-permute-start | bytes 1769480 | tf_op jit(solution)/shard_map/ppermute | solution.py:24
  132.4 1.9 collective-permute-start.31
  136.9 8.4 %all-to-all-start = ((f32[8,1,768]{2,1,0:T(1,128)}), f32[8,1,768]{2,1,0:T(1,128)S(1)}, u32[]{:S(2)}, u32[]{:S(2)}) async-start(f32[8,1,768]{2,1,0:T(1,128)} %broadcast_in_dim.2), calls=%async_computation | async-start | bytes 49152 | tf_op jit(solution)/shard_map/all_to_all | solution.py:153
  147.0 2.7 %collective-permute-start.32 = (bf16[192,2048]{1,0:T(8,128)(2,1)S(1)}, bf16[192,2048]{1,0:T(8,128)(2,1)S(1)}, u32[]{:S(2)}, u32[]{:S(2)}) collective-permute-start(bf16[192,2048]{1,0:T(8,128)(2,1)S(1)} %convolution_convert_fusion), channel_id=1, source_target_pairs={{0,1},{1,0},{2,3},{3,2},{4,5},{5,4},{6,7},{7,6},{8,9},{9,8},{10,11... | collective-permute-start | bytes 2359304 | tf_op jit(solution)/shard_map/ppermute | solution.py:24
  150.0 7.7 %collective-permute-start.33 = (bf16[48,2048]{1,0:T(8,128)(2,1)S(1)}, bf16[48,2048]{1,0:T(8,128)(2,1)S(1)}, u32[]{:S(2)}, u32[]{:S(2)}) collective-permute-start(bf16[48,2048]{1,0:T(8,128)(2,1)S(1)} %get-tuple-element.76), channel_id=1, source_target_pairs={{0,4},{1,5},{2,6},{3,7},{4,0},{5,1},{6,2},{7,3},{8,12},{9,13},{10,... | collective-permute-start | bytes 589832 | tf_op jit(solution)/shard_map/ppermute | solution.py:24
  150.9 9.5 %collective-permute-start.34 = (bf16[48,2048]{1,0:T(8,128)(2,1)S(1)}, bf16[48,2048]{1,0:T(8,128)(2,1)S(1)}, u32[]{:S(2)}, u32[]{:S(2)}) collective-permute-start(bf16[48,2048]{1,0:T(8,128)(2,1)S(1)} %get-tuple-element.78), channel_id=1, source_target_pairs={{0,6},{1,7},{2,0},{3,1},{4,2},{5,3},{6,4},{7,5},{8,14},{9,15},{10,... | collective-permute-start | bytes 589832 | tf_op jit(solution)/shard_map/ppermute | solution.py:24
  152.8 9.8 %collective-permute-start.35 = (bf16[48,2048]{1,0:T(8,128)(2,1)S(1)}, bf16[48,2048]{1,0:T(8,128)(2,1)S(1)}, u32[]{:S(2)}, u32[]{:S(2)}) collective-permute-start(bf16[48,2048]{1,0:T(8,128)(2,1)S(1)} %get-tuple-element.77), channel_id=1, source_target_pairs={{0,2},{1,3},{2,4},{3,5},{4,6},{5,7},{6,0},{7,1},{8,10},{9,11},{10,... | collective-permute-start | bytes 589832 | tf_op jit(solution)/shard_map/ppermute | solution.py:24
  163.3 6.2 %collective-permute-start.36 = (bf16[48,2048]{1,0:T(8,128)(2,1)S(1)}, bf16[48,2048]{1,0:T(8,128)(2,1)S(1)}, u32[]{:S(2)}, u32[]{:S(2)}) collective-permute-start(bf16[48,2048]{1,0:T(8,128)(2,1)S(1)} %get-tuple-element.36), channel_id=1, source_target_pairs={{0,6},{1,7},{2,0},{3,1},{4,2},{5,3},{6,4},{7,5},{8,14},{9,15},{10,... | collective-permute-start | bytes 589832 | tf_op jit(solution)/shard_map/ppermute | solution.py:24
  164.3 8.3 %collective-permute-start.37 = (bf16[48,2048]{1,0:T(8,128)(2,1)S(1)}, bf16[48,2048]{1,0:T(8,128)(2,1)S(1)}, u32[]{:S(2)}, u32[]{:S(2)}) collective-permute-start(bf16[48,2048]{1,0:T(8,128)(2,1)S(1)} %get-tuple-element.36), channel_id=1, source_target_pairs={{0,2},{1,3},{2,4},{3,5},{4,6},{5,7},{6,0},{7,1},{8,10},{9,11},{10,... | collective-permute-start | bytes 589832 | tf_op jit(solution)/shard_map/ppermute | solution.py:24
  164.8 12.4 %collective-permute-start.38 = (bf16[48,2048]{1,0:T(8,128)(2,1)S(1)}, bf16[48,2048]{1,0:T(8,128)(2,1)S(1)}, u32[]{:S(2)}, u32[]{:S(2)}) collective-permute-start(bf16[48,2048]{1,0:T(8,128)(2,1)S(1)} %get-tuple-element.36), channel_id=1, source_target_pairs={{0,4},{1,5},{2,6},{3,7},{4,0},{5,1},{6,2},{7,3},{8,12},{9,13},{10,... | collective-permute-start | bytes 589832 | tf_op jit(solution)/shard_map/ppermute | solution.py:24
  172.6 6.2 %collective-permute-start.39 = (bf16[144,2048]{1,0:T(8,128)(2,1)S(1)}, bf16[144,2048]{1,0:T(8,128)(2,1)S(1)}, u32[]{:S(2)}, u32[]{:S(2)}) collective-permute-start(bf16[144,2048]{1,0:T(8,128)(2,1)S(1)} %pad_maximum_fusion.2), channel_id=1, source_target_pairs={{0,1},{1,0},{2,3},{3,2},{4,5},{5,4},{6,7},{7,6},{8,9},{9,8},{10,11... | collective-permute-start | bytes 1769480 | tf_op jit(solution)/shard_map/ppermute | solution.py:24
  177.2 1.9 collective-permute-start.40
  186.0 2.4 %collective-permute-start.41 = (bf16[192,2048]{1,0:T(8,128)(2,1)S(1)}, bf16[192,2048]{1,0:T(8,128)(2,1)S(1)}, u32[]{:S(2)}, u32[]{:S(2)}) collective-permute-start(bf16[192,2048]{1,0:T(8,128)(2,1)S(1)} %fusion.11), channel_id=1, source_target_pairs={{0,1},{1,0},{2,3},{3,2},{4,5},{5,4},{6,7},{7,6},{8,9},{9,8},{10,11... | collective-permute-start | bytes 2359304 | tf_op jit(solution)/shard_map/ppermute | solution.py:24
  188.7 7.7 %collective-permute-start.42 = (bf16[48,2048]{1,0:T(8,128)(2,1)S(1)}, bf16[48,2048]{1,0:T(8,128)(2,1)S(1)}, u32[]{:S(2)}, u32[]{:S(2)}) collective-permute-start(bf16[48,2048]{1,0:T(8,128)(2,1)S(1)} %get-tuple-element.73), channel_id=1, source_target_pairs={{0,4},{1,5},{2,6},{3,7},{4,0},{5,1},{6,2},{7,3},{8,12},{9,13},{10,... | collective-permute-start | bytes 589832 | tf_op jit(solution)/shard_map/ppermute | solution.py:24
  188.8 8.7 %collective-permute-start.43 = (bf16[48,2048]{1,0:T(8,128)(2,1)S(1)}, bf16[48,2048]{1,0:T(8,128)(2,1)S(1)}, u32[]{:S(2)}, u32[]{:S(2)}) collective-permute-start(bf16[48,2048]{1,0:T(8,128)(2,1)S(1)} %get-tuple-element.75), channel_id=1, source_target_pairs={{0,6},{1,7},{2,0},{3,1},{4,2},{5,3},{6,4},{7,5},{8,14},{9,15},{10,... | collective-permute-start | bytes 589832 | tf_op jit(solution)/shard_map/ppermute | solution.py:24
  188.9 12.4 %collective-permute-start.44 = (bf16[48,2048]{1,0:T(8,128)(2,1)S(1)}, bf16[48,2048]{1,0:T(8,128)(2,1)S(1)}, u32[]{:S(2)}, u32[]{:S(2)}) collective-permute-start(bf16[48,2048]{1,0:T(8,128)(2,1)S(1)} %get-tuple-element.74), channel_id=1, source_target_pairs={{0,2},{1,3},{2,4},{3,5},{4,6},{5,7},{6,0},{7,1},{8,10},{9,11},{10,... | collective-permute-start | bytes 589832 | tf_op jit(solution)/shard_map/ppermute | solution.py:24
  (12 other events, 77.9 us)
Sparse Core Ops, SparseCore 0:
  9.4 82.0 all-gather.2
  93.6 76.5 all-gather.4
